TPU v7x, 256 devices: a 4x2x16 block of a 4x16x16 slice. The times are simulated.
256 devices in a mesh: grp: 2 (over y), sp: 32 (over z, core), tp: 4 (over x).
Axes of the slice: x: 4, y: 2, z: 16, core: 2. Of those that a mesh axis runs over, the one named last changes fastest.
The devices are a block of a 4x16x16 slice.
Arguments:
- skip_stream: bfloat16 [8192, 2048], P(('grp', 'sp', 'tp')), parts along dimension 0, may hold values from -6 to 6
- wide_probe_logits: bfloat16 [8192, 512], P(('grp', 'sp'), 'tp'), parts along dimension 0, may hold values from -6 to 6
- narrow_probe_logits: bfloat16 [8192, 512], P(('grp', 'sp'), 'tp'), parts along dimension 0, may hold values from -6 to 6
- wide_decay_logits: bfloat16 [8192, 512], P(('grp', 'sp'), 'tp'), parts along dimension 0, may hold values from -7.5 to 7.5
- narrow_decay_logits: bfloat16 [8192, 512], P(('grp', 'sp'), 'tp'), parts along dimension 0, may hold values from -7.5 to 7.5
- wide_floor_complement: float32 [2, 512], P(None, 'tp'), may hold values from 3.4179688e-05 to 0.21
- narrow_floor_complement: float32 [2, 512], P(None, 'tp'), may hold values from 3.4179688e-05 to 0.21
- payloads: bfloat16 [8192, 1536], P(('grp', 'sp'), 'tp'), parts along dimension 0, may hold values from -6 to 6
- result_switch_logits: bfloat16 [8192, 1536], P(('grp', 'sp'), 'tp'), parts along dimension 0, may hold values from -6 to 6
- spike_decays: float32 [8192, 12], P(('grp', 'sp'), 'tp'), parts along dimension 0, may hold values from -1.5 to 0
- channel_scale_vector: float32 [1536], P('tp'), may hold values from 0.1 to 1.9
- result_mapping_matrix: bfloat16 [1536, 2048], P('tp'), may hold values from -0.15625 to 0.15625
- specialist_scale_vector: float32 [2048], replicated, may hold values from 0.1 to 1.9
- assignments: int32 [8192, 2], P(('grp', 'sp', 'tp')), parts along dimension 0, may hold values from 0 to 31, all different within a row; in each aligned block of 32 rows (0 to 31, 32 to 63, ...) at most 4 rows name the same one
- assignment_share: float32 [8192, 2], P(('grp', 'sp', 'tp')), parts along dimension 0, may hold values from 0.2 to 1
- specialist_switch_matrix: bfloat16 [32, 2048, 3584], P('sp', None, 'tp'), may hold values from -0.125 to 0.125
- specialist_raising_matrix: bfloat16 [32, 2048, 3584], P('sp', None, 'tp'), may hold values from -0.125 to 0.125
- specialist_lowering_matrix: bfloat16 [32, 3584, 2048], P('sp', 'tp'), may hold values from -0.09375 to 0.09375
Outputs:
- layer_output: bfloat16 [8192, 2048], P(('grp', 'sp', 'tp')), parts along dimension 0
There are 2 independent parts, one for each index of `grp`. A program takes and returns all parts, laid end to end along the dimension named above; an argument that names none is the same for every part. Nothing has to cross between parts.
Inputs may be any that keep to these rules, and one draw needn't show every extreme that they name: `assignments`: each row names 2 different experts; in each aligned block of 32 rows no expert is named by more than 4 rows, a bound that some block reaches.
All inputs are finite; a program needn't handle non-finite values.
Results may differ from a plain program's by a relative error of at most 0.015.
Values may be sent and summed in bfloat16 or wider, within the bound.
No kernel may reach another device: no remote copies, remote signals or barrier semaphores. Data moves between devices by JAX's collectives and lax.ppermute only.
A program may use at most 128 MiB of HBM per device.

v0:
```python
import jax
import jax.numpy as jnp
from jax import lax
from jax.experimental import pallas as pl
from jax.experimental.pallas import tpu as pltpu
from jax.sharding import Mesh
from jax.sharding import PartitionSpec as P

F32 = jnp.float32
BF16 = jnp.bfloat16
EPS = 1e-06
HALF = 64
SLICE = 32
PAY = 80
CAP = 4
ZG = ("zl", "c")
SP = ("zh", "zl", "c")
GRP_SP = ("grp", "zh", "zl", "c")
GRP_SP_TP = ("grp", "zh", "zl", "c", "tp")


def dot(a, b, contract=(1, 0), precision=None):
    dims = (((contract[0],), (contract[1],)), ((), ()))
    return lax.dot_general(a, b, dims, precision=precision, preferred_element_type=F32)


def iota(shape, axis):
    return lax.broadcasted_iota(jnp.int32, shape, axis)


def split_parts(x):
    hi = x.astype(BF16)
    return hi, (x - hi.astype(F32)).astype(BF16)


def key_and_decay(logits, leaks, spikes):
    gate = jax.nn.sigmoid(-logits.astype(F32))
    rows = [leaks[d : d + 1] * gate for d in range(2)]
    return rows, [jnp.log1p(-k) + spikes for k in rows]


def scan_terms(wd, nd, wleak, nleak, spk):
    n, width = wd.shape
    exact = lax.Precision.HIGHEST
    heads = spk.shape[0]
    lane = iota((heads, 2 * width), 1)
    owner = jnp.where(lane < width, 0, jnp.where(lane < 3 * width // 2, 1, 2))
    spikes = dot(spk, (iota((heads, 2 * width), 0) == owner).astype(F32), (0, 0), exact)
    kw, aw = key_and_decay(wd, wleak, spikes[:, :width])
    kn, an = key_and_decay(nd, nleak, spikes[:, width:])
    row, col = iota((n, n), 0), iota((n, n), 1)
    fwd = dot((row >= col).astype(F32), jnp.concatenate([aw[0], an[0]], axis=1), precision=exact)
    bwd = dot((row <= col).astype(F32), jnp.concatenate([aw[1], an[1]], axis=1), precision=exact)
    keys = [jnp.concatenate([kw[d], kn[d]], axis=1) for d in range(2)]
    return keys, (fwd, bwd)


def decay_rows(rows):
    width = rows[0].shape[1]
    at = iota((16, width), 0)
    block = jnp.zeros((16, width), F32)
    for n, row in enumerate(rows):
        hi = row.astype(BF16).astype(F32)
        block = jnp.where(at == 2 * n, hi, block)
        block = jnp.where(at == 2 * n + 1, row - hi, block)
    return block.astype(BF16)


def summary_kernel(wd, nd, wleak, nleak, v, spk, out):
    keys, running = scan_terms(wd[...], nd[...], wleak[...], nleak[...], spk[...])
    n, width = wd.shape
    values = v[...]
    last = (n - 1, 0)
    rows = []
    for d in range(2):
        closing = running[d][last[d] : last[d] + 1]
        fresh = (keys[d] * jnp.exp(closing - running[d])).astype(BF16)
        wide = dot(fresh[:, :width], values[:, :width], (0, 0))
        both = dot(fresh[:, width:], values[:, width:], (0, 0))
        slim = jnp.where(iota((width, width), 0) < width // 2, both[:, :width], both[:, width:])
        state = jnp.concatenate([wide, slim], axis=0).astype(BF16)
        for j in range(out.shape[0]):
            out[j, d * SLICE : (d + 1) * SLICE, :] = state[j * SLICE : (j + 1) * SLICE]
        rows += [closing[:, :width], closing[:, width:]]
    block = decay_rows(rows)
    for j in range(out.shape[0]):
        out[j, 2 * SLICE :, :] = block


def local_kernel(wp, np_, wd, nd, wleak, nleak, v, spk, o_ref, qf_ref, qb_ref):
    keys, running = scan_terms(wd[...], nd[...], wleak[...], nleak[...], spk[...])
    _, width = wd.shape
    q = jnp.concatenate(
        [
            jax.nn.silu(wp[...].astype(F32)) * width ** (-0.5),
            jax.nn.silu(np_[...].astype(F32)) * (width // 2) ** (-0.5),
        ],
        axis=1,
    )
    qf_ref[...] = (q * jnp.exp(running[0])).astype(BF16)
    qb_ref[...] = (q * jnp.exp(running[1])).astype(BF16)
    lane = iota((HALF, 2 * width), 1)
    heads = (lane < width, (lane >= width) & (lane < 3 * width // 2), lane >= 3 * width // 2)
    row, col = iota((HALF, HALF), 0), iota((HALF, HALF), 1)

    def pair(d, t, s, ref):
        rt = running[d][t * HALF : (t + 1) * HALF]
        rs = running[d][s * HALF : (s + 1) * HALF]
        base = running[d][ref : ref + 1]
        qs = q[t * HALF : (t + 1) * HALF] * jnp.exp(rt - base)
        ks = (keys[d][s * HALF : (s + 1) * HALF] * jnp.exp(base - rs)).astype(BF16)
        return qs, ks

    mid = HALF // 2
    terms = {
        (0, 0): [(0, pair(0, 0, 0, mid - 1)), (1, pair(1, 0, 0, mid))],
        (1, 1): [(0, pair(0, 1, 1, HALF + mid - 1)), (1, pair(1, 1, 1, HALF + mid))],
        (1, 0): [(None, pair(0, 1, 0, HALF - 1))],
        (0, 1): [(None, pair(1, 0, 1, HALF))],
    }

    def scores(block, head):
        total = None
        for d, (qs, ks) in terms[block]:
            lo = 0 if head == 0 else width
            picked = jnp.where(heads[head], qs, 0.0)[:, lo : lo + width].astype(BF16)
            part = dot(picked, ks[:, lo : lo + width], (1, 1))
            if d is not None:
                part = jnp.where(row >= col if d == 0 else row <= col, part, 0.0)
            total = part if total is None else total + part
        return total

    for head in range(3):
        full = jnp.concatenate(
            [
                jnp.concatenate([scores((0, 0), head), scores((0, 1), head)], axis=1),
                jnp.concatenate([scores((1, 0), head), scores((1, 1), head)], axis=1),
            ],
            axis=0,
        ).astype(BF16)
        at = slice(head * width, (head + 1) * width)
        o_ref[:, at] = dot(full, v[:, at])


def pick_column(block, d, member):
    width = block.shape[1]
    per = width // SLICE
    rows = block.astype(F32)
    wide = rows[4 * d : 4 * d + 1] + rows[4 * d + 1 : 4 * d + 2]
    slim = rows[4 * d + 2 : 4 * d + 3] + rows[4 * d + 3 : 4 * d + 4]
    row = jnp.where(member >= per, slim, wide)
    want = iota((SLICE, width), 0) + SLICE * (member % per)
    hit = iota((SLICE, width), 1) == want
    return jnp.sum(jnp.where(hit, row, 0.0), axis=1, keepdims=True)


def group_kernel(place, got, pre_ref, dec_ref, tot_ref):
    member = place[1]
    count, _, width = got.shape
    summed = jnp.zeros((16, width), F32)
    for i in range(count):
        summed = summed + got[i, 2 * SLICE :, :].astype(F32)
    for d in range(2):
        at = slice(d * SLICE, (d + 1) * SLICE)
        state = jnp.zeros((SLICE, width), F32)
        total = jnp.zeros((SLICE, 1), F32)
        for i in range(count) if d == 0 else reversed(range(count)):
            pre_ref[i, at, :] = state
            dec_ref[i, at, :] = jnp.broadcast_to(jnp.exp(total), (SLICE, width))
            column = pick_column(got[i, 2 * SLICE :, :], d, member)
            state = jnp.exp(column) * state + got[i, at, :].astype(F32)
            total = total + column
        tot_ref[at, :] = state.astype(BF16)
    rows = [summed[2 * n : 2 * n + 1] + summed[2 * n + 1 : 2 * n + 2] for n in range(4)]
    tot_ref[2 * SLICE :, :] = decay_rows(rows)


def carry_kernel(place, r1, r2, r3, pre, dec, out):
    group, member, groups = place[0], place[1], place[2]
    count, _, width = pre.shape
    came = {1: r1, 2: r2, 3: r3}
    for d in range(2):
        at = slice(d * SLICE, (d + 1) * SLICE)
        carry = jnp.zeros((SLICE, width), F32)
        for back in (3, 2, 1):
            ref = came[back] if d == 0 else came[4 - back]
            live = group - back >= 0 if d == 0 else group + back < groups
            column = pick_column(ref[2 * SLICE :, :], d, member)
            moved = jnp.exp(column) * carry + ref[at, :].astype(F32)
            carry = jnp.where(live, moved, carry)
        for i in range(count):
            out[i, at, :] = (pre[i, at, :] + dec[i, at, :] * carry).astype(BF16)


def mix_kernel(states, o_ref, qf, qb, gate, gain, proj, out):
    n, width = o_ref.shape[0], states.shape[2]
    members = states.shape[0]
    entering = [
        jnp.concatenate(
            [states[j, d * SLICE : (d + 1) * SLICE, :] for j in range(members)], axis=0
        )
        for d in range(2)
    ]
    low = iota((n, width), 1) < width // 2
    mixed = []
    for head in range(3):
        at = slice(head * width, (head + 1) * width)
        total = o_ref[:, at]
        for d, q in enumerate((qf, qb)):
            if head == 0:
                total = total + dot(q[:, :width], entering[d][:width])
            else:
                keep = low if head == 1 else jnp.logical_not(low)
                own = jnp.where(keep, q[:, width:].astype(F32), 0.0).astype(BF16)
                total = total + dot(own, entering[d][width:])
        total = total * lax.rsqrt(jnp.mean(total * total, axis=1, keepdims=True) + EPS)
        total = total * gain[:, at] * jax.nn.silu(gate[:, at].astype(F32))
        mixed.append(total.astype(BF16))
    out[...] = dot(jnp.concatenate(mixed, axis=1), proj[...]).astype(BF16)


def slot_matrix(routes):
    rows = routes.shape[1]
    slots = 32 * CAP
    expert = iota((slots, rows), 0) // CAP
    first = routes[0:1] == expert
    second = routes[1:2] == expert
    named = jnp.logical_or(first, second)
    before = (iota((rows, rows), 0) < iota((rows, rows), 1)).astype(F32).astype(BF16)
    rank = dot(named.astype(F32).astype(BF16), before)
    placed = rank.astype(jnp.int32) == iota((slots, rows), 0) % CAP
    return jnp.logical_and(first, placed), jnp.logical_and(second, placed)


def dispatch_kernel(parts, skip, gain, routes, hidden_ref, out):
    mixing = parts[0].astype(F32)
    for k in range(1, parts.shape[0]):
        mixing = mixing + parts[k].astype(F32)
    hidden_bf = (skip[...].astype(F32) + mixing).astype(BF16)
    hidden_ref[...] = hidden_bf
    hidden = hidden_bf.astype(F32)
    normed = hidden * lax.rsqrt(jnp.mean(hidden * hidden, axis=1, keepdims=True) + EPS)
    normed = (normed * gain[...]).astype(BF16)
    first, second = slot_matrix(routes[...])
    chosen = jnp.logical_or(first, second).astype(F32).astype(BF16)
    out[...] = dot(chosen, normed).astype(BF16)


def expert_part(rows, wg, wu, wd):
    gate = jnp.dot(rows, wg, preferred_element_type=F32)
    up = jnp.dot(rows, wu, preferred_element_type=F32)
    act = (jax.nn.silu(gate) * up).astype(BF16)
    return jnp.dot(act, wd, preferred_element_type=F32).astype(BF16)


def combine_kernel(hidden, back, routes, share, out):
    first, second = slot_matrix(routes[...])
    weight = jnp.where(first, share[0:1], 0.0) + jnp.where(second, share[1:2], 0.0)
    hi, lo = split_parts(weight)
    rows = back[...]
    mixture = dot(hi, rows, (0, 0)) + dot(lo, rows, (0, 0))
    out[...] = (hidden[...].astype(F32) + mixture).astype(BF16)


def sds(shape, dtype):
    return jax.ShapeDtypeStruct(shape, dtype)


VMEM = pl.BlockSpec(memory_space=pltpu.VMEM)
SMEM = pl.BlockSpec(memory_space=pltpu.SMEM)


def cost(flops):
    return pl.CostEstimate(flops=flops, bytes_accessed=1 << 20, transcendentals=0)


def local(
    skip_stream,
    wide_probe_logits,
    narrow_probe_logits,
    wide_decay_logits,
    narrow_decay_logits,
    wide_floor_complement,
    narrow_floor_complement,
    payloads,
    result_switch_logits,
    spike_decays,
    channel_scale_vector,
    result_mapping_matrix,
    specialist_scale_vector,
    assignments,
    assignment_share,
    specialist_switch_matrix,
    specialist_raising_matrix,
    specialist_lowering_matrix,
):
    tokens, width = wide_probe_logits.shape
    rows, model = skip_stream.shape
    joint = payloads.shape[1]
    members = lax.axis_size(ZG)
    groups = lax.axis_size("zh")
    shards = lax.axis_size("tp")
    experts = lax.axis_size(SP)
    place = jnp.stack(
        [lax.axis_index("zh"), lax.axis_index(ZG), jnp.int32(groups)]
    ).astype(jnp.int32)
    decay_args = (
        wide_decay_logits,
        narrow_decay_logits,
        wide_floor_complement,
        narrow_floor_complement,
        payloads,
        spike_decays.T,
    )

    summary = pl.pallas_call(
        summary_kernel, out_shape=sds((members, PAY, width), BF16), cost_estimate=cost(4 << 20)
    )(*decay_args)
    by_slice = lax.all_to_all(summary, ZG, 0, 0, tiled=True)
    inside, q_fwd, q_bwd = pl.pallas_call(
        local_kernel,
        out_shape=[
            sds((tokens, joint), F32),
            sds((tokens, 2 * width), BF16),
            sds((tokens, 2 * width), BF16),
        ],
        cost_estimate=cost(64 << 20),
    )(wide_probe_logits, narrow_probe_logits, *decay_args)
    before, decayed, total = pl.pallas_call(
        group_kernel,
        in_specs=[SMEM, VMEM],
        out_shape=[
            sds((members, 2 * SLICE, width), F32),
            sds((members, 2 * SLICE, width), F32),
            sds((PAY, width), BF16),
        ],
        cost_estimate=cost(4 << 20),
    )(place, by_slice)
    came = [
        lax.ppermute(total, "zh", [(i, (i + k) % groups) for i in range(groups)])
        for k in (1, 2, 3)
    ]
    carried = pl.pallas_call(
        carry_kernel,
        in_specs=[SMEM] + [VMEM] * 5,
        out_shape=sds((members, 2 * SLICE, width), BF16),
        cost_estimate=cost(4 << 20),
    )(place, *came, before, decayed)
    entering = lax.all_to_all(carried, ZG, 0, 0, tiled=True)
    mixed = pl.pallas_call(
        mix_kernel, out_shape=sds((tokens, model), BF16), cost_estimate=cost(256 << 20)
    )(
        entering,
        inside,
        q_fwd,
        q_bwd,
        result_switch_logits,
        channel_scale_vector.reshape(1, joint),
        result_mapping_matrix,
    )
    parts = lax.all_to_all(mixed.reshape(shards, rows, model), "tp", 0, 0, tiled=True)
    routes = assignments.T
    share = assignment_share.T
    slots = experts * CAP
    hidden, outgoing = pl.pallas_call(
        dispatch_kernel,
        out_shape=[sds((rows, model), BF16), sds((slots, model), BF16)],
        cost_estimate=cost(16 << 20),
    )(parts, skip_stream, specialist_scale_vector.reshape(1, model), routes)
    own = lax.all_to_all(outgoing.reshape(experts, CAP, model), SP, 0, 0, tiled=True)
    own = own.reshape(slots, model)

    up_ring = [(i, (i + 1) % shards) for i in range(shards)]
    down_ring = [(i, (i - 1) % shards) for i in range(shards)]
    up = lambda x: lax.ppermute(x, "tp", up_ring)
    down = lambda x: lax.ppermute(x, "tp", down_ring)
    half = slots // 2
    weights = (
        specialist_switch_matrix[0],
        specialist_raising_matrix[0],
        specialist_lowering_matrix[0],
    )
    hold = lax.optimization_barrier
    from_left = up(own)
    from_right = down(own)
    own_part = expert_part(own, *weights)
    from_left, from_right, own_part = hold((from_left, from_right, own_part))
    far_low = up(from_left[:half])
    far_high = down(from_right[half:])
    left_part = expert_part(from_left, *weights)
    right_part = expert_part(from_right, *weights)
    far_low, far_high, left_part, right_part = hold((far_low, far_high, left_part, right_part))
    left_got_high = up(right_part[half:])
    right_got_low = down(left_part[:half])
    opposite = expert_part(jnp.concatenate([far_low, far_high], axis=0), *weights)
    add_low, add_high = up(opposite[:half]), down(opposite[half:])
    joined = lambda a, b: (a.astype(F32) + b.astype(F32)).astype(BF16)
    left_got_low = up(joined(right_part[:half], add_low))
    right_got_high = down(joined(left_part[half:], add_high))
    f = lambda x: x.astype(F32)
    summed = jnp.concatenate(
        [
            (f(own_part[:half]) + f(left_got_low) + f(right_got_low)).astype(BF16),
            (f(own_part[half:]) + f(left_got_high) + f(right_got_high)).astype(BF16),
        ],
        axis=0,
    )
    back = lax.all_to_all(summed.reshape(experts, CAP, model), SP, 0, 0, tiled=True)
    return pl.pallas_call(
        combine_kernel, out_shape=sds((rows, model), BF16), cost_estimate=cost(16 << 20)
    )(hidden, back.reshape(slots, model), routes, share)


def solution(mesh):
    torus = Mesh(
        mesh.devices.reshape(mesh.shape["grp"], 4, 4, 2, mesh.shape["tp"]),
        GRP_SP_TP,
    )
    placed = (
        P(GRP_SP_TP, None),
        P(GRP_SP, "tp"),
        P(GRP_SP, "tp"),
        P(GRP_SP, "tp"),
        P(GRP_SP, "tp"),
        P(None, "tp"),
        P(None, "tp"),
        P(GRP_SP, "tp"),
        P(GRP_SP, "tp"),
        P(GRP_SP, "tp"),
        P("tp"),
        P("tp", None),
        P(),
        P(GRP_SP_TP, None),
        P(GRP_SP_TP, None),
        P(SP, None, "tp"),
        P(SP, None, "tp"),
        P(SP, "tp", None),
    )
    return jax.shard_map(
        local, mesh=torus, in_specs=placed, out_specs=P(GRP_SP_TP, None), check_vma=False
    )
```

profile of v0, /device:TPU:33, one launch (start us, length us, event | category | flops | bytes accessed | tf_op | source)
XLA Modules:
  0.0 232.2 jit_solution(5121936018428364212)
XLA Ops:
  0.0 2.7 %shard_map.172 = bf16[8,80,128]{2,1,0:T(8,128)(2,1)} custom-call(bf16[128,128]{1,0:T(8,128)(2,1)} %wd.3, bf16[128,128]{1,0:T(8,128)(2,1)} %nd.3, f32[2,128]{1,0:T(2,128)} %wleak.3, f32[2,128]{1,0:T(2,128)} %nleak.3, bf16[128,384]{1,0:T(8,128)(2,1)} %v.3, f32[3,128]{1,0:T(4,128)} %bitcast.74), custom_call_target="tpu_custom_call" | custom-call | flops 4194304 | bytes 1048576 | tf_op jit(solution)/shard_map/pallas_call | solution.py:316
  2.7 23.7 %all-to-all-start = ((bf16[8,80,128]{2,1,0:T(8,128)(2,1)}), bf16[8,80,128]{2,1,0:T(8,128)(2,1)S(1)}, u32[]{:S(2)}, u32[]{:S(2)}) async-start(bf16[8,80,128]{2,1,0:T(8,128)(2,1)} %shard_map.172), calls=%async_computation | async-start | bytes 327680 | tf_op jit(solution)/shard_map/all_to_all | solution.py:319
  27.0 5.5 %all-to-all-done.got = bf16[8,80,128]{2,1,0:T(8,128)(2,1)S(1)} async-done(((bf16[8,80,128]{2,1,0:T(8,128)(2,1)}), bf16[8,80,128]{2,1,0:T(8,128)(2,1)S(1)}, u32[]{:S(2)}, u32[]{:S(2)}) %all-to-all-start) | async-done | bytes 163872 | tf_op jit(solution)/shard_map/all_to_all | solution.py:319
  33.2 1.9 shard_map.173
  35.1 9.4 %collective-permute-start.1 = (bf16[80,128]{1,0:T(8,128)(2,1)}, bf16[80,128]{1,0:T(8,128)(2,1)S(1)}, u32[]{:S(2)}, u32[]{:S(2)}) collective-permute-start(bf16[80,128]{1,0:T(8,128)(2,1)} %get-tuple-element.20), channel_id=1, source_target_pairs={{0,64},{32,96},{64,0},{96,32},{1,65},{33,97},{65,1},{97,33},{2,66}... | collective-permute-start | bytes 61448 | tf_op jit(solution)/shard_map/ppermute | solution.py:340
  44.5 2.3 collective-permute-done.1.r2
  46.7 4.6 %collective-permute-done.2.r3 = bf16[80,128]{1,0:T(8,128)(2,1)S(1)} collective-permute-done((bf16[80,128]{1,0:T(8,128)(2,1)}, bf16[80,128]{1,0:T(8,128)(2,1)S(1)}, u32[]{:S(2)}, u32[]{:S(2)}) %collective-permute-start.2) | collective-permute-done | bytes 20512 | tf_op jit(solution)/shard_map/ppermute | solution.py:340
  52.0 1.9 shard_map.174
  53.8 6.4 %all-to-all-start.1 = ((bf16[8,64,128]{2,1,0:T(8,128)(2,1)}), bf16[8,64,128]{2,1,0:T(8,128)(2,1)S(1)}, u32[]{:S(2)}, u32[]{:S(2)}) async-start(bf16[8,64,128]{2,1,0:T(8,128)(2,1)} %shard_map.174), calls=%async_computation.1 | async-start | bytes 262144 | tf_op jit(solution)/shard_map/all_to_all | solution.py:349
  61.5 3.5 %shard_map.175 = (f32[128,384]{1,0:T(8,128)}, bf16[128,256]{1,0:T(8,128)(2,1)}, bf16[128,256]{1,0:T(8,128)(2,1)}) custom-call(bf16[128,128]{1,0:T(8,128)(2,1)} %wp.1, bf16[128,128]{1,0:T(8,128)(2,1)} %np_.1, bf16[128,128]{1,0:T(8,128)(2,1)} %wd.3, bf16[128,128]{1,0:T(8,128)(2,1)} %nd.3, f32[2,128]{1,0:T(2,128)} %wleak.3, f32[2,128]{1,0:T(2,128)} %nleak.3, ...), custom_call_target="tpu_custom_call" | custom-call | flops 67108864 | bytes 1048576 | tf_op jit(solution)/shard_map/pallas_call | solution.py:320
  66.8 3.2 %shard_map.176 = bf16[128,2048]{1,0:T(8,128)(2,1)} custom-call(bf16[8,64,128]{2,1,0:T(8,128)(2,1)} %copy-done.2, f32[128,384]{1,0:T(8,128)} %get-tuple-element.23.o_ref, bf16[128,256]{1,0:T(8,128)(2,1)} %get-tuple-element.24.qf, bf16[128,256]{1,0:T(8,128)(2,1)} %get-tuple-element.25.qb, bf16[128,384]{1,0:T(8,128)(2,1)} %gate.1, f32[1,384]{1,0:T(1,128)} %reshape.21.gain, ...), custom_call_target="tpu_custom_call" | custom-call | flops 268435456 | bytes 1048576 | tf_op jit(solution)/shard_map/pallas_call | solution.py:350
  70.1 12.8 %all_to_all.25.parts = bf16[4,32,2048]{2,1,0:T(8,128)(2,1)} all-to-all(bf16[4,32,2048]{2,1,0:T(8,128)(2,1)} %bitcast.70), channel_id=1, replica_groups=mesh['grp'=2,'zh'=4,'zl'=4,'c'=2,'tp'=4] {'tp'}, dimensions={0} | all-to-all | bytes 1048576 | tf_op jit(solution)/shard_map/all_to_all | solution.py:361
  82.9 2.4 %shard_map.177 = (bf16[32,2048]{1,0:T(8,128)(2,1)}, bf16[128,2048]{1,0:T(8,128)(2,1)}) custom-call(bf16[4,32,2048]{2,1,0:T(8,128)(2,1)} %all_to_all.25.parts, bf16[32,2048]{1,0:T(8,128)(2,1)} %skip.1, f32[1,2048]{1,0:T(1,128)} %bitcast.71, s32[2,32]{1,0:T(2,128)} %bitcast.72), custom_call_target="tpu_custom_call" | custom-call | flops 16777216 | bytes 1048576 | tf_op jit(solution)/shard_map/pallas_call | solution.py:365
  86.5 41.3 %all_to_all.26 = bf16[32,4,2048]{2,1,0:T(4,128)(2,1)S(1)} all-to-all(bf16[32,4,2048]{2,1,0:T(4,128)(2,1)S(1)} %reshape.24), channel_id=1, replica_groups=mesh['grp'=2,'zh'=4,'zl'=4,'c'=2,'tp'=4] {'zh','zl','c'}, dimensions={0} | all-to-all | bytes 1048576 | tf_op jit(solution)/shard_map/all_to_all | solution.py:370
  128.4 2.3 collective-permute-start.4
  130.7 2.8 %fusion.22 = f32[128,896]{1,0:T(8,128)S(1)} fusion(bf16[128,2048]{1,0:T(8,128)(2,1)S(1)} %reshape.25, bf16[1,2048,896]{2,1,0:T(8,128)(2,1)} %param.33), kind=kOutput, calls=%fused_computation.22 | convolution fusion | flops 469762048 | bytes 4653056 | tf_op jit(solution)/shard_map/dot_general | solution.py:250
  133.5 4.5 %fusion.24 = bf16[128,2048]{1,0:T(8,128)(2,1)S(1)} fusion(bf16[1,896,2048]{2,1,0:T(8,128)(2,1)} %param.35, bf16[128,2048]{1,0:T(8,128)(2,1)S(1)} %reshape.25, bf16[1,2048,896]{2,1,0:T(8,128)(2,1)} %param.34, f32[128,896]{1,0:T(8,128)S(1)} %fusion.22), kind=kOutput, calls=%fused_computation.24 | convolution fusion | flops 940474368 | bytes 8847360 | tf_op jit(solution)/shard_map/dot_general | solution.py:253
  137.9 4.3 %collective-permute-done.3 = bf16[128,2048]{1,0:T(8,128)(2,1)S(1)} collective-permute-done((bf16[128,2048]{1,0:T(8,128)(2,1)S(1)}, bf16[128,2048]{1,0:T(8,128)(2,1)S(1)}, u32[]{:S(2)}, u32[]{:S(2)}) %collective-permute-start.3) | collective-permute-done | bytes 524320 | tf_op jit(solution)/shard_map/ppermute | solution.py:375
  142.2 2.8 %fusion.12 = f32[128,896]{1,0:T(8,128)S(1)} fusion(bf16[128,2048]{1,0:T(8,128)(2,1)S(1)} %collective-permute-done.3, bf16[1,2048,896]{2,1,0:T(8,128)(2,1)} %param.34), kind=kOutput, calls=%fused_computation.12 | convolution fusion | flops 469762048 | bytes 4653056 | tf_op jit(solution)/shard_map/dot_general | solution.py:251
  146.4 4.5 %fusion.30 = bf16[128,2048]{1,0:T(8,128)(2,1)S(1)} fusion(bf16[1,896,2048]{2,1,0:T(8,128)(2,1)} %param.35, f32[128,896]{1,0:T(8,128)S(1)} %fusion.10, bf16[128,2048]{1,0:T(8,128)(2,1)S(1)} %collective-permute-done.4, bf16[1,2048,896]{2,1,0:T(8,128)(2,1)} %param.33), kind=kOutput, calls=%fused_computation.26 | convolution fusion | flops 940474368 | bytes 8847360 | tf_op jit(solution)/shard_map/dot_general | solution.py:253
  151.1 2.7 %collective-permute-start.6 = (bf16[64,2048]{1,0:T(8,128)(2,1)S(1)}, bf16[64,2048]{1,0:T(8,128)(2,1)}, u32[]{:S(2)}, u32[]{:S(2)}) collective-permute-start(bf16[64,2048]{1,0:T(8,128)(2,1)S(1)} %slice.32), channel_id=1, source_target_pairs={{0,3},{1,0},{2,1},{3,2},{4,7},{5,4},{6,5},{7,6},{8,11},{9,8},{10,9... | collective-permute-start | bytes 786440 | tf_op jit(solution)/shard_map/ppermute | solution.py:376
  153.8 4.5 %fusion.27 = bf16[128,2048]{1,0:T(8,128)(2,1)S(1)} fusion(bf16[1,896,2048]{2,1,0:T(8,128)(2,1)} %param.35, f32[128,896]{1,0:T(8,128)S(1)} %fusion.12, bf16[128,2048]{1,0:T(8,128)(2,1)S(1)} %collective-permute-done.3, bf16[1,2048,896]{2,1,0:T(8,128)(2,1)} %param.33), kind=kOutput, calls=%fused_computation.25 | convolution fusion | flops 940474368 | bytes 8847360 | tf_op jit(solution)/shard_map/dot_general | solution.py:253
  160.0 2.8 %fusion.16 = f32[128,896]{1,0:T(8,128)S(1)} fusion(bf16[128,2048]{1,0:T(8,128)(2,1)S(1)} %constant_dynamic-update-slice_fusion, bf16[1,2048,896]{2,1,0:T(8,128)(2,1)} %param.33), kind=kOutput, calls=%fused_computation.16 | convolution fusion | flops 469762048 | bytes 4653056 | tf_op jit(solution)/shard_map/dot_general | solution.py:250
  162.8 4.5 %fusion.33 = bf16[128,2048]{1,0:T(8,128)(2,1)S(1)} fusion(bf16[1,896,2048]{2,1,0:T(8,128)(2,1)} %param.35, bf16[128,2048]{1,0:T(8,128)(2,1)S(1)} %constant_dynamic-update-slice_fusion, bf16[1,2048,896]{2,1,0:T(8,128)(2,1)} %param.34, f32[128,896]{1,0:T(8,128)S(1)} %fusion.16), kind=kOutput, calls=%fused_computation.27 | convolution fusion | flops 940474368 | bytes 8847360 | tf_op jit(solution)/shard_map/dot_general | solution.py:253
  167.3 2.4 %collective-permute-start.11 = (bf16[64,2048]{1,0:T(8,128)(2,1)S(1)}, bf16[64,2048]{1,0:T(8,128)(2,1)S(1)}, u32[]{:S(2)}, u32[]{:S(2)}) collective-permute-start(bf16[64,2048]{1,0:T(8,128)(2,1)S(1)} %get-tuple-element.38), channel_id=1, source_target_pairs={{0,3},{1,0},{2,1},{3,2},{4,7},{5,4},{6,5},{7,6},{8,11},{9,8},{10,9... | collective-permute-start | bytes 786440 | tf_op jit(solution)/shard_map/ppermute | solution.py:376
  169.9 3.0 %collective-permute-start.9 = (bf16[64,2048]{1,0:T(8,128)(2,1)S(1)}, bf16[64,2048]{1,0:T(8,128)(2,1)S(1)}, u32[]{:S(2)}, u32[]{:S(2)}) collective-permute-start(bf16[64,2048]{1,0:T(8,128)(2,1)S(1)} %slice.35), channel_id=1, source_target_pairs={{0,3},{1,0},{2,1},{3,2},{4,7},{5,4},{6,5},{7,6},{8,11},{9,8},{10,9... | collective-permute-start | bytes 786440 | tf_op jit(solution)/shard_map/ppermute | solution.py:376
  173.1 3.2 %collective-permute-start.12 = (bf16[64,2048]{1,0:T(8,128)(2,1)S(1)}, bf16[64,2048]{1,0:T(8,128)(2,1)S(1)}, u32[]{:S(2)}, u32[]{:S(2)}) collective-permute-start(bf16[64,2048]{1,0:T(8,128)(2,1)S(1)} %add_convert_fusion.1), channel_id=1, source_target_pairs={{0,3},{1,0},{2,1},{3,2},{4,7},{5,4},{6,5},{7,6},{8,11},{9,8},{10,9... | collective-permute-start | bytes 786440 | tf_op jit(solution)/shard_map/ppermute | solution.py:376
  176.5 5.1 %collective-permute-done.10 = bf16[64,2048]{1,0:T(8,128)(2,1)S(1)} collective-permute-done((bf16[64,2048]{1,0:T(8,128)(2,1)S(1)}, bf16[64,2048]{1,0:T(8,128)(2,1)S(1)}, u32[]{:S(2)}, u32[]{:S(2)}) %collective-permute-start.10) | collective-permute-done | bytes 262176 | tf_op jit(solution)/shard_map/ppermute | solution.py:375
  181.6 3.0 %collective-permute-done.12 = bf16[64,2048]{1,0:T(8,128)(2,1)S(1)} collective-permute-done((bf16[64,2048]{1,0:T(8,128)(2,1)S(1)}, bf16[64,2048]{1,0:T(8,128)(2,1)S(1)}, u32[]{:S(2)}, u32[]{:S(2)}) %collective-permute-start.12) | collective-permute-done | bytes 262176 | tf_op jit(solution)/shard_map/ppermute | solution.py:376
  184.6 2.6 %collective-permute-done.8 = bf16[64,2048]{1,0:T(8,128)(2,1)S(1)} collective-permute-done((bf16[64,2048]{1,0:T(8,128)(2,1)S(1)}, bf16[64,2048]{1,0:T(8,128)(2,1)S(1)}, u32[]{:S(2)}, u32[]{:S(2)}) %collective-permute-start.8) | collective-permute-done | bytes 262176 | tf_op jit(solution)/shard_map/ppermute | solution.py:375
  187.7 41.3 %all_to_all.27 = bf16[32,4,2048]{2,1,0:T(4,128)(2,1)S(1)} all-to-all(bf16[32,4,2048]{2,1,0:T(4,128)(2,1)S(1)} %reshape.26), channel_id=1, replica_groups=mesh['grp'=2,'zh'=4,'zl'=4,'c'=2,'tp'=4] {'zh','zl','c'}, dimensions={0} | all-to-all | bytes 1048576 | tf_op jit(solution)/shard_map/all_to_all | solution.py:408
  230.0 2.2 shard_map.178
  (45 shorter events, 12.2 us)
Async XLA Ops:
  2.7 29.9 %all-to-all-start = ((bf16[8,80,128]{2,1,0:T(8,128)(2,1)}), bf16[8,80,128]{2,1,0:T(8,128)(2,1)S(1)}, u32[]{:S(2)}, u32[]{:S(2)}) async-start(bf16[8,80,128]{2,1,0:T(8,128)(2,1)} %shard_map.172), calls=%async_computation | async-start | bytes 327680 | tf_op jit(solution)/shard_map/all_to_all | solution.py:319
  32.5 0.7 copy-start.1
  35.1 9.4 %collective-permute-start = (bf16[80,128]{1,0:T(8,128)(2,1)}, bf16[80,128]{1,0:T(8,128)(2,1)S(1)}, u32[]{:S(2)}, u32[]{:S(2)}) collective-permute-start(bf16[80,128]{1,0:T(8,128)(2,1)} %get-tuple-element.20), channel_id=1, source_target_pairs={{0,32},{32,64},{64,96},{96,0},{1,33},{33,65},{65,97},{97,1},{2,34}... | collective-permute-start | bytes 61448 | tf_op jit(solution)/shard_map/ppermute | solution.py:340
  35.1 11.6 %collective-permute-start.1 = (bf16[80,128]{1,0:T(8,128)(2,1)}, bf16[80,128]{1,0:T(8,128)(2,1)S(1)}, u32[]{:S(2)}, u32[]{:S(2)}) collective-permute-start(bf16[80,128]{1,0:T(8,128)(2,1)} %get-tuple-element.20), channel_id=1, source_target_pairs={{0,64},{32,96},{64,0},{96,32},{1,65},{33,97},{65,1},{97,33},{2,66}... | collective-permute-start | bytes 61448 | tf_op jit(solution)/shard_map/ppermute | solution.py:340
  44.4 6.9 %collective-permute-start.2 = (bf16[80,128]{1,0:T(8,128)(2,1)}, bf16[80,128]{1,0:T(8,128)(2,1)S(1)}, u32[]{:S(2)}, u32[]{:S(2)}) collective-permute-start(bf16[80,128]{1,0:T(8,128)(2,1)} %get-tuple-element.20), channel_id=1, source_target_pairs={{0,96},{32,0},{64,32},{96,64},{1,97},{33,1},{65,33},{97,65},{2,98}... | collective-permute-start | bytes 61448 | tf_op jit(solution)/shard_map/ppermute | solution.py:340
  44.5 6.9 %copy-start.3 = (bf16[80,128]{1,0:T(8,128)(2,1)}, bf16[80,128]{1,0:T(8,128)(2,1)S(1)}, u32[]{:S(2)}) copy-start(bf16[80,128]{1,0:T(8,128)(2,1)S(1)} %collective-permute-done.r1) | copy-start | bytes 61444
  46.7 4.6 %copy-start.4 = (bf16[80,128]{1,0:T(8,128)(2,1)}, bf16[80,128]{1,0:T(8,128)(2,1)S(1)}, u32[]{:S(2)}) copy-start(bf16[80,128]{1,0:T(8,128)(2,1)S(1)} %collective-permute-done.1.r2) | copy-start | bytes 61444
  51.4 0.6 copy-start.5
  53.8 12.3 %all-to-all-start.1 = ((bf16[8,64,128]{2,1,0:T(8,128)(2,1)}), bf16[8,64,128]{2,1,0:T(8,128)(2,1)S(1)}, u32[]{:S(2)}, u32[]{:S(2)}) async-start(bf16[8,64,128]{2,1,0:T(8,128)(2,1)} %shard_map.174), calls=%async_computation.1 | async-start | bytes 262144 | tf_op jit(solution)/shard_map/all_to_all | solution.py:349
  66.2 0.7 copy-start.2
  127.9 14.3 %collective-permute-start.3 = (bf16[128,2048]{1,0:T(8,128)(2,1)S(1)}, bf16[128,2048]{1,0:T(8,128)(2,1)S(1)}, u32[]{:S(2)}, u32[]{:S(2)}) collective-permute-start(bf16[128,2048]{1,0:T(8,128)(2,1)S(1)} %reshape.25), channel_id=1, source_target_pairs={{0,1},{1,2},{2,3},{3,0},{4,5},{5,6},{6,7},{7,4},{8,9},{9,10},{10,1... | collective-permute-start | bytes 1572872 | tf_op jit(solution)/shard_map/ppermute | solution.py:375
  128.4 13.8 %collective-permute-start.4 = (bf16[128,2048]{1,0:T(8,128)(2,1)S(1)}, bf16[128,2048]{1,0:T(8,128)(2,1)S(1)}, u32[]{:S(2)}, u32[]{:S(2)}) collective-permute-start(bf16[128,2048]{1,0:T(8,128)(2,1)S(1)} %reshape.25), channel_id=1, source_target_pairs={{0,3},{1,0},{2,1},{3,2},{4,7},{5,4},{6,5},{7,6},{8,11},{9,8},{10,9... | collective-permute-start | bytes 1572872 | tf_op jit(solution)/shard_map/ppermute | solution.py:376
  137.9 7.7 %copy-start = (bf16[1,2048,896]{2,1,0:T(8,128)(2,1)S(1)}, bf16[1,2048,896]{2,1,0:T(8,128)(2,1)}, u32[]{:S(2)}) copy-start(bf16[1,2048,896]{2,1,0:T(8,128)(2,1)} %param.34) | copy-start | bytes 11010052
  151.0 8.0 %collective-permute-start.5 = (bf16[64,2048]{1,0:T(8,128)(2,1)}, bf16[64,2048]{1,0:T(8,128)(2,1)S(1)}, u32[]{:S(2)}, u32[]{:S(2)}) collective-permute-start(bf16[64,2048]{1,0:T(8,128)(2,1)} %slice.31), channel_id=1, source_target_pairs={{0,1},{1,2},{2,3},{3,0},{4,5},{5,6},{6,7},{7,4},{8,9},{9,10},{10,1... | collective-permute-start | bytes 786440 | tf_op jit(solution)/shard_map/ppermute | solution.py:375
  151.1 7.9 %collective-permute-start.6 = (bf16[64,2048]{1,0:T(8,128)(2,1)S(1)}, bf16[64,2048]{1,0:T(8,128)(2,1)}, u32[]{:S(2)}, u32[]{:S(2)}) collective-permute-start(bf16[64,2048]{1,0:T(8,128)(2,1)S(1)} %slice.32), channel_id=1, source_target_pairs={{0,3},{1,0},{2,1},{3,2},{4,7},{5,4},{6,5},{7,6},{8,11},{9,8},{10,9... | collective-permute-start | bytes 786440 | tf_op jit(solution)/shard_map/ppermute | solution.py:376
  167.3 5.8 %collective-permute-start.11 = (bf16[64,2048]{1,0:T(8,128)(2,1)S(1)}, bf16[64,2048]{1,0:T(8,128)(2,1)S(1)}, u32[]{:S(2)}, u32[]{:S(2)}) collective-permute-start(bf16[64,2048]{1,0:T(8,128)(2,1)S(1)} %get-tuple-element.38), channel_id=1, source_target_pairs={{0,3},{1,0},{2,1},{3,2},{4,7},{5,4},{6,5},{7,6},{8,11},{9,8},{10,9... | collective-permute-start | bytes 786440 | tf_op jit(solution)/shard_map/ppermute | solution.py:376
  169.7 6.6 %collective-permute-start.7 = (bf16[64,2048]{1,0:T(8,128)(2,1)S(1)}, bf16[64,2048]{1,0:T(8,128)(2,1)S(1)}, u32[]{:S(2)}, u32[]{:S(2)}) collective-permute-start(bf16[64,2048]{1,0:T(8,128)(2,1)S(1)} %get-tuple-element.37), channel_id=1, source_target_pairs={{0,1},{1,2},{2,3},{3,0},{4,5},{5,6},{6,7},{7,4},{8,9},{9,10},{10,1... | collective-permute-start | bytes 786440 | tf_op jit(solution)/shard_map/ppermute | solution.py:375
  169.7 11.9 %collective-permute-start.10 = (bf16[64,2048]{1,0:T(8,128)(2,1)S(1)}, bf16[64,2048]{1,0:T(8,128)(2,1)S(1)}, u32[]{:S(2)}, u32[]{:S(2)}) collective-permute-start(bf16[64,2048]{1,0:T(8,128)(2,1)S(1)} %slice.37), channel_id=1, source_target_pairs={{0,1},{1,2},{2,3},{3,0},{4,5},{5,6},{6,7},{7,4},{8,9},{9,10},{10,1... | collective-permute-start | bytes 786440 | tf_op jit(solution)/shard_map/ppermute | solution.py:375
  169.9 11.7 %collective-permute-start.9 = (bf16[64,2048]{1,0:T(8,128)(2,1)S(1)}, bf16[64,2048]{1,0:T(8,128)(2,1)S(1)}, u32[]{:S(2)}, u32[]{:S(2)}) collective-permute-start(bf16[64,2048]{1,0:T(8,128)(2,1)S(1)} %slice.35), channel_id=1, source_target_pairs={{0,3},{1,0},{2,1},{3,2},{4,7},{5,4},{6,5},{7,6},{8,11},{9,8},{10,9... | collective-permute-start | bytes 786440 | tf_op jit(solution)/shard_map/ppermute | solution.py:376
  173.1 11.5 %collective-permute-start.12 = (bf16[64,2048]{1,0:T(8,128)(2,1)S(1)}, bf16[64,2048]{1,0:T(8,128)(2,1)S(1)}, u32[]{:S(2)}, u32[]{:S(2)}) collective-permute-start(bf16[64,2048]{1,0:T(8,128)(2,1)S(1)} %add_convert_fusion.1), channel_id=1, source_target_pairs={{0,3},{1,0},{2,1},{3,2},{4,7},{5,4},{6,5},{7,6},{8,11},{9,8},{10,9... | collective-permute-start | bytes 786440 | tf_op jit(solution)/shard_map/ppermute | solution.py:376
  176.4 10.9 %collective-permute-start.8 = (bf16[64,2048]{1,0:T(8,128)(2,1)S(1)}, bf16[64,2048]{1,0:T(8,128)(2,1)S(1)}, u32[]{:S(2)}, u32[]{:S(2)}) collective-permute-start(bf16[64,2048]{1,0:T(8,128)(2,1)S(1)} %add_convert_fusion.3), channel_id=1, source_target_pairs={{0,1},{1,2},{2,3},{3,0},{4,5},{5,6},{6,7},{7,4},{8,9},{9,10},{10,1... | collective-permute-start | bytes 786440 | tf_op jit(solution)/shard_map/ppermute | solution.py:375
where the time goes:
time: 233 us; the launch traced here: 232 us
  blocking collectives  95.4 us (41%)
  starting transfers between devices  53.9 us (23%)
  waiting for transfers between devices  29.5 us (13%)
  matrix products  27 us (12%)
  Pallas kernels  17.7 us (8%)
  local copies, waits for them, and re-layouts  7.44 us (3%)
    all_to_all x1, blocking collectives, local(): lax.all_to_all(summed.reshape(experts, CAP, model), SP, 0, 0, tiled=True)  41.3 us
    all_to_all x1, blocking collectives, local(): lax.all_to_all(outgoing.reshape(experts, CAP, model), SP, 0, 0, tiled=True)  41.3 us
    all_to_all x1, starting transfers between devices, local(): by_slice = lax.all_to_all(summary, ZG, 0, 0, tiled=True)  23.7 us
    dot_general x4, matrix products, expert_part(): return jnp.dot(act, wd, preferred_element_type=F32).astype(BF16)  18 us
    ppermute x5, starting transfers between devices, local(): down = lambda x: lax.ppermute(x, 'tp', down_ring)  13.6 us
    all_to_all x1, blocking collectives, local(): lax.all_to_all(mixed.reshape(shards, rows, model), 'tp', 0, 0, tiled=True)  12.8 us
    ppermute x5, waiting for transfers between devices, local(): up = lambda x: lax.ppermute(x, 'tp', up_ring)  12.7 us
    ppermute x3, starting transfers between devices, local(): lax.ppermute(total, 'zh', [(i, (i + k) % groups) for i in range(groups)])  9.36 us
  transfers between devices with their start and end apart: 15, of which 10 were waited for; matrix products, arithmetic and copies ran while one was open for 6% of the time, Pallas kernels for 1%

commit v1 on v0

--- a/solution.py
+++ b/solution.py
@@ -243,27 +243,86 @@
     normed = (normed * gain[...]).astype(BF16)
     first, second = slot_matrix(routes[...])
     chosen = jnp.logical_or(first, second).astype(F32).astype(BF16)
-    out[...] = dot(chosen, normed).astype(BF16)
-
-
-def expert_part(rows, wg, wu, wd):
-    gate = jnp.dot(rows, wg, preferred_element_type=F32)
-    up = jnp.dot(rows, wu, preferred_element_type=F32)
-    act = (jax.nn.silu(gate) * up).astype(BF16)
-    return jnp.dot(act, wd, preferred_element_type=F32).astype(BF16)
+    out[...] = block_of(dot(chosen, normed).astype(BF16))
+
+
+def rows_of(block):
+    return block.astype(F32).reshape(-1, block.shape[-1]).astype(BF16)
+
+
+def block_of(rows):
+    return rows.astype(F32).reshape(-1, CAP, rows.shape[-1]).astype(BF16)
+
+
+def split_kernel(got, low, high):
+    half = got.shape[0] // 2
+    low[...] = rows_of(got[:half])
+    high[...] = rows_of(got[half:])
+
+
+def own_kernel(low, high, a, b, c, part_low, part_high, wg, wu, wd, sems):
+    moves = [
+        pltpu.make_async_copy(src, dst, sems.at[n])
+        for n, (src, dst) in enumerate(((a, wg), (b, wu), (c, wd)))
+    ]
+    for move in moves:
+        move.start()
+    rows = jnp.concatenate([low[...], high[...]], axis=0)
+    moves[0].wait()
+    gate = jax.nn.silu(dot(rows, wg[...]))
+    moves[1].wait()
+    act = (gate * dot(rows, wu[...])).astype(BF16)
+    moves[2].wait()
+    part = dot(act, wd[...]).astype(BF16)
+    half = low.shape[0]
+    part_low[...] = part[:half]
+    part_high[...] = part[half:]
+
+
+def piece_kernel(x, wg, wu, wd, out):
+    rows = x[...]
+    act = (jax.nn.silu(dot(rows, wg[...])) * dot(rows, wu[...])).astype(BF16)
+    out[...] = dot(act, wd[...]).astype(BF16)
+
+
+def add_kernel(a, b, out):
+    out[...] = (a[...].astype(F32) + b[...].astype(F32)).astype(BF16)
+
+
+def sum_kernel(low_a, low_b, low_c, high_a, high_b, high_c, out):
+    half = out.shape[0] // 2
+    f = lambda ref: ref[...].astype(F32)
+    out[:half] = block_of((f(low_a) + f(low_b) + f(low_c)).astype(BF16))
+    out[half:] = block_of((f(high_a) + f(high_b) + f(high_c)).astype(BF16))
 
 
 def combine_kernel(hidden, back, routes, share, out):
     first, second = slot_matrix(routes[...])
     weight = jnp.where(first, share[0:1], 0.0) + jnp.where(second, share[1:2], 0.0)
     hi, lo = split_parts(weight)
-    rows = back[...]
+    rows = rows_of(back[...])
     mixture = dot(hi, rows, (0, 0)) + dot(lo, rows, (0, 0))
     out[...] = (hidden[...].astype(F32) + mixture).astype(BF16)
 
 
 def sds(shape, dtype):
     return jax.ShapeDtypeStruct(shape, dtype)
+
+
+def near(shape, dtype):
+    return pltpu.VMEM(shape, dtype)
+
+
+def nearby(*arrays):
+    return tuple(pltpu.with_memory_space_constraint(a, pltpu.VMEM) for a in arrays)
+
+
+def params(mib=24):
+    return pltpu.CompilerParams(vmem_limit_bytes=mib << 20)
+
+
+def distant(*arrays):
+    return tuple(pltpu.with_memory_space_constraint(a, pltpu.HBM) for a in arrays)
 
 
 VMEM = pl.BlockSpec(memory_space=pltpu.VMEM)
@@ -314,28 +373,33 @@
     )
 
     summary = pl.pallas_call(
-        summary_kernel, out_shape=sds((members, PAY, width), BF16), cost_estimate=cost(4 << 20)
-    )(*decay_args)
+        summary_kernel,
+        out_shape=near((members, PAY, width), BF16),
+        compiler_params=params(),
+        cost_estimate=cost(4 << 20),
+    )(*distant(*decay_args))
     by_slice = lax.all_to_all(summary, ZG, 0, 0, tiled=True)
     inside, q_fwd, q_bwd = pl.pallas_call(
         local_kernel,
         out_shape=[
-            sds((tokens, joint), F32),
-            sds((tokens, 2 * width), BF16),
-            sds((tokens, 2 * width), BF16),
+            near((tokens, joint), F32),
+            near((tokens, 2 * width), BF16),
+            near((tokens, 2 * width), BF16),
         ],
+        compiler_params=params(),
         cost_estimate=cost(64 << 20),
-    )(wide_probe_logits, narrow_probe_logits, *decay_args)
+    )(*distant(wide_probe_logits, narrow_probe_logits, *decay_args))
     before, decayed, total = pl.pallas_call(
         group_kernel,
         in_specs=[SMEM, VMEM],
         out_shape=[
-            sds((members, 2 * SLICE, width), F32),
-            sds((members, 2 * SLICE, width), F32),
-            sds((PAY, width), BF16),
+            near((members, 2 * SLICE, width), F32),
+            near((members, 2 * SLICE, width), F32),
+            near((PAY, width), BF16),
         ],
+        compiler_params=params(),
         cost_estimate=cost(4 << 20),
-    )(place, by_slice)
+    )(place, *nearby(by_slice))
     came = [
         lax.ppermute(total, "zh", [(i, (i + k) % groups) for i in range(groups)])
         for k in (1, 2, 3)
@@ -343,20 +407,21 @@
     carried = pl.pallas_call(
         carry_kernel,
         in_specs=[SMEM] + [VMEM] * 5,
-        out_shape=sds((members, 2 * SLICE, width), BF16),
+        out_shape=near((members, 2 * SLICE, width), BF16),
+        compiler_params=params(),
         cost_estimate=cost(4 << 20),
-    )(place, *came, before, decayed)
+    )(place, *nearby(*came, before, decayed))
     entering = lax.all_to_all(carried, ZG, 0, 0, tiled=True)
     mixed = pl.pallas_call(
-        mix_kernel, out_shape=sds((tokens, model), BF16), cost_estimate=cost(256 << 20)
+        mix_kernel,
+        out_shape=near((tokens, model), BF16),
+        compiler_params=params(),
+        cost_estimate=cost(256 << 20),
     )(
-        entering,
-        inside,
-        q_fwd,
-        q_bwd,
-        result_switch_logits,
-        channel_scale_vector.reshape(1, joint),
-        result_mapping_matrix,
+        *nearby(entering, inside, q_fwd, q_bwd),
+        *distant(
+            result_switch_logits, channel_scale_vector.reshape(1, joint), result_mapping_matrix
+        ),
     )
     parts = lax.all_to_all(mixed.reshape(shards, rows, model), "tp", 0, 0, tiled=True)
     routes = assignments.T
@@ -364,51 +429,75 @@
     slots = experts * CAP
     hidden, outgoing = pl.pallas_call(
         dispatch_kernel,
-        out_shape=[sds((rows, model), BF16), sds((slots, model), BF16)],
+        out_shape=[sds((rows, model), BF16), near((experts, CAP, model), BF16)],
+        compiler_params=params(),
         cost_estimate=cost(16 << 20),
-    )(parts, skip_stream, specialist_scale_vector.reshape(1, model), routes)
-    own = lax.all_to_all(outgoing.reshape(experts, CAP, model), SP, 0, 0, tiled=True)
-    own = own.reshape(slots, model)
+    )(*nearby(parts), *distant(skip_stream, specialist_scale_vector.reshape(1, model), routes))
+    own = lax.all_to_all(outgoing, SP, 0, 0, tiled=True)
 
     up_ring = [(i, (i + 1) % shards) for i in range(shards)]
     down_ring = [(i, (i - 1) % shards) for i in range(shards)]
-    up = lambda x: lax.ppermute(x, "tp", up_ring)
-    down = lambda x: lax.ppermute(x, "tp", down_ring)
+
+    def up(x):
+        return lax.ppermute(x, "tp", up_ring)
+
+    def down(x):
+        return lax.ppermute(x, "tp", down_ring)
+
     half = slots // 2
+    piece = near((half, model), BF16)
+
+    def call(kernel, flops, *arrays, **rest):
+        rest = {"out_shape": piece, **rest}
+        return pl.pallas_call(
+            kernel, compiler_params=params(), cost_estimate=cost(flops), **rest
+        )(*arrays)
+
     weights = (
         specialist_switch_matrix[0],
         specialist_raising_matrix[0],
         specialist_lowering_matrix[0],
     )
-    hold = lax.optimization_barrier
-    from_left = up(own)
-    from_right = down(own)
-    own_part = expert_part(own, *weights)
-    from_left, from_right, own_part = hold((from_left, from_right, own_part))
-    far_low = up(from_left[:half])
-    far_high = down(from_right[half:])
-    left_part = expert_part(from_left, *weights)
-    right_part = expert_part(from_right, *weights)
-    far_low, far_high, left_part, right_part = hold((far_low, far_high, left_part, right_part))
-    left_got_high = up(right_part[half:])
-    right_got_low = down(left_part[:half])
-    opposite = expert_part(jnp.concatenate([far_low, far_high], axis=0), *weights)
-    add_low, add_high = up(opposite[:half]), down(opposite[half:])
-    joined = lambda a, b: (a.astype(F32) + b.astype(F32)).astype(BF16)
-    left_got_low = up(joined(right_part[:half], add_low))
-    right_got_high = down(joined(left_part[half:], add_high))
-    f = lambda x: x.astype(F32)
-    summed = jnp.concatenate(
-        [
-            (f(own_part[:half]) + f(left_got_low) + f(right_got_low)).astype(BF16),
-            (f(own_part[half:]) + f(left_got_high) + f(right_got_high)).astype(BF16),
-        ],
-        axis=0,
-    )
-    back = lax.all_to_all(summed.reshape(experts, CAP, model), SP, 0, 0, tiled=True)
+    own_low, own_high = call(split_kernel, 1 << 20, *nearby(own), out_shape=[piece] * 2)
+    left_low, right_high = up(own_low), down(own_high)
+    left_high, right_low = up(own_high), down(own_low)
+    sum_low, sum_high, *weights = call(
+        own_kernel,
+        2 << 30,
+        *nearby(own_low, own_high),
+        *distant(*weights),
+        in_specs=[VMEM] * 2 + [pl.BlockSpec(memory_space=pl.ANY)] * 3,
+        out_shape=[piece] * 2 + [near(w.shape, w.dtype) for w in weights],
+        scratch_shapes=[pltpu.SemaphoreType.DMA((3,))],
+    )
+
+    def part(x):
+        return call(piece_kernel, 1 << 30, *nearby(x, *weights))
+
+    def add(a, b):
+        return call(add_kernel, 1 << 20, *nearby(a, b))
+
+    far_low, far_high = up(left_low), down(right_high)
+    for_left_low, for_right_high = part(left_low), part(right_high)
+    got_high, got_low = up(for_right_high), down(for_left_low)
+    for_left_high, for_right_low = part(left_high), part(right_low)
+    add_low = up(part(far_low))
+    add_high = down(part(far_high))
+    last_low = up(add(for_right_low, add_low))
+    last_high = down(add(for_left_high, add_high))
+    summed = call(
+        sum_kernel,
+        1 << 20,
+        *nearby(sum_low, last_low, got_low, sum_high, last_high, got_high),
+        out_shape=near((experts, CAP, model), BF16),
+    )
+    back = lax.all_to_all(summed, SP, 0, 0, tiled=True)
     return pl.pallas_call(
-        combine_kernel, out_shape=sds((rows, model), BF16), cost_estimate=cost(16 << 20)
-    )(hidden, back.reshape(slots, model), routes, share)
+        combine_kernel,
+        out_shape=sds((rows, model), BF16),
+        compiler_params=params(),
+        cost_estimate=cost(16 << 20),
+    )(*distant(hidden), *nearby(back), *distant(routes, share))
 
 
 def solution(mesh):

time: 233 us -> 205 us (0.88)
  matrix products: 27 us -> 0 us
  Pallas kernels: 17.7 us -> 30.7 us
  local copies, waits for them, and re-layouts: 7.44 us -> 1.25 us
  blocking collectives: 95.4 us -> 92.5 us
  waiting for transfers between devices: 29.5 us -> 26.7 us
    dot_general x8 -> x0, matrix products: 27 us -> none  [the longest x4 18 us: expert_part(): return jnp.dot(act, wd, preferred_element_type=F32).astype(BF16)]
    pallas_call x7 -> x18, Pallas kernels: 17.7 us -> 30.7 us  [the longest x11 17.5 us: call(): pl.pallas_call(kernel, compiler_params=params(), cost_estimate=cost(flops...]
    ppermute x10 -> x12, waiting for transfers between devices: 15.9 us -> 12.1 us  [the longest x6 12.1 us: up(): return lax.ppermute(x, 'tp', up_ring)]
    reshape x4 -> x0, local copies, waits for them, and re-layouts: 2.48 us -> none  [the longest x1 1.24 us: local(): outgoing.reshape(experts, CAP, model)]
    ppermute x10 -> x12, starting transfers between devices: 14.4 us -> 13.2 us  [the longest x6 10.7 us: down(): return lax.ppermute(x, 'tp', down_ring)]
  transfers between devices with their start and end apart: 15 -> 17, of which waited for: 10 -> 7; matrix products, arithmetic and copies ran while one was open for 6% -> 1% of each run, Pallas kernels for 1% -> 10%
where the time goes in v1:
time: 205 us; the launch traced here: 204 us
  blocking collectives  92.5 us (45%)
  starting transfers between devices  52.8 us (26%)
  Pallas kernels  30.7 us (15%)
  waiting for transfers between devices  26.7 us (13%)
    all_to_all x1, blocking collectives, local(): own = lax.all_to_all(outgoing, SP, 0, 0, tiled=True)  41.9 us
    all_to_all x1, blocking collectives, local(): back = lax.all_to_all(summed, SP, 0, 0, tiled=True)  38.6 us
    all_to_all x1, starting transfers between devices, local(): by_slice = lax.all_to_all(summary, ZG, 0, 0, tiled=True)  23.7 us
    pallas_call x11, Pallas kernels, call(): pl.pallas_call(kernel, compiler_params=params(), cost_estimate=cost(flops...  17.5 us
    ppermute x6, waiting for transfers between devices, up(): return lax.ppermute(x, 'tp', up_ring)  12.1 us
    all_to_all x1, blocking collectives, local(): lax.all_to_all(mixed.reshape(shards, rows, model), 'tp', 0, 0, tiled=True)  12 us
    ppermute x6, starting transfers between devices, down(): return lax.ppermute(x, 'tp', down_ring)  10.7 us
    ppermute x3, starting transfers between devices, local(): lax.ppermute(total, 'zh', [(i, (i + k) % groups) for i in range(groups)])  9.46 us
  transfers between devices with their start and end apart: 17, of which 7 were waited for; matrix products, arithmetic and copies ran while one was open for 1% of the time, Pallas kernels for 10%

profile of v1, /device:TPU:33, one launch (start us, length us, event | category | flops | bytes accessed | tf_op | source)
XLA Modules:
  0.0 204.2 jit_solution(15580793793613072508)
XLA Ops:
  0.0 2.7 %shard_map.172 = bf16[8,80,128]{2,1,0:T(8,128)(2,1)} custom-call(bf16[128,128]{1,0:T(8,128)(2,1)} %wd.3, bf16[128,128]{1,0:T(8,128)(2,1)} %nd.3, f32[2,128]{1,0:T(2,128)} %wleak.3, f32[2,128]{1,0:T(2,128)} %nleak.3, bf16[128,384]{1,0:T(8,128)(2,1)} %v.3, f32[3,128]{1,0:T(4,128)} %bitcast.17), custom_call_target="tpu_custom_call" | custom-call | flops 4194304 | bytes 1048576 | tf_op jit(solution)/shard_map/pallas_call | solution.py:375
  2.7 23.7 %all-to-all-start = ((bf16[8,80,128]{2,1,0:T(8,128)(2,1)}), bf16[8,80,128]{2,1,0:T(8,128)(2,1)S(1)}, u32[]{:S(2)}, u32[]{:S(2)}) async-start(bf16[8,80,128]{2,1,0:T(8,128)(2,1)} %shard_map.172), calls=%async_computation | async-start | bytes 327680 | tf_op jit(solution)/shard_map/all_to_all | solution.py:381
  26.5 6.1 %all-to-all-done.got = bf16[8,80,128]{2,1,0:T(8,128)(2,1)S(1)} async-done(((bf16[8,80,128]{2,1,0:T(8,128)(2,1)}), bf16[8,80,128]{2,1,0:T(8,128)(2,1)S(1)}, u32[]{:S(2)}, u32[]{:S(2)}) %all-to-all-start) | async-done | bytes 163872 | tf_op jit(solution)/shard_map/all_to_all | solution.py:381
  33.4 9.3 %collective-permute-start.1 = (bf16[80,128]{1,0:T(8,128)(2,1)S(1)}, bf16[80,128]{1,0:T(8,128)(2,1)S(1)}, u32[]{:S(2)}, u32[]{:S(2)}) collective-permute-start(bf16[80,128]{1,0:T(8,128)(2,1)S(1)} %get-tuple-element.20), channel_id=1, source_target_pairs={{0,64},{32,96},{64,0},{96,32},{1,65},{33,97},{65,1},{97,33},{2,66}... | collective-permute-start | bytes 61448 | tf_op jit(solution)/shard_map/ppermute | solution.py:404
  42.7 2.1 %collective-permute-done.1.r2 = bf16[80,128]{1,0:T(8,128)(2,1)S(1)} collective-permute-done((bf16[80,128]{1,0:T(8,128)(2,1)S(1)}, bf16[80,128]{1,0:T(8,128)(2,1)S(1)}, u32[]{:S(2)}, u32[]{:S(2)}) %collective-permute-start.1) | collective-permute-done | bytes 20512 | tf_op jit(solution)/shard_map/ppermute | solution.py:404
  44.8 4.6 %collective-permute-done.2.r3 = bf16[80,128]{1,0:T(8,128)(2,1)S(1)} collective-permute-done((bf16[80,128]{1,0:T(8,128)(2,1)S(1)}, bf16[80,128]{1,0:T(8,128)(2,1)S(1)}, u32[]{:S(2)}, u32[]{:S(2)}) %collective-permute-start.2) | collective-permute-done | bytes 20512 | tf_op jit(solution)/shard_map/ppermute | solution.py:404
  49.4 1.3 shard_map.174
  50.7 6.4 %all-to-all-start.1 = ((bf16[8,64,128]{2,1,0:T(8,128)(2,1)}), bf16[8,64,128]{2,1,0:T(8,128)(2,1)S(1)}, u32[]{:S(2)}, u32[]{:S(2)}) async-start(bf16[8,64,128]{2,1,0:T(8,128)(2,1)} %shard_map.174), calls=%async_computation.1 | async-start | bytes 262144 | tf_op jit(solution)/shard_map/all_to_all | solution.py:414
  57.2 1.2 reshape.9.gain
  58.4 2.8 %shard_map.175 = (f32[128,384]{1,0:T(8,128)S(1)}, bf16[128,256]{1,0:T(8,128)(2,1)S(1)}, bf16[128,256]{1,0:T(8,128)(2,1)S(1)}) custom-call(bf16[128,128]{1,0:T(8,128)(2,1)} %wp.1, bf16[128,128]{1,0:T(8,128)(2,1)} %np_.1, bf16[128,128]{1,0:T(8,128)(2,1)} %wd.3, bf16[128,128]{1,0:T(8,128)(2,1)} %nd.3, f32[2,128]{1,0:T(2,128)} %wleak.3, f32[2,128]{1,0:T(2,128)} %nleak.3, ...), custom_call_target="tpu_custom_call" | custom-call | flops 67108864 | bytes 1048576 | tf_op jit(solution)/shard_map/pallas_call | solution.py:382
  61.2 1.9 all-to-all-done.1.states
  63.1 2.2 %shard_map.176 = bf16[128,2048]{1,0:T(8,128)(2,1)S(1)} custom-call(bf16[8,64,128]{2,1,0:T(8,128)(2,1)S(1)} %all-to-all-done.1.states, f32[128,384]{1,0:T(8,128)S(1)} %get-tuple-element.23.o_ref, bf16[128,256]{1,0:T(8,128)(2,1)S(1)} %get-tuple-element.24.qf, bf16[128,256]{1,0:T(8,128)(2,1)S(1)} %get-tuple-element.25.qb, bf16[128,384]{1,0:T(8,128)(2,1)} %gate.1, ...), custom_call_target="tpu_custom_call" | custom-call | flops 268435456 | bytes 1048576 | tf_op jit(solution)/shard_map/pallas_call | solution.py:415
  65.2 12.0 %all_to_all.25.parts = bf16[4,32,2048]{2,1,0:T(8,128)(2,1)S(1)} all-to-all(bf16[4,32,2048]{2,1,0:T(8,128)(2,1)S(1)} %bitcast.10), channel_id=1, replica_groups=mesh['grp'=2,'zh'=4,'zl'=4,'c'=2,'tp'=4] {'tp'}, dimensions={0} | all-to-all | bytes 1048576 | tf_op jit(solution)/shard_map/all_to_all | solution.py:426
  77.3 1.5 shard_map.177
  78.7 41.9 %all_to_all.26.got = bf16[32,4,2048]{2,1,0:T(4,128)(2,1)S(1)} all-to-all(bf16[32,4,2048]{2,1,0:T(4,128)(2,1)S(1)} %get-tuple-element.27), channel_id=1, replica_groups=mesh['grp'=2,'zh'=4,'zl'=4,'c'=2,'tp'=4] {'zh','zl','c'}, dimensions={0} | all-to-all | bytes 1048576 | tf_op jit(solution)/shard_map/all_to_all | solution.py:436
  121.1 2.4 %collective-permute-start.10 = (bf16[64,2048]{1,0:T(8,128)(2,1)S(1)}, bf16[64,2048]{1,0:T(8,128)(2,1)S(1)}, u32[]{:S(2)}, u32[]{:S(2)}) collective-permute-start(bf16[64,2048]{1,0:T(8,128)(2,1)S(1)} %get-tuple-element.29.high), channel_id=1, source_target_pairs={{0,3},{1,0},{2,1},{3,2},{4,7},{5,4},{6,5},{7,6},{8,11},{9,8},{10,9... | collective-permute-start | bytes 786440 | tf_op jit(solution)/shard_map/ppermute | solution.py:445
  123.5 1.4 collective-permute-start.9
  125.0 4.4 %collective-permute-done.4.x = bf16[64,2048]{1,0:T(8,128)(2,1)S(1)} collective-permute-done((bf16[64,2048]{1,0:T(8,128)(2,1)S(1)}, bf16[64,2048]{1,0:T(8,128)(2,1)S(1)}, u32[]{:S(2)}, u32[]{:S(2)}) %collective-permute-start.4) | collective-permute-done | bytes 262176 | tf_op jit(solution)/shard_map/ppermute | solution.py:442
  129.4 2.7 %collective-permute-start.11 = (bf16[64,2048]{1,0:T(8,128)(2,1)S(1)}, bf16[64,2048]{1,0:T(8,128)(2,1)S(1)}, u32[]{:S(2)}, u32[]{:S(2)}) collective-permute-start(bf16[64,2048]{1,0:T(8,128)(2,1)S(1)} %collective-permute-done.10.x), channel_id=1, source_target_pairs={{0,3},{1,0},{2,1},{3,2},{4,7},{5,4},{6,5},{7,6},{8,11},{9,8},{10,9... | collective-permute-start | bytes 786440 | tf_op jit(solution)/shard_map/ppermute | solution.py:445
  132.1 5.0 %shard_map.179 = (bf16[64,2048]{1,0:T(8,128)(2,1)S(1)}, bf16[64,2048]{1,0:T(8,128)(2,1)S(1)}, bf16[2048,896]{1,0:T(8,128)(2,1)S(1)}, bf16[2048,896]{1,0:T(8,128)(2,1)S(1)}, bf16[896,2048]{1,0:T(8,128)(2,1)S(1)}) custom-call(bf16[64,2048]{1,0:T(8,128)(2,1)S(1)} %get-tuple-element.28.low, bf16[64,2048]{1,0:T(8,128)(2,1)S(1)} %get-tuple-element.29.high, ...), custom_call_target="tpu_custom_call" | custom-call | flops 2147483648 | bytes 1048576 | tf_op jit(solution)/shard_map/pallas_call | solution.py:452
  137.1 2.0 shard_map.183
  139.2 1.4 collective-permute-done.5.x
  140.6 2.0 shard_map.181
  142.8 2.0 shard_map.185
  144.8 2.8 %collective-permute-start.12 = (bf16[64,2048]{1,0:T(8,128)(2,1)S(1)}, bf16[64,2048]{1,0:T(8,128)(2,1)S(1)}, u32[]{:S(2)}, u32[]{:S(2)}) collective-permute-start(bf16[64,2048]{1,0:T(8,128)(2,1)S(1)} %shard_map.185), channel_id=1, source_target_pairs={{0,3},{1,0},{2,1},{3,2},{4,7},{5,4},{6,5},{7,6},{8,11},{9,8},{10,9... | collective-permute-start | bytes 786440 | tf_op jit(solution)/shard_map/ppermute | solution.py:445
  147.6 2.0 shard_map.187
  149.9 2.0 shard_map.180.a
  151.9 2.0 shard_map.184.a
  154.3 2.8 %collective-permute-start.13 = (bf16[64,2048]{1,0:T(8,128)(2,1)S(1)}, bf16[64,2048]{1,0:T(8,128)(2,1)S(1)}, u32[]{:S(2)}, u32[]{:S(2)}) collective-permute-start(bf16[64,2048]{1,0:T(8,128)(2,1)S(1)} %shard_map.186), channel_id=1, source_target_pairs={{0,3},{1,0},{2,1},{3,2},{4,7},{5,4},{6,5},{7,6},{8,11},{9,8},{10,9... | collective-permute-start | bytes 786440 | tf_op jit(solution)/shard_map/ppermute | solution.py:445
  157.0 6.2 %collective-permute-done.7.low_b = bf16[64,2048]{1,0:T(8,128)(2,1)S(1)} collective-permute-done((bf16[64,2048]{1,0:T(8,128)(2,1)S(1)}, bf16[64,2048]{1,0:T(8,128)(2,1)S(1)}, u32[]{:S(2)}, u32[]{:S(2)}) %collective-permute-start.7) | collective-permute-done | bytes 262176 | tf_op jit(solution)/shard_map/ppermute | solution.py:442
  163.6 38.6 %all_to_all.27.back = bf16[32,4,2048]{2,1,0:T(4,128)(2,1)S(1)} all-to-all(bf16[32,4,2048]{2,1,0:T(4,128)(2,1)S(1)} %shard_map.188), channel_id=1, replica_groups=mesh['grp'=2,'zh'=4,'zl'=4,'c'=2,'tp'=4] {'zh','zl','c'}, dimensions={0} | all-to-all | bytes 1048576 | tf_op jit(solution)/shard_map/all_to_all | solution.py:494
  202.1 2.0 shard_map.189
  (27 shorter events, 2.7 us)
Async XLA Ops:
  2.7 29.9 %all-to-all-start = ((bf16[8,80,128]{2,1,0:T(8,128)(2,1)}), bf16[8,80,128]{2,1,0:T(8,128)(2,1)S(1)}, u32[]{:S(2)}, u32[]{:S(2)}) async-start(bf16[8,80,128]{2,1,0:T(8,128)(2,1)} %shard_map.172), calls=%async_computation | async-start | bytes 327680 | tf_op jit(solution)/shard_map/all_to_all | solution.py:381
  33.2 9.5 %collective-permute-start = (bf16[80,128]{1,0:T(8,128)(2,1)S(1)}, bf16[80,128]{1,0:T(8,128)(2,1)S(1)}, u32[]{:S(2)}, u32[]{:S(2)}) collective-permute-start(bf16[80,128]{1,0:T(8,128)(2,1)S(1)} %get-tuple-element.20), channel_id=1, source_target_pairs={{0,32},{32,64},{64,96},{96,0},{1,33},{33,65},{65,97},{97,1},{2,34}... | collective-permute-start | bytes 61448 | tf_op jit(solution)/shard_map/ppermute | solution.py:404
  33.4 11.5 %collective-permute-start.1 = (bf16[80,128]{1,0:T(8,128)(2,1)S(1)}, bf16[80,128]{1,0:T(8,128)(2,1)S(1)}, u32[]{:S(2)}, u32[]{:S(2)}) collective-permute-start(bf16[80,128]{1,0:T(8,128)(2,1)S(1)} %get-tuple-element.20), channel_id=1, source_target_pairs={{0,64},{32,96},{64,0},{96,32},{1,65},{33,97},{65,1},{97,33},{2,66}... | collective-permute-start | bytes 61448 | tf_op jit(solution)/shard_map/ppermute | solution.py:404
  42.7 6.7 %collective-permute-start.2 = (bf16[80,128]{1,0:T(8,128)(2,1)S(1)}, bf16[80,128]{1,0:T(8,128)(2,1)S(1)}, u32[]{:S(2)}, u32[]{:S(2)}) collective-permute-start(bf16[80,128]{1,0:T(8,128)(2,1)S(1)} %get-tuple-element.20), channel_id=1, source_target_pairs={{0,96},{32,0},{64,32},{96,64},{1,97},{33,1},{65,33},{97,65},{2,98}... | collective-permute-start | bytes 61448 | tf_op jit(solution)/shard_map/ppermute | solution.py:404
  50.7 12.3 %all-to-all-start.1 = ((bf16[8,64,128]{2,1,0:T(8,128)(2,1)}), bf16[8,64,128]{2,1,0:T(8,128)(2,1)S(1)}, u32[]{:S(2)}, u32[]{:S(2)}) async-start(bf16[8,64,128]{2,1,0:T(8,128)(2,1)} %shard_map.174), calls=%async_computation.1 | async-start | bytes 262144 | tf_op jit(solution)/shard_map/all_to_all | solution.py:414
  78.7 58.3 %copy-start = (bf16[32,2048]{1,0:T(8,128)(2,1)}, bf16[32,2048]{1,0:T(8,128)(2,1)S(1)}, u32[]{:S(2)}) copy-start(bf16[32,2048]{1,0:T(8,128)(2,1)S(1)} %get-tuple-element.26.hidden) | copy-start | bytes 393220
  120.7 8.7 %collective-permute-start.4 = (bf16[64,2048]{1,0:T(8,128)(2,1)S(1)}, bf16[64,2048]{1,0:T(8,128)(2,1)S(1)}, u32[]{:S(2)}, u32[]{:S(2)}) collective-permute-start(bf16[64,2048]{1,0:T(8,128)(2,1)S(1)} %get-tuple-element.28.low), channel_id=1, source_target_pairs={{0,1},{1,2},{2,3},{3,0},{4,5},{5,6},{6,7},{7,4},{8,9},{9,10},{10,1... | collective-permute-start | bytes 786440 | tf_op jit(solution)/shard_map/ppermute | solution.py:442
  121.1 8.3 %collective-permute-start.10 = (bf16[64,2048]{1,0:T(8,128)(2,1)S(1)}, bf16[64,2048]{1,0:T(8,128)(2,1)S(1)}, u32[]{:S(2)}, u32[]{:S(2)}) collective-permute-start(bf16[64,2048]{1,0:T(8,128)(2,1)S(1)} %get-tuple-element.29.high), channel_id=1, source_target_pairs={{0,3},{1,0},{2,1},{3,2},{4,7},{5,4},{6,5},{7,6},{8,11},{9,8},{10,9... | collective-permute-start | bytes 786440 | tf_op jit(solution)/shard_map/ppermute | solution.py:445
  123.5 26.1 %collective-permute-start.3 = (bf16[64,2048]{1,0:T(8,128)(2,1)S(1)}, bf16[64,2048]{1,0:T(8,128)(2,1)S(1)}, u32[]{:S(2)}, u32[]{:S(2)}) collective-permute-start(bf16[64,2048]{1,0:T(8,128)(2,1)S(1)} %get-tuple-element.28.low), channel_id=1, source_target_pairs={{0,3},{1,0},{2,1},{3,2},{4,7},{5,4},{6,5},{7,6},{8,11},{9,8},{10,9... | collective-permute-start | bytes 786440 | tf_op jit(solution)/shard_map/ppermute | solution.py:445
  123.5 28.4 %collective-permute-start.9 = (bf16[64,2048]{1,0:T(8,128)(2,1)S(1)}, bf16[64,2048]{1,0:T(8,128)(2,1)S(1)}, u32[]{:S(2)}, u32[]{:S(2)}) collective-permute-start(bf16[64,2048]{1,0:T(8,128)(2,1)S(1)} %get-tuple-element.29.high), channel_id=1, source_target_pairs={{0,1},{1,2},{2,3},{3,0},{4,5},{5,6},{6,7},{7,4},{8,9},{9,10},{10,1... | collective-permute-start | bytes 786440 | tf_op jit(solution)/shard_map/ppermute | solution.py:442
  129.4 11.2 %collective-permute-start.5 = (bf16[64,2048]{1,0:T(8,128)(2,1)S(1)}, bf16[64,2048]{1,0:T(8,128)(2,1)S(1)}, u32[]{:S(2)}, u32[]{:S(2)}) collective-permute-start(bf16[64,2048]{1,0:T(8,128)(2,1)S(1)} %collective-permute-done.4.x), channel_id=1, source_target_pairs={{0,1},{1,2},{2,3},{3,0},{4,5},{5,6},{6,7},{7,4},{8,9},{9,10},{10,1... | collective-permute-start | bytes 786440 | tf_op jit(solution)/shard_map/ppermute | solution.py:442
  129.4 13.4 %collective-permute-start.11 = (bf16[64,2048]{1,0:T(8,128)(2,1)S(1)}, bf16[64,2048]{1,0:T(8,128)(2,1)S(1)}, u32[]{:S(2)}, u32[]{:S(2)}) collective-permute-start(bf16[64,2048]{1,0:T(8,128)(2,1)S(1)} %collective-permute-done.10.x), channel_id=1, source_target_pairs={{0,3},{1,0},{2,1},{3,2},{4,7},{5,4},{6,5},{7,6},{8,11},{9,8},{10,9... | collective-permute-start | bytes 786440 | tf_op jit(solution)/shard_map/ppermute | solution.py:445
  139.1 18.0 %collective-permute-start.8 = (bf16[64,2048]{1,0:T(8,128)(2,1)S(1)}, bf16[64,2048]{1,0:T(8,128)(2,1)S(1)}, u32[]{:S(2)}, u32[]{:S(2)}) collective-permute-start(bf16[64,2048]{1,0:T(8,128)(2,1)S(1)} %shard_map.183), channel_id=1, source_target_pairs={{0,3},{1,0},{2,1},{3,2},{4,7},{5,4},{6,5},{7,6},{8,11},{9,8},{10,9... | collective-permute-start | bytes 786440 | tf_op jit(solution)/shard_map/ppermute | solution.py:445
  142.6 11.3 %collective-permute-start.6 = (bf16[64,2048]{1,0:T(8,128)(2,1)S(1)}, bf16[64,2048]{1,0:T(8,128)(2,1)S(1)}, u32[]{:S(2)}, u32[]{:S(2)}) collective-permute-start(bf16[64,2048]{1,0:T(8,128)(2,1)S(1)} %shard_map.181), channel_id=1, source_target_pairs={{0,1},{1,2},{2,3},{3,0},{4,5},{5,6},{6,7},{7,4},{8,9},{9,10},{10,1... | collective-permute-start | bytes 786440 | tf_op jit(solution)/shard_map/ppermute | solution.py:442
  144.8 9.4 %collective-permute-start.12 = (bf16[64,2048]{1,0:T(8,128)(2,1)S(1)}, bf16[64,2048]{1,0:T(8,128)(2,1)S(1)}, u32[]{:S(2)}, u32[]{:S(2)}) collective-permute-start(bf16[64,2048]{1,0:T(8,128)(2,1)S(1)} %shard_map.185), channel_id=1, source_target_pairs={{0,3},{1,0},{2,1},{3,2},{4,7},{5,4},{6,5},{7,6},{8,11},{9,8},{10,9... | collective-permute-start | bytes 786440 | tf_op jit(solution)/shard_map/ppermute | solution.py:445
  149.6 7.4 %collective-permute-start.14 = (bf16[64,2048]{1,0:T(8,128)(2,1)S(1)}, bf16[64,2048]{1,0:T(8,128)(2,1)S(1)}, u32[]{:S(2)}, u32[]{:S(2)}) collective-permute-start(bf16[64,2048]{1,0:T(8,128)(2,1)S(1)} %shard_map.187), channel_id=1, source_target_pairs={{0,1},{1,2},{2,3},{3,0},{4,5},{5,6},{6,7},{7,4},{8,9},{9,10},{10,1... | collective-permute-start | bytes 786440 | tf_op jit(solution)/shard_map/ppermute | solution.py:442
  154.0 9.2 %collective-permute-start.7 = (bf16[64,2048]{1,0:T(8,128)(2,1)S(1)}, bf16[64,2048]{1,0:T(8,128)(2,1)S(1)}, u32[]{:S(2)}, u32[]{:S(2)}) collective-permute-start(bf16[64,2048]{1,0:T(8,128)(2,1)S(1)} %shard_map.182), channel_id=1, source_target_pairs={{0,1},{1,2},{2,3},{3,0},{4,5},{5,6},{6,7},{7,4},{8,9},{9,10},{10,1... | collective-permute-start | bytes 786440 | tf_op jit(solution)/shard_map/ppermute | solution.py:442
  154.3 8.9 %collective-permute-start.13 = (bf16[64,2048]{1,0:T(8,128)(2,1)S(1)}, bf16[64,2048]{1,0:T(8,128)(2,1)S(1)}, u32[]{:S(2)}, u32[]{:S(2)}) collective-permute-start(bf16[64,2048]{1,0:T(8,128)(2,1)S(1)} %shard_map.186), channel_id=1, source_target_pairs={{0,3},{1,0},{2,1},{3,2},{4,7},{5,4},{6,5},{7,6},{8,11},{9,8},{10,9... | collective-permute-start | bytes 786440 | tf_op jit(solution)/shard_map/ppermute | solution.py:445

commit v2 on v1

--- a/solution.py
+++ b/solution.py
@@ -33,6 +33,16 @@
     return hi, (x - hi.astype(F32)).astype(BF16)
 
 
+def exact_sums(ones, x):
+    hi, rest = x.astype(BF16), x
+    parts = [hi]
+    for _ in range(2):
+        rest = rest - parts[-1].astype(F32)
+        parts.append(rest.astype(BF16))
+    bits = ones.astype(F32).astype(BF16)
+    return dot(jnp.concatenate([bits] * 3, axis=1), jnp.concatenate(parts, axis=0))
+
+
 def key_and_decay(logits, leaks, spikes):
     gate = jax.nn.sigmoid(-logits.astype(F32))
     rows = [leaks[d : d + 1] * gate for d in range(2)]
@@ -41,16 +51,16 @@
 
 def scan_terms(wd, nd, wleak, nleak, spk):
     n, width = wd.shape
-    exact = lax.Precision.HIGHEST
     heads = spk.shape[0]
     lane = iota((heads, 2 * width), 1)
     owner = jnp.where(lane < width, 0, jnp.where(lane < 3 * width // 2, 1, 2))
+    exact = lax.Precision.HIGHEST
     spikes = dot(spk, (iota((heads, 2 * width), 0) == owner).astype(F32), (0, 0), exact)
     kw, aw = key_and_decay(wd, wleak, spikes[:, :width])
     kn, an = key_and_decay(nd, nleak, spikes[:, width:])
     row, col = iota((n, n), 0), iota((n, n), 1)
-    fwd = dot((row >= col).astype(F32), jnp.concatenate([aw[0], an[0]], axis=1), precision=exact)
-    bwd = dot((row <= col).astype(F32), jnp.concatenate([aw[1], an[1]], axis=1), precision=exact)
+    fwd = exact_sums(row >= col, jnp.concatenate([aw[0], an[0]], axis=1))
+    bwd = exact_sums(row <= col, jnp.concatenate([aw[1], an[1]], axis=1))
     keys = [jnp.concatenate([kw[d], kn[d]], axis=1) for d in range(2)]
     return keys, (fwd, bwd)
 
@@ -192,7 +202,9 @@
             out[i, at, :] = (pre[i, at, :] + dec[i, at, :] * carry).astype(BF16)
 
 
-def mix_kernel(states, o_ref, qf, qb, gate, gain, proj, out):
+def mix_kernel(states, o_ref, qf, qb, gate, gain, proj_far, out, proj, sem):
+    fetch = pltpu.make_async_copy(proj_far, proj, sem)
+    fetch.start()
     n, width = o_ref.shape[0], states.shape[2]
     members = states.shape[0]
     entering = [
@@ -216,6 +228,7 @@
         total = total * lax.rsqrt(jnp.mean(total * total, axis=1, keepdims=True) + EPS)
         total = total * gain[:, at] * jax.nn.silu(gate[:, at].astype(F32))
         mixed.append(total.astype(BF16))
+    fetch.wait()
     out[...] = dot(jnp.concatenate(mixed, axis=1), proj[...]).astype(BF16)
 
 
@@ -232,7 +245,14 @@
     return jnp.logical_and(first, placed), jnp.logical_and(second, placed)
 
 
-def dispatch_kernel(parts, skip, gain, routes, hidden_ref, out):
+def route_kernel(routes, share, chosen_ref, hi_ref, lo_ref):
+    first, second = slot_matrix(routes[...])
+    chosen_ref[...] = jnp.logical_or(first, second).astype(F32).astype(BF16)
+    weight = jnp.where(first, share[0:1], 0.0) + jnp.where(second, share[1:2], 0.0)
+    hi_ref[...], lo_ref[...] = split_parts(weight)
+
+
+def dispatch_kernel(parts, skip, gain, chosen, hidden_ref, out):
     mixing = parts[0].astype(F32)
     for k in range(1, parts.shape[0]):
         mixing = mixing + parts[k].astype(F32)
@@ -241,9 +261,7 @@
     hidden = hidden_bf.astype(F32)
     normed = hidden * lax.rsqrt(jnp.mean(hidden * hidden, axis=1, keepdims=True) + EPS)
     normed = (normed * gain[...]).astype(BF16)
-    first, second = slot_matrix(routes[...])
-    chosen = jnp.logical_or(first, second).astype(F32).astype(BF16)
-    out[...] = block_of(dot(chosen, normed).astype(BF16))
+    out[...] = block_of(dot(chosen[...], normed).astype(BF16))
 
 
 def rows_of(block):
@@ -279,10 +297,13 @@
     part_high[...] = part[half:]
 
 
-def piece_kernel(x, wg, wu, wd, out):
-    rows = x[...]
+def piece_kernel(x, y, wg, wu, wd, out_x, out_y):
+    rows = jnp.concatenate([x[...], y[...]], axis=0)
     act = (jax.nn.silu(dot(rows, wg[...])) * dot(rows, wu[...])).astype(BF16)
-    out[...] = dot(act, wd[...]).astype(BF16)
+    part = dot(act, wd[...]).astype(BF16)
+    half = x.shape[0]
+    out_x[...] = part[:half]
+    out_y[...] = part[half:]
 
 
 def add_kernel(a, b, out):
@@ -296,12 +317,9 @@
     out[half:] = block_of((f(high_a) + f(high_b) + f(high_c)).astype(BF16))
 
 
-def combine_kernel(hidden, back, routes, share, out):
-    first, second = slot_matrix(routes[...])
-    weight = jnp.where(first, share[0:1], 0.0) + jnp.where(second, share[1:2], 0.0)
-    hi, lo = split_parts(weight)
+def combine_kernel(hidden, back, hi, lo, out):
     rows = rows_of(back[...])
-    mixture = dot(hi, rows, (0, 0)) + dot(lo, rows, (0, 0))
+    mixture = dot(hi[...], rows, (0, 0)) + dot(lo[...], rows, (0, 0))
     out[...] = (hidden[...].astype(F32) + mixture).astype(BF16)
 
 
@@ -379,6 +397,13 @@
         cost_estimate=cost(4 << 20),
     )(*distant(*decay_args))
     by_slice = lax.all_to_all(summary, ZG, 0, 0, tiled=True)
+    slots = experts * CAP
+    chosen, share_hi, share_lo = pl.pallas_call(
+        route_kernel,
+        out_shape=[sds((slots, rows), BF16)] * 3,
+        compiler_params=params(),
+        cost_estimate=cost(1 << 20),
+    )(*distant(assignments.T, assignment_share.T))
     inside, q_fwd, q_bwd = pl.pallas_call(
         local_kernel,
         out_shape=[
@@ -414,7 +439,12 @@
     entering = lax.all_to_all(carried, ZG, 0, 0, tiled=True)
     mixed = pl.pallas_call(
         mix_kernel,
+        in_specs=[VMEM] * 6 + [pl.BlockSpec(memory_space=pl.ANY)],
         out_shape=near((tokens, model), BF16),
+        scratch_shapes=[
+            pltpu.VMEM(result_mapping_matrix.shape, BF16),
+            pltpu.SemaphoreType.DMA,
+        ],
         compiler_params=params(),
         cost_estimate=cost(256 << 20),
     )(
@@ -424,15 +454,12 @@
         ),
     )
     parts = lax.all_to_all(mixed.reshape(shards, rows, model), "tp", 0, 0, tiled=True)
-    routes = assignments.T
-    share = assignment_share.T
-    slots = experts * CAP
     hidden, outgoing = pl.pallas_call(
         dispatch_kernel,
         out_shape=[sds((rows, model), BF16), near((experts, CAP, model), BF16)],
         compiler_params=params(),
         cost_estimate=cost(16 << 20),
-    )(*nearby(parts), *distant(skip_stream, specialist_scale_vector.reshape(1, model), routes))
+    )(*nearby(parts), *distant(skip_stream, specialist_scale_vector.reshape(1, model), chosen))
     own = lax.all_to_all(outgoing, SP, 0, 0, tiled=True)
 
     up_ring = [(i, (i + 1) % shards) for i in range(shards)]
@@ -471,18 +498,18 @@
         scratch_shapes=[pltpu.SemaphoreType.DMA((3,))],
     )
 
-    def part(x):
-        return call(piece_kernel, 1 << 30, *nearby(x, *weights))
+    def part(x, y):
+        return call(piece_kernel, 2 << 30, *nearby(x, y, *weights), out_shape=[piece] * 2)
 
     def add(a, b):
         return call(add_kernel, 1 << 20, *nearby(a, b))
 
     far_low, far_high = up(left_low), down(right_high)
-    for_left_low, for_right_high = part(left_low), part(right_high)
+    for_left_low, for_right_high = part(left_low, right_high)
     got_high, got_low = up(for_right_high), down(for_left_low)
-    for_left_high, for_right_low = part(left_high), part(right_low)
-    add_low = up(part(far_low))
-    add_high = down(part(far_high))
+    for_left_high, for_right_low = part(left_high, right_low)
+    for_far_low, for_far_high = part(far_low, far_high)
+    add_low, add_high = up(for_far_low), down(for_far_high)
     last_low = up(add(for_right_low, add_low))
     last_high = down(add(for_left_high, add_high))
     summed = call(
@@ -497,7 +524,7 @@
         out_shape=sds((rows, model), BF16),
         compiler_params=params(),
         cost_estimate=cost(16 << 20),
-    )(*distant(hidden), *nearby(back), *distant(routes, share))
+    )(*distant(hidden), *nearby(back), *distant(share_hi, share_lo))
 
 
 def solution(mesh):

time: 205 us -> 204 us (level)
  blocking collectives: 92.5 us -> 83.3 us
  waiting for transfers between devices: 26.7 us -> 32.4 us
  starting transfers between devices: 52.8 us -> 57.4 us
  Pallas kernels: 30.7 us -> 26.1 us
  local copies, waits for them, and re-layouts: 1.25 us -> 3.71 us
    all_to_all x1 -> x0, blocking collectives: 12 us -> none  [local(): lax.all_to_all(mixed.reshape(shards, rows, model), 'tp', 0, 0, tiled=True)]
    pallas_call x11 -> x8, Pallas kernels: 17.5 us -> 11.1 us  [call(): pl.pallas_call(kernel, compiler_params=params(), cost_estimate=cost(flops...]
    all_to_all x0 -> x1, waiting for transfers between devices: none -> 5.37 us  [local(): lax.all_to_all(mixed.reshape(shards, rows, model), 'tp', 0, 0, tiled=True)]
    all_to_all x0 -> x1, starting transfers between devices: none -> 4.32 us  [local(): lax.all_to_all(mixed.reshape(shards, rows, model), 'tp', 0, 0, tiled=True)]
    unnamed x2 -> x8, local copies, waits for them, and re-layouts: 0.01 us -> 2.47 us
    pallas_call x1 -> x2, Pallas kernels: 2.16 us -> 4.59 us  [the longest x1 3.73 us: local(): pl.pallas_call(mix_kernel, in_specs=[VMEM] * 6 + [pl.BlockSpec(memory_spa...]
  transfers between devices with their start and end apart: 17 -> 18, of which waited for: 7 -> 9; matrix products, arithmetic and copies ran while one was open for 1% -> 1% of each run, Pallas kernels for 10% -> 7%
where the time goes in v2:
time: 204 us; the launch traced here: 203 us
  blocking collectives  83.3 us (41%)
  starting transfers between devices  57.4 us (28%)
  waiting for transfers between devices  32.4 us (16%)
  Pallas kernels  26.1 us (13%)
  local copies, waits for them, and re-layouts  3.71 us (2%)
    all_to_all x1, blocking collectives, local(): own = lax.all_to_all(outgoing, SP, 0, 0, tiled=True)  43 us
    all_to_all x1, blocking collectives, local(): back = lax.all_to_all(summed, SP, 0, 0, tiled=True)  40.2 us
    all_to_all x1, starting transfers between devices, local(): by_slice = lax.all_to_all(summary, ZG, 0, 0, tiled=True)  23.7 us
    pallas_call x8, Pallas kernels, call(): pl.pallas_call(kernel, compiler_params=params(), cost_estimate=cost(flops...  11.1 us
    ppermute x6, starting transfers between devices, down(): return lax.ppermute(x, 'tp', down_ring)  10.6 us
    ppermute x6, waiting for transfers between devices, up(): return lax.ppermute(x, 'tp', up_ring)  10.6 us
    ppermute x3, starting transfers between devices, local(): lax.ppermute(total, 'zh', [(i, (i + k) % groups) for i in range(groups)])  9.61 us
    ppermute x3, waiting for transfers between devices, local(): lax.ppermute(total, 'zh', [(i, (i + k) % groups) for i in range(groups)])  6.39 us
  transfers between devices with their start and end apart: 18, of which 9 were waited for; matrix products, arithmetic and copies ran while one was open for 1% of the time, Pallas kernels for 7%

profile of v2, /device:TPU:33, one launch (start us, length us, event | category | flops | bytes accessed | tf_op | source)
XLA Modules:
  0.0 203.1 jit_solution(4537537414741954484)
XLA Ops:
  0.0 2.5 %shard_map.172 = bf16[8,80,128]{2,1,0:T(8,128)(2,1)} custom-call(bf16[128,128]{1,0:T(8,128)(2,1)} %wd.3, bf16[128,128]{1,0:T(8,128)(2,1)} %nd.3, f32[2,128]{1,0:T(2,128)} %wleak.3, f32[2,128]{1,0:T(2,128)} %nleak.3, bf16[128,384]{1,0:T(8,128)(2,1)} %v.3, f32[3,128]{1,0:T(4,128)} %bitcast.14), custom_call_target="tpu_custom_call" | custom-call | flops 4194304 | bytes 1048576 | tf_op jit(solution)/shard_map/pallas_call | solution.py:393
  2.5 23.7 %all-to-all-start = ((bf16[8,80,128]{2,1,0:T(8,128)(2,1)}), bf16[8,80,128]{2,1,0:T(8,128)(2,1)S(1)}, u32[]{:S(2)}, u32[]{:S(2)}) async-start(bf16[8,80,128]{2,1,0:T(8,128)(2,1)} %shard_map.172), calls=%async_computation | async-start | bytes 327680 | tf_op jit(solution)/shard_map/all_to_all | solution.py:399
  26.3 6.1 %all-to-all-done.got = bf16[8,80,128]{2,1,0:T(8,128)(2,1)S(1)} async-done(((bf16[8,80,128]{2,1,0:T(8,128)(2,1)}), bf16[8,80,128]{2,1,0:T(8,128)(2,1)S(1)}, u32[]{:S(2)}, u32[]{:S(2)}) %all-to-all-start) | async-done | bytes 163872 | tf_op jit(solution)/shard_map/all_to_all | solution.py:399
  33.1 4.4 %collective-permute-start.2 = (bf16[80,128]{1,0:T(8,128)(2,1)S(1)}, bf16[80,128]{1,0:T(8,128)(2,1)S(1)}, u32[]{:S(2)}, u32[]{:S(2)}) collective-permute-start(bf16[80,128]{1,0:T(8,128)(2,1)S(1)} %get-tuple-element.29), channel_id=1, source_target_pairs={{0,96},{32,0},{64,32},{96,64},{1,97},{33,1},{65,33},{97,65},{2,98}... | collective-permute-start | bytes 61448 | tf_op jit(solution)/shard_map/ppermute | solution.py:429
  37.5 5.2 %collective-permute-start = (bf16[80,128]{1,0:T(8,128)(2,1)S(1)}, bf16[80,128]{1,0:T(8,128)(2,1)S(1)}, u32[]{:S(2)}, u32[]{:S(2)}) collective-permute-start(bf16[80,128]{1,0:T(8,128)(2,1)S(1)} %get-tuple-element.29), channel_id=1, source_target_pairs={{0,32},{32,64},{64,96},{96,0},{1,33},{33,65},{65,97},{97,1},{2,34}... | collective-permute-start | bytes 61448 | tf_op jit(solution)/shard_map/ppermute | solution.py:429
  42.7 6.4 %collective-permute-done.1.r2 = bf16[80,128]{1,0:T(8,128)(2,1)S(1)} collective-permute-done((bf16[80,128]{1,0:T(8,128)(2,1)S(1)}, bf16[80,128]{1,0:T(8,128)(2,1)S(1)}, u32[]{:S(2)}, u32[]{:S(2)}) %collective-permute-start.1) | collective-permute-done | bytes 20512 | tf_op jit(solution)/shard_map/ppermute | solution.py:429
  49.1 1.3 shard_map.174
  50.4 5.6 %all-to-all-start.1 = ((bf16[8,64,128]{2,1,0:T(8,128)(2,1)}), bf16[8,64,128]{2,1,0:T(8,128)(2,1)S(1)}, u32[]{:S(2)}, u32[]{:S(2)}) async-start(bf16[8,64,128]{2,1,0:T(8,128)(2,1)} %shard_map.174), calls=%async_computation.1 | async-start | bytes 262144 | tf_op jit(solution)/shard_map/all_to_all | solution.py:439
  56.0 1.2 reshape.9.gain
  57.2 2.5 %shard_map.175 = (f32[128,384]{1,0:T(8,128)S(1)}, bf16[128,256]{1,0:T(8,128)(2,1)S(1)}, bf16[128,256]{1,0:T(8,128)(2,1)S(1)}) custom-call(bf16[128,128]{1,0:T(8,128)(2,1)} %wp.1, bf16[128,128]{1,0:T(8,128)(2,1)} %np_.1, bf16[128,128]{1,0:T(8,128)(2,1)} %wd.3, bf16[128,128]{1,0:T(8,128)(2,1)} %nd.3, f32[2,128]{1,0:T(2,128)} %wleak.3, f32[2,128]{1,0:T(2,128)} %nleak.3, ...), custom_call_target="tpu_custom_call" | custom-call | flops 67108864 | bytes 1048576 | tf_op jit(solution)/shard_map/pallas_call | solution.py:407
  59.8 2.2 %all-to-all-done.1.states = bf16[8,64,128]{2,1,0:T(8,128)(2,1)S(1)} async-done(((bf16[8,64,128]{2,1,0:T(8,128)(2,1)}), bf16[8,64,128]{2,1,0:T(8,128)(2,1)S(1)}, u32[]{:S(2)}, u32[]{:S(2)}) %all-to-all-start.1) | async-done | bytes 131104 | tf_op jit(solution)/shard_map/all_to_all | solution.py:439
  61.9 3.7 %shard_map.176 = bf16[128,2048]{1,0:T(8,128)(2,1)} custom-call(bf16[8,64,128]{2,1,0:T(8,128)(2,1)S(1)} %all-to-all-done.1.states, f32[128,384]{1,0:T(8,128)S(1)} %get-tuple-element.32.o_ref, bf16[128,256]{1,0:T(8,128)(2,1)S(1)} %get-tuple-element.33.qf, bf16[128,256]{1,0:T(8,128)(2,1)S(1)} %get-tuple-element.34.qb, bf16[128,384]{1,0:T(8,128)(2,1)} %gate.1, ...), custom_call_target="tpu_custom_call" | custom-call | flops 268435456 | bytes 1048576 | tf_op jit(solution)/shard_map/pallas_call | solution.py:440
  65.7 4.3 %all-to-all-start.2 = ((bf16[4,32,2048]{2,1,0:T(8,128)(2,1)}), bf16[4,32,2048]{2,1,0:T(8,128)(2,1)S(1)}, u32[]{:S(2)}, u32[]{:S(2)}) async-start(bf16[4,32,2048]{2,1,0:T(8,128)(2,1)} %bitcast.3), calls=%async_computation.2 | async-start | bytes 1048576 | tf_op jit(solution)/shard_map/all_to_all | solution.py:456
  72.7 5.4 %all-to-all-done.2.parts = bf16[4,32,2048]{2,1,0:T(8,128)(2,1)S(1)} async-done(((bf16[4,32,2048]{2,1,0:T(8,128)(2,1)}), bf16[4,32,2048]{2,1,0:T(8,128)(2,1)S(1)}, u32[]{:S(2)}, u32[]{:S(2)}) %all-to-all-start.2) | async-done | bytes 524320 | tf_op jit(solution)/shard_map/all_to_all | solution.py:456
  78.0 1.5 shard_map.178
  80.1 43.0 %all_to_all.25.got = bf16[32,4,2048]{2,1,0:T(4,128)(2,1)S(1)} all-to-all(bf16[32,4,2048]{2,1,0:T(4,128)(2,1)S(1)} %get-tuple-element.37), channel_id=1, replica_groups=mesh['grp'=2,'zh'=4,'zl'=4,'c'=2,'tp'=4] {'zh','zl','c'}, dimensions={0} | all-to-all | bytes 1048576 | tf_op jit(solution)/shard_map/all_to_all | solution.py:463
  123.7 2.4 %collective-permute-start.7 = (bf16[64,2048]{1,0:T(8,128)(2,1)S(1)}, bf16[64,2048]{1,0:T(8,128)(2,1)S(1)}, u32[]{:S(2)}, u32[]{:S(2)}) collective-permute-start(bf16[64,2048]{1,0:T(8,128)(2,1)S(1)} %get-tuple-element.39.high), channel_id=1, source_target_pairs={{0,3},{1,0},{2,1},{3,2},{4,7},{5,4},{6,5},{7,6},{8,11},{9,8},{10,9... | collective-permute-start | bytes 786440 | tf_op jit(solution)/shard_map/ppermute | solution.py:472
  126.1 5.9 %collective-permute-done.5.x = bf16[64,2048]{1,0:T(8,128)(2,1)S(1)} collective-permute-done((bf16[64,2048]{1,0:T(8,128)(2,1)S(1)}, bf16[64,2048]{1,0:T(8,128)(2,1)S(1)}, u32[]{:S(2)}, u32[]{:S(2)}) %collective-permute-start.5) | collective-permute-done | bytes 262176 | tf_op jit(solution)/shard_map/ppermute | solution.py:469
  132.0 2.7 %collective-permute-start.8 = (bf16[64,2048]{1,0:T(8,128)(2,1)S(1)}, bf16[64,2048]{1,0:T(8,128)(2,1)S(1)}, u32[]{:S(2)}, u32[]{:S(2)}) collective-permute-start(bf16[64,2048]{1,0:T(8,128)(2,1)S(1)} %collective-permute-done.7.y), channel_id=1, source_target_pairs={{0,3},{1,0},{2,1},{3,2},{4,7},{5,4},{6,5},{7,6},{8,11},{9,8},{10,9... | collective-permute-start | bytes 786440 | tf_op jit(solution)/shard_map/ppermute | solution.py:472
  134.7 1.4 collective-permute-start.3
  136.1 5.0 %shard_map.180 = (bf16[64,2048]{1,0:T(8,128)(2,1)S(1)}, bf16[64,2048]{1,0:T(8,128)(2,1)S(1)}, bf16[2048,896]{1,0:T(8,128)(2,1)S(1)}, bf16[2048,896]{1,0:T(8,128)(2,1)S(1)}, bf16[896,2048]{1,0:T(8,128)(2,1)S(1)}) custom-call(bf16[64,2048]{1,0:T(8,128)(2,1)S(1)} %get-tuple-element.38.low, bf16[64,2048]{1,0:T(8,128)(2,1)S(1)} %get-tuple-element.39.high, ...), custom_call_target="tpu_custom_call" | custom-call | flops 2147483648 | bytes 1048576 | tf_op jit(solution)/shard_map/pallas_call | solution.py:479
  141.1 1.9 shard_map.182
  143.1 2.6 %collective-permute-start.12 = (bf16[64,2048]{1,0:T(8,128)(2,1)S(1)}, bf16[64,2048]{1,0:T(8,128)(2,1)S(1)}, u32[]{:S(2)}, u32[]{:S(2)}) collective-permute-start(bf16[64,2048]{1,0:T(8,128)(2,1)S(1)} %get-tuple-element.49), channel_id=1, source_target_pairs={{0,3},{1,0},{2,1},{3,2},{4,7},{5,4},{6,5},{7,6},{8,11},{9,8},{10,9... | collective-permute-start | bytes 786440 | tf_op jit(solution)/shard_map/ppermute | solution.py:472
  145.8 1.9 shard_map.184
  147.8 1.4 collective-permute-start.14
  149.2 1.9 shard_map.181
  151.4 2.8 %collective-permute-start.13 = (bf16[64,2048]{1,0:T(8,128)(2,1)S(1)}, bf16[64,2048]{1,0:T(8,128)(2,1)S(1)}, u32[]{:S(2)}, u32[]{:S(2)}) collective-permute-start(bf16[64,2048]{1,0:T(8,128)(2,1)S(1)} %shard_map.185), channel_id=1, source_target_pairs={{0,3},{1,0},{2,1},{3,2},{4,7},{5,4},{6,5},{7,6},{8,11},{9,8},{10,9... | collective-permute-start | bytes 786440 | tf_op jit(solution)/shard_map/ppermute | solution.py:472
  154.1 0.9 collective-permute-done.11.low_c
  155.4 4.3 %collective-permute-done.10.low_b = bf16[64,2048]{1,0:T(8,128)(2,1)S(1)} collective-permute-done((bf16[64,2048]{1,0:T(8,128)(2,1)S(1)}, bf16[64,2048]{1,0:T(8,128)(2,1)S(1)}, u32[]{:S(2)}, u32[]{:S(2)}) %collective-permute-start.10) | collective-permute-done | bytes 262176 | tf_op jit(solution)/shard_map/ppermute | solution.py:469
  159.7 0.9 collective-permute-done.13.high_b
  161.0 40.2 %all_to_all.26.back = bf16[32,4,2048]{2,1,0:T(4,128)(2,1)S(1)} all-to-all(bf16[32,4,2048]{2,1,0:T(4,128)(2,1)S(1)} %shard_map.186), channel_id=1, replica_groups=mesh['grp'=2,'zh'=4,'zl'=4,'c'=2,'tp'=4] {'zh','zl','c'}, dimensions={0} | all-to-all | bytes 1048576 | tf_op jit(solution)/shard_map/all_to_all | solution.py:521
  201.2 1.9 shard_map.187
  (32 shorter events, 5.9 us)
Async XLA Ops:
  2.5 29.9 %all-to-all-start = ((bf16[8,80,128]{2,1,0:T(8,128)(2,1)}), bf16[8,80,128]{2,1,0:T(8,128)(2,1)S(1)}, u32[]{:S(2)}, u32[]{:S(2)}) async-start(bf16[8,80,128]{2,1,0:T(8,128)(2,1)} %shard_map.172), calls=%async_computation | async-start | bytes 327680 | tf_op jit(solution)/shard_map/all_to_all | solution.py:399
  33.1 9.6 %collective-permute-start.2 = (bf16[80,128]{1,0:T(8,128)(2,1)S(1)}, bf16[80,128]{1,0:T(8,128)(2,1)S(1)}, u32[]{:S(2)}, u32[]{:S(2)}) collective-permute-start(bf16[80,128]{1,0:T(8,128)(2,1)S(1)} %get-tuple-element.29), channel_id=1, source_target_pairs={{0,96},{32,0},{64,32},{96,64},{1,97},{33,1},{65,33},{97,65},{2,98}... | collective-permute-start | bytes 61448 | tf_op jit(solution)/shard_map/ppermute | solution.py:429
  37.5 11.6 %collective-permute-start.1 = (bf16[80,128]{1,0:T(8,128)(2,1)S(1)}, bf16[80,128]{1,0:T(8,128)(2,1)S(1)}, u32[]{:S(2)}, u32[]{:S(2)}) collective-permute-start(bf16[80,128]{1,0:T(8,128)(2,1)S(1)} %get-tuple-element.29), channel_id=1, source_target_pairs={{0,64},{32,96},{64,0},{96,32},{1,65},{33,97},{65,1},{97,33},{2,66}... | collective-permute-start | bytes 61448 | tf_op jit(solution)/shard_map/ppermute | solution.py:429
  37.5 11.6 %collective-permute-start = (bf16[80,128]{1,0:T(8,128)(2,1)S(1)}, bf16[80,128]{1,0:T(8,128)(2,1)S(1)}, u32[]{:S(2)}, u32[]{:S(2)}) collective-permute-start(bf16[80,128]{1,0:T(8,128)(2,1)S(1)} %get-tuple-element.29), channel_id=1, source_target_pairs={{0,32},{32,64},{64,96},{96,0},{1,33},{33,65},{65,97},{97,1},{2,34}... | collective-permute-start | bytes 61448 | tf_op jit(solution)/shard_map/ppermute | solution.py:429
  50.4 11.5 %all-to-all-start.1 = ((bf16[8,64,128]{2,1,0:T(8,128)(2,1)}), bf16[8,64,128]{2,1,0:T(8,128)(2,1)S(1)}, u32[]{:S(2)}, u32[]{:S(2)}) async-start(bf16[8,64,128]{2,1,0:T(8,128)(2,1)} %shard_map.174), calls=%async_computation.1 | async-start | bytes 262144 | tf_op jit(solution)/shard_map/all_to_all | solution.py:439
  65.7 12.4 %all-to-all-start.2 = ((bf16[4,32,2048]{2,1,0:T(8,128)(2,1)}), bf16[4,32,2048]{2,1,0:T(8,128)(2,1)S(1)}, u32[]{:S(2)}, u32[]{:S(2)}) async-start(bf16[4,32,2048]{2,1,0:T(8,128)(2,1)} %bitcast.3), calls=%async_computation.2 | async-start | bytes 1048576 | tf_op jit(solution)/shard_map/all_to_all | solution.py:456
  70.8 0.6 copy-start.1
  71.4 0.6 copy-start.2
  72.1 0.6 copy-start.3
  79.5 0.7 copy-start
  123.3 8.7 %collective-permute-start.5 = (bf16[64,2048]{1,0:T(8,128)(2,1)S(1)}, bf16[64,2048]{1,0:T(8,128)(2,1)S(1)}, u32[]{:S(2)}, u32[]{:S(2)}) collective-permute-start(bf16[64,2048]{1,0:T(8,128)(2,1)S(1)} %get-tuple-element.38.low), channel_id=1, source_target_pairs={{0,1},{1,2},{2,3},{3,0},{4,5},{5,6},{6,7},{7,4},{8,9},{9,10},{10,1... | collective-permute-start | bytes 786440 | tf_op jit(solution)/shard_map/ppermute | solution.py:469
  123.7 8.3 %collective-permute-start.7 = (bf16[64,2048]{1,0:T(8,128)(2,1)S(1)}, bf16[64,2048]{1,0:T(8,128)(2,1)S(1)}, u32[]{:S(2)}, u32[]{:S(2)}) collective-permute-start(bf16[64,2048]{1,0:T(8,128)(2,1)S(1)} %get-tuple-element.39.high), channel_id=1, source_target_pairs={{0,3},{1,0},{2,1},{3,2},{4,7},{5,4},{6,5},{7,6},{8,11},{9,8},{10,9... | collective-permute-start | bytes 786440 | tf_op jit(solution)/shard_map/ppermute | solution.py:472
  132.0 9.1 %collective-permute-start.6 = (bf16[64,2048]{1,0:T(8,128)(2,1)S(1)}, bf16[64,2048]{1,0:T(8,128)(2,1)S(1)}, u32[]{:S(2)}, u32[]{:S(2)}) collective-permute-start(bf16[64,2048]{1,0:T(8,128)(2,1)S(1)} %collective-permute-done.5.x), channel_id=1, source_target_pairs={{0,1},{1,2},{2,3},{3,0},{4,5},{5,6},{6,7},{7,4},{8,9},{9,10},{10,1... | collective-permute-start | bytes 786440 | tf_op jit(solution)/shard_map/ppermute | solution.py:469
  132.0 9.1 %collective-permute-start.8 = (bf16[64,2048]{1,0:T(8,128)(2,1)S(1)}, bf16[64,2048]{1,0:T(8,128)(2,1)S(1)}, u32[]{:S(2)}, u32[]{:S(2)}) collective-permute-start(bf16[64,2048]{1,0:T(8,128)(2,1)S(1)} %collective-permute-done.7.y), channel_id=1, source_target_pairs={{0,3},{1,0},{2,1},{3,2},{4,7},{5,4},{6,5},{7,6},{8,11},{9,8},{10,9... | collective-permute-start | bytes 786440 | tf_op jit(solution)/shard_map/ppermute | solution.py:472
  134.7 13.1 %collective-permute-start.4 = (bf16[64,2048]{1,0:T(8,128)(2,1)S(1)}, bf16[64,2048]{1,0:T(8,128)(2,1)S(1)}, u32[]{:S(2)}, u32[]{:S(2)}) collective-permute-start(bf16[64,2048]{1,0:T(8,128)(2,1)S(1)} %get-tuple-element.38.low), channel_id=1, source_target_pairs={{0,3},{1,0},{2,1},{3,2},{4,7},{5,4},{6,5},{7,6},{8,11},{9,8},{10,9... | collective-permute-start | bytes 786440 | tf_op jit(solution)/shard_map/ppermute | solution.py:472
  134.7 14.5 %collective-permute-start.3 = (bf16[64,2048]{1,0:T(8,128)(2,1)S(1)}, bf16[64,2048]{1,0:T(8,128)(2,1)S(1)}, u32[]{:S(2)}, u32[]{:S(2)}) collective-permute-start(bf16[64,2048]{1,0:T(8,128)(2,1)S(1)} %get-tuple-element.39.high), channel_id=1, source_target_pairs={{0,1},{1,2},{2,3},{3,0},{4,5},{5,6},{6,7},{7,4},{8,9},{9,10},{10,1... | collective-permute-start | bytes 786440 | tf_op jit(solution)/shard_map/ppermute | solution.py:469
  143.0 8.1 %collective-permute-start.9 = (bf16[64,2048]{1,0:T(8,128)(2,1)S(1)}, bf16[64,2048]{1,0:T(8,128)(2,1)S(1)}, u32[]{:S(2)}, u32[]{:S(2)}) collective-permute-start(bf16[64,2048]{1,0:T(8,128)(2,1)S(1)} %get-tuple-element.45), channel_id=1, source_target_pairs={{0,1},{1,2},{2,3},{3,0},{4,5},{5,6},{6,7},{7,4},{8,9},{9,10},{10,1... | collective-permute-start | bytes 786440 | tf_op jit(solution)/shard_map/ppermute | solution.py:469
  143.1 8.2 %collective-permute-start.12 = (bf16[64,2048]{1,0:T(8,128)(2,1)S(1)}, bf16[64,2048]{1,0:T(8,128)(2,1)S(1)}, u32[]{:S(2)}, u32[]{:S(2)}) collective-permute-start(bf16[64,2048]{1,0:T(8,128)(2,1)S(1)} %get-tuple-element.49), channel_id=1, source_target_pairs={{0,3},{1,0},{2,1},{3,2},{4,7},{5,4},{6,5},{7,6},{8,11},{9,8},{10,9... | collective-permute-start | bytes 786440 | tf_op jit(solution)/shard_map/ppermute | solution.py:472
  147.6 7.4 %collective-permute-start.11 = (bf16[64,2048]{1,0:T(8,128)(2,1)S(1)}, bf16[64,2048]{1,0:T(8,128)(2,1)S(1)}, u32[]{:S(2)}, u32[]{:S(2)}) collective-permute-start(bf16[64,2048]{1,0:T(8,128)(2,1)S(1)} %get-tuple-element.46), channel_id=1, source_target_pairs={{0,3},{1,0},{2,1},{3,2},{4,7},{5,4},{6,5},{7,6},{8,11},{9,8},{10,9... | collective-permute-start | bytes 786440 | tf_op jit(solution)/shard_map/ppermute | solution.py:472
  147.8 7.6 %collective-permute-start.14 = (bf16[64,2048]{1,0:T(8,128)(2,1)S(1)}, bf16[64,2048]{1,0:T(8,128)(2,1)S(1)}, u32[]{:S(2)}, u32[]{:S(2)}) collective-permute-start(bf16[64,2048]{1,0:T(8,128)(2,1)S(1)} %get-tuple-element.50), channel_id=1, source_target_pairs={{0,1},{1,2},{2,3},{3,0},{4,5},{5,6},{6,7},{7,4},{8,9},{9,10},{10,1... | collective-permute-start | bytes 786440 | tf_op jit(solution)/shard_map/ppermute | solution.py:469
  151.2 8.6 %collective-permute-start.10 = (bf16[64,2048]{1,0:T(8,128)(2,1)S(1)}, bf16[64,2048]{1,0:T(8,128)(2,1)S(1)}, u32[]{:S(2)}, u32[]{:S(2)}) collective-permute-start(bf16[64,2048]{1,0:T(8,128)(2,1)S(1)} %shard_map.183), channel_id=1, source_target_pairs={{0,1},{1,2},{2,3},{3,0},{4,5},{5,6},{6,7},{7,4},{8,9},{9,10},{10,1... | collective-permute-start | bytes 786440 | tf_op jit(solution)/shard_map/ppermute | solution.py:469
  151.4 9.2 %collective-permute-start.13 = (bf16[64,2048]{1,0:T(8,128)(2,1)S(1)}, bf16[64,2048]{1,0:T(8,128)(2,1)S(1)}, u32[]{:S(2)}, u32[]{:S(2)}) collective-permute-start(bf16[64,2048]{1,0:T(8,128)(2,1)S(1)} %shard_map.185), channel_id=1, source_target_pairs={{0,3},{1,0},{2,1},{3,2},{4,7},{5,4},{6,5},{7,6},{8,11},{9,8},{10,9... | collective-permute-start | bytes 786440 | tf_op jit(solution)/shard_map/ppermute | solution.py:472

commit v3 on v2

--- a/solution.py
+++ b/solution.py
@@ -97,7 +97,12 @@
         out[j, 2 * SLICE :, :] = block
 
 
-def local_kernel(wp, np_, wd, nd, wleak, nleak, v, spk, o_ref, qf_ref, qb_ref):
+def local_kernel(
+    wp, np_, wd, nd, wleak, nleak, v, spk, gate, gain, proj_far, o_ref, qf_ref, qb_ref, scale_ref, proj, sem
+):
+    fetch = pltpu.make_async_copy(proj_far, proj, sem)
+    fetch.start()
+    scale_ref[...] = gain[...] * jax.nn.silu(gate[...].astype(F32))
     keys, running = scan_terms(wd[...], nd[...], wleak[...], nleak[...], spk[...])
     _, width = wd.shape
     q = jnp.concatenate(
@@ -150,6 +155,7 @@
         ).astype(BF16)
         at = slice(head * width, (head + 1) * width)
         o_ref[:, at] = dot(full, v[:, at])
+    fetch.wait()
 
 
 def pick_column(block, d, member):
@@ -202,9 +208,7 @@
             out[i, at, :] = (pre[i, at, :] + dec[i, at, :] * carry).astype(BF16)
 
 
-def mix_kernel(states, o_ref, qf, qb, gate, gain, proj_far, out, proj, sem):
-    fetch = pltpu.make_async_copy(proj_far, proj, sem)
-    fetch.start()
+def mix_kernel(states, o_ref, qf, qb, scale, proj, out):
     n, width = o_ref.shape[0], states.shape[2]
     members = states.shape[0]
     entering = [
@@ -226,9 +230,8 @@
                 own = jnp.where(keep, q[:, width:].astype(F32), 0.0).astype(BF16)
                 total = total + dot(own, entering[d][width:])
         total = total * lax.rsqrt(jnp.mean(total * total, axis=1, keepdims=True) + EPS)
-        total = total * gain[:, at] * jax.nn.silu(gate[:, at].astype(F32))
+        total = total * scale[:, at]
         mixed.append(total.astype(BF16))
-    fetch.wait()
     out[...] = dot(jnp.concatenate(mixed, axis=1), proj[...]).astype(BF16)
 
 
@@ -245,7 +248,9 @@
     return jnp.logical_and(first, placed), jnp.logical_and(second, placed)
 
 
-def route_kernel(routes, share, chosen_ref, hi_ref, lo_ref):
+def route_kernel(routes, share, skip, gain, chosen_ref, hi_ref, lo_ref, skip_ref, gain_ref):
+    skip_ref[...] = skip[...]
+    gain_ref[...] = gain[...]
     first, second = slot_matrix(routes[...])
     chosen_ref[...] = jnp.logical_or(first, second).astype(F32).astype(BF16)
     weight = jnp.where(first, share[0:1], 0.0) + jnp.where(second, share[1:2], 0.0)
@@ -398,22 +403,43 @@
     )(*distant(*decay_args))
     by_slice = lax.all_to_all(summary, ZG, 0, 0, tiled=True)
     slots = experts * CAP
-    chosen, share_hi, share_lo = pl.pallas_call(
+    chosen, share_hi, share_lo, skip, norm_gain = pl.pallas_call(
         route_kernel,
-        out_shape=[sds((slots, rows), BF16)] * 3,
+        out_shape=[near((slots, rows), BF16)] * 3
+        + [near((rows, model), BF16), near((1, model), F32)],
         compiler_params=params(),
         cost_estimate=cost(1 << 20),
-    )(*distant(assignments.T, assignment_share.T))
-    inside, q_fwd, q_bwd = pl.pallas_call(
+    )(
+        *distant(
+            assignments.T,
+            assignment_share.T,
+            skip_stream,
+            specialist_scale_vector.reshape(1, model),
+        )
+    )
+    inside, q_fwd, q_bwd, scale, projection = pl.pallas_call(
         local_kernel,
+        in_specs=[VMEM] * 10 + [pl.BlockSpec(memory_space=pl.ANY)],
         out_shape=[
             near((tokens, joint), F32),
             near((tokens, 2 * width), BF16),
             near((tokens, 2 * width), BF16),
+            near((tokens, joint), F32),
+            near(result_mapping_matrix.shape, BF16),
         ],
+        scratch_shapes=[pltpu.SemaphoreType.DMA],
         compiler_params=params(),
         cost_estimate=cost(64 << 20),
-    )(*distant(wide_probe_logits, narrow_probe_logits, *decay_args))
+    )(
+        *distant(
+            wide_probe_logits,
+            narrow_probe_logits,
+            *decay_args,
+            result_switch_logits,
+            channel_scale_vector.reshape(1, joint),
+            result_mapping_matrix,
+        )
+    )
     before, decayed, total = pl.pallas_call(
         group_kernel,
         in_specs=[SMEM, VMEM],
@@ -439,27 +465,17 @@
     entering = lax.all_to_all(carried, ZG, 0, 0, tiled=True)
     mixed = pl.pallas_call(
         mix_kernel,
-        in_specs=[VMEM] * 6 + [pl.BlockSpec(memory_space=pl.ANY)],
         out_shape=near((tokens, model), BF16),
-        scratch_shapes=[
-            pltpu.VMEM(result_mapping_matrix.shape, BF16),
-            pltpu.SemaphoreType.DMA,
-        ],
         compiler_params=params(),
         cost_estimate=cost(256 << 20),
-    )(
-        *nearby(entering, inside, q_fwd, q_bwd),
-        *distant(
-            result_switch_logits, channel_scale_vector.reshape(1, joint), result_mapping_matrix
-        ),
-    )
+    )(*nearby(entering, inside, q_fwd, q_bwd, scale, projection))
     parts = lax.all_to_all(mixed.reshape(shards, rows, model), "tp", 0, 0, tiled=True)
     hidden, outgoing = pl.pallas_call(
         dispatch_kernel,
-        out_shape=[sds((rows, model), BF16), near((experts, CAP, model), BF16)],
+        out_shape=[near((rows, model), BF16), near((experts, CAP, model), BF16)],
         compiler_params=params(),
         cost_estimate=cost(16 << 20),
-    )(*nearby(parts), *distant(skip_stream, specialist_scale_vector.reshape(1, model), chosen))
+    )(*nearby(parts, skip, norm_gain, chosen))
     own = lax.all_to_all(outgoing, SP, 0, 0, tiled=True)
 
     up_ring = [(i, (i + 1) % shards) for i in range(shards)]
@@ -524,7 +540,7 @@
         out_shape=sds((rows, model), BF16),
         compiler_params=params(),
         cost_estimate=cost(16 << 20),
-    )(*distant(hidden), *nearby(back), *distant(share_hi, share_lo))
+    )(*nearby(hidden, back, share_hi, share_lo))
 
 
 def solution(mesh):

time: 204 us -> 199 us (0.975)
  Pallas kernels: 26.1 us -> 23 us
  local copies, waits for them, and re-layouts: 3.71 us -> 1.26 us
    unnamed x8 -> x0, local copies, waits for them, and re-layouts: 2.47 us -> none
    pallas_call x4, Pallas kernels: 8.56 us -> 6.32 us  [the longest x1 3.18 us: local(): pl.pallas_call(local_kernel, in_specs=[VMEM] * 10 + [pl.BlockSpec(memory_...]
  transfers between devices with their start and end apart: 18 -> 18, of which waited for: 9 -> 9; matrix products, arithmetic and copies ran while one was open for 1% -> 1% of each run, Pallas kernels for 7% -> 8%
where the time goes in v3:
time: 199 us; the launch traced here: 198 us
  blocking collectives  83.3 us (42%)
  starting transfers between devices  57.4 us (29%)
  waiting for transfers between devices  33.3 us (17%)
  Pallas kernels  23 us (12%)
    all_to_all x1, blocking collectives, local(): own = lax.all_to_all(outgoing, SP, 0, 0, tiled=True)  43.1 us
    all_to_all x1, blocking collectives, local(): back = lax.all_to_all(summed, SP, 0, 0, tiled=True)  40.2 us
    all_to_all x1, starting transfers between devices, local(): by_slice = lax.all_to_all(summary, ZG, 0, 0, tiled=True)  23.7 us
    pallas_call x8, Pallas kernels, call(): pl.pallas_call(kernel, compiler_params=params(), cost_estimate=cost(flops...  11.1 us
    ppermute x6, starting transfers between devices, down(): return lax.ppermute(x, 'tp', down_ring)  10.6 us
    ppermute x6, waiting for transfers between devices, up(): return lax.ppermute(x, 'tp', up_ring)  10.6 us
    ppermute x3, starting transfers between devices, local(): lax.ppermute(total, 'zh', [(i, (i + k) % groups) for i in range(groups)])  9.61 us
    all_to_all x1, waiting for transfers between devices, local(): lax.all_to_all(mixed.reshape(shards, rows, model), 'tp', 0, 0, tiled=True)  6.94 us
  transfers between devices with their start and end apart: 18, of which 9 were waited for; matrix products, arithmetic and copies ran while one was open for 1% of the time, Pallas kernels for 8%

profile of v3, /device:TPU:33, one launch (start us, length us, event | category | flops | bytes accessed | tf_op | source)
XLA Modules:
  0.0 198.4 jit_solution(7396474826325302449)
XLA Ops:
  0.0 2.5 %shard_map.172 = bf16[8,80,128]{2,1,0:T(8,128)(2,1)} custom-call(bf16[128,128]{1,0:T(8,128)(2,1)} %wd.3, bf16[128,128]{1,0:T(8,128)(2,1)} %nd.3, f32[2,128]{1,0:T(2,128)} %wleak.3, f32[2,128]{1,0:T(2,128)} %nleak.3, bf16[128,384]{1,0:T(8,128)(2,1)} %v.3, f32[3,128]{1,0:T(4,128)} %bitcast.14), custom_call_target="tpu_custom_call" | custom-call | flops 4194304 | bytes 1048576 | tf_op jit(solution)/shard_map/pallas_call | solution.py:398
  2.5 23.7 %all-to-all-start = ((bf16[8,80,128]{2,1,0:T(8,128)(2,1)}), bf16[8,80,128]{2,1,0:T(8,128)(2,1)S(1)}, u32[]{:S(2)}, u32[]{:S(2)}) async-start(bf16[8,80,128]{2,1,0:T(8,128)(2,1)} %shard_map.172), calls=%async_computation | async-start | bytes 327680 | tf_op jit(solution)/shard_map/all_to_all | solution.py:404
  26.3 6.1 %all-to-all-done.got = bf16[8,80,128]{2,1,0:T(8,128)(2,1)S(1)} async-done(((bf16[8,80,128]{2,1,0:T(8,128)(2,1)}), bf16[8,80,128]{2,1,0:T(8,128)(2,1)S(1)}, u32[]{:S(2)}, u32[]{:S(2)}) %all-to-all-start) | async-done | bytes 163872 | tf_op jit(solution)/shard_map/all_to_all | solution.py:404
  33.1 4.4 %collective-permute-start.2 = (bf16[80,128]{1,0:T(8,128)(2,1)S(1)}, bf16[80,128]{1,0:T(8,128)(2,1)S(1)}, u32[]{:S(2)}, u32[]{:S(2)}) collective-permute-start(bf16[80,128]{1,0:T(8,128)(2,1)S(1)} %get-tuple-element.33), channel_id=1, source_target_pairs={{0,96},{32,0},{64,32},{96,64},{1,97},{33,1},{65,33},{97,65},{2,98}... | collective-permute-start | bytes 61448 | tf_op jit(solution)/shard_map/ppermute | solution.py:455
  37.5 5.2 %collective-permute-start = (bf16[80,128]{1,0:T(8,128)(2,1)S(1)}, bf16[80,128]{1,0:T(8,128)(2,1)S(1)}, u32[]{:S(2)}, u32[]{:S(2)}) collective-permute-start(bf16[80,128]{1,0:T(8,128)(2,1)S(1)} %get-tuple-element.33), channel_id=1, source_target_pairs={{0,32},{32,64},{64,96},{96,0},{1,33},{33,65},{65,97},{97,1},{2,34}... | collective-permute-start | bytes 61448 | tf_op jit(solution)/shard_map/ppermute | solution.py:455
  42.7 6.4 %collective-permute-done.1.r2 = bf16[80,128]{1,0:T(8,128)(2,1)S(1)} collective-permute-done((bf16[80,128]{1,0:T(8,128)(2,1)S(1)}, bf16[80,128]{1,0:T(8,128)(2,1)S(1)}, u32[]{:S(2)}, u32[]{:S(2)}) %collective-permute-start.1) | collective-permute-done | bytes 20512 | tf_op jit(solution)/shard_map/ppermute | solution.py:455
  49.1 1.3 shard_map.174
  50.4 5.6 %all-to-all-start.1 = ((bf16[8,64,128]{2,1,0:T(8,128)(2,1)}), bf16[8,64,128]{2,1,0:T(8,128)(2,1)S(1)}, u32[]{:S(2)}, u32[]{:S(2)}) async-start(bf16[8,64,128]{2,1,0:T(8,128)(2,1)} %shard_map.174), calls=%async_computation.1 | async-start | bytes 262144 | tf_op jit(solution)/shard_map/all_to_all | solution.py:465
  56.0 1.3 reshape.9.gain
  57.3 3.2 %shard_map.175 = (f32[128,384]{1,0:T(8,128)S(1)}, bf16[128,256]{1,0:T(8,128)(2,1)S(1)}, bf16[128,256]{1,0:T(8,128)(2,1)S(1)}, f32[128,384]{1,0:T(8,128)S(1)}, bf16[384,2048]{1,0:T(8,128)(2,1)S(1)}) custom-call(bf16[128,128]{1,0:T(8,128)(2,1)} %wp.1, bf16[128,128]{1,0:T(8,128)(2,1)} %np_.1, bf16[128,128]{1,0:T(8,128)(2,1)} %wd.3, bf16[128,128]{1,0:T(8,128)(2,1)} %nd.3, ...), custom_call_target="tpu_custom_call" | custom-call | flops 67108864 | bytes 1048576 | tf_op jit(solution)/shard_map/pallas_call | solution.py:420
  60.5 1.5 all-to-all-done.1.states
  61.9 1.5 shard_map.176
  63.4 4.3 %all-to-all-start.2 = ((bf16[4,32,2048]{2,1,0:T(8,128)(2,1)}), bf16[4,32,2048]{2,1,0:T(8,128)(2,1)S(1)}, u32[]{:S(2)}, u32[]{:S(2)}) async-start(bf16[4,32,2048]{2,1,0:T(8,128)(2,1)} %bitcast.3), calls=%async_computation.2 | async-start | bytes 1048576 | tf_op jit(solution)/shard_map/all_to_all | solution.py:472
  67.7 1.1 shard_map.177
  68.8 6.9 %all-to-all-done.2.parts = bf16[4,32,2048]{2,1,0:T(8,128)(2,1)S(1)} async-done(((bf16[4,32,2048]{2,1,0:T(8,128)(2,1)}), bf16[4,32,2048]{2,1,0:T(8,128)(2,1)S(1)}, u32[]{:S(2)}, u32[]{:S(2)}) %all-to-all-start.2) | async-done | bytes 524320 | tf_op jit(solution)/shard_map/all_to_all | solution.py:472
  76.3 43.1 %all_to_all.25.got = bf16[32,4,2048]{2,1,0:T(4,128)(2,1)S(1)} all-to-all(bf16[32,4,2048]{2,1,0:T(4,128)(2,1)S(1)} %get-tuple-element.45), channel_id=1, replica_groups=mesh['grp'=2,'zh'=4,'zl'=4,'c'=2,'tp'=4] {'zh','zl','c'}, dimensions={0} | all-to-all | bytes 1048576 | tf_op jit(solution)/shard_map/all_to_all | solution.py:479
  119.9 2.4 %collective-permute-start.7 = (bf16[64,2048]{1,0:T(8,128)(2,1)S(1)}, bf16[64,2048]{1,0:T(8,128)(2,1)S(1)}, u32[]{:S(2)}, u32[]{:S(2)}) collective-permute-start(bf16[64,2048]{1,0:T(8,128)(2,1)S(1)} %get-tuple-element.47.high), channel_id=1, source_target_pairs={{0,3},{1,0},{2,1},{3,2},{4,7},{5,4},{6,5},{7,6},{8,11},{9,8},{10,9... | collective-permute-start | bytes 786440 | tf_op jit(solution)/shard_map/ppermute | solution.py:488
  122.3 5.9 %collective-permute-done.5.x = bf16[64,2048]{1,0:T(8,128)(2,1)S(1)} collective-permute-done((bf16[64,2048]{1,0:T(8,128)(2,1)S(1)}, bf16[64,2048]{1,0:T(8,128)(2,1)S(1)}, u32[]{:S(2)}, u32[]{:S(2)}) %collective-permute-start.5) | collective-permute-done | bytes 262176 | tf_op jit(solution)/shard_map/ppermute | solution.py:485
  128.2 2.7 %collective-permute-start.8 = (bf16[64,2048]{1,0:T(8,128)(2,1)S(1)}, bf16[64,2048]{1,0:T(8,128)(2,1)S(1)}, u32[]{:S(2)}, u32[]{:S(2)}) collective-permute-start(bf16[64,2048]{1,0:T(8,128)(2,1)S(1)} %collective-permute-done.7.y), channel_id=1, source_target_pairs={{0,3},{1,0},{2,1},{3,2},{4,7},{5,4},{6,5},{7,6},{8,11},{9,8},{10,9... | collective-permute-start | bytes 786440 | tf_op jit(solution)/shard_map/ppermute | solution.py:488
  130.9 1.4 collective-permute-start.3
  132.3 5.0 %shard_map.180 = (bf16[64,2048]{1,0:T(8,128)(2,1)S(1)}, bf16[64,2048]{1,0:T(8,128)(2,1)S(1)}, bf16[2048,896]{1,0:T(8,128)(2,1)S(1)}, bf16[2048,896]{1,0:T(8,128)(2,1)S(1)}, bf16[896,2048]{1,0:T(8,128)(2,1)S(1)}) custom-call(bf16[64,2048]{1,0:T(8,128)(2,1)S(1)} %get-tuple-element.46.low, bf16[64,2048]{1,0:T(8,128)(2,1)S(1)} %get-tuple-element.47.high, ...), custom_call_target="tpu_custom_call" | custom-call | flops 2147483648 | bytes 1048576 | tf_op jit(solution)/shard_map/pallas_call | solution.py:495
  137.3 1.9 shard_map.182
  139.3 2.6 %collective-permute-start.12 = (bf16[64,2048]{1,0:T(8,128)(2,1)S(1)}, bf16[64,2048]{1,0:T(8,128)(2,1)S(1)}, u32[]{:S(2)}, u32[]{:S(2)}) collective-permute-start(bf16[64,2048]{1,0:T(8,128)(2,1)S(1)} %get-tuple-element.57), channel_id=1, source_target_pairs={{0,3},{1,0},{2,1},{3,2},{4,7},{5,4},{6,5},{7,6},{8,11},{9,8},{10,9... | collective-permute-start | bytes 786440 | tf_op jit(solution)/shard_map/ppermute | solution.py:488
  142.0 1.9 shard_map.184
  144.0 1.4 collective-permute-start.14
  145.4 1.9 shard_map.181
  147.6 2.8 %collective-permute-start.13 = (bf16[64,2048]{1,0:T(8,128)(2,1)S(1)}, bf16[64,2048]{1,0:T(8,128)(2,1)S(1)}, u32[]{:S(2)}, u32[]{:S(2)}) collective-permute-start(bf16[64,2048]{1,0:T(8,128)(2,1)S(1)} %shard_map.185), channel_id=1, source_target_pairs={{0,3},{1,0},{2,1},{3,2},{4,7},{5,4},{6,5},{7,6},{8,11},{9,8},{10,9... | collective-permute-start | bytes 786440 | tf_op jit(solution)/shard_map/ppermute | solution.py:488
  150.3 0.9 collective-permute-done.11.low_c
  151.6 4.3 %collective-permute-done.10.low_b = bf16[64,2048]{1,0:T(8,128)(2,1)S(1)} collective-permute-done((bf16[64,2048]{1,0:T(8,128)(2,1)S(1)}, bf16[64,2048]{1,0:T(8,128)(2,1)S(1)}, u32[]{:S(2)}, u32[]{:S(2)}) %collective-permute-start.10) | collective-permute-done | bytes 262176 | tf_op jit(solution)/shard_map/ppermute | solution.py:485
  155.9 0.9 collective-permute-done.13.high_b
  157.2 40.2 %all_to_all.26.back = bf16[32,4,2048]{2,1,0:T(4,128)(2,1)S(1)} all-to-all(bf16[32,4,2048]{2,1,0:T(4,128)(2,1)S(1)} %shard_map.186), channel_id=1, replica_groups=mesh['grp'=2,'zh'=4,'zl'=4,'c'=2,'tp'=4] {'zh','zl','c'}, dimensions={0} | all-to-all | bytes 1048576 | tf_op jit(solution)/shard_map/all_to_all | solution.py:537
  197.4 1.0 shard_map.187
  (24 shorter events, 3.1 us)
Async XLA Ops:
  2.5 29.9 %all-to-all-start = ((bf16[8,80,128]{2,1,0:T(8,128)(2,1)}), bf16[8,80,128]{2,1,0:T(8,128)(2,1)S(1)}, u32[]{:S(2)}, u32[]{:S(2)}) async-start(bf16[8,80,128]{2,1,0:T(8,128)(2,1)} %shard_map.172), calls=%async_computation | async-start | bytes 327680 | tf_op jit(solution)/shard_map/all_to_all | solution.py:404
  33.1 9.6 %collective-permute-start.2 = (bf16[80,128]{1,0:T(8,128)(2,1)S(1)}, bf16[80,128]{1,0:T(8,128)(2,1)S(1)}, u32[]{:S(2)}, u32[]{:S(2)}) collective-permute-start(bf16[80,128]{1,0:T(8,128)(2,1)S(1)} %get-tuple-element.33), channel_id=1, source_target_pairs={{0,96},{32,0},{64,32},{96,64},{1,97},{33,1},{65,33},{97,65},{2,98}... | collective-permute-start | bytes 61448 | tf_op jit(solution)/shard_map/ppermute | solution.py:455
  37.5 11.6 %collective-permute-start.1 = (bf16[80,128]{1,0:T(8,128)(2,1)S(1)}, bf16[80,128]{1,0:T(8,128)(2,1)S(1)}, u32[]{:S(2)}, u32[]{:S(2)}) collective-permute-start(bf16[80,128]{1,0:T(8,128)(2,1)S(1)} %get-tuple-element.33), channel_id=1, source_target_pairs={{0,64},{32,96},{64,0},{96,32},{1,65},{33,97},{65,1},{97,33},{2,66}... | collective-permute-start | bytes 61448 | tf_op jit(solution)/shard_map/ppermute | solution.py:455
  37.5 11.6 %collective-permute-start = (bf16[80,128]{1,0:T(8,128)(2,1)S(1)}, bf16[80,128]{1,0:T(8,128)(2,1)S(1)}, u32[]{:S(2)}, u32[]{:S(2)}) collective-permute-start(bf16[80,128]{1,0:T(8,128)(2,1)S(1)} %get-tuple-element.33), channel_id=1, source_target_pairs={{0,32},{32,64},{64,96},{96,0},{1,33},{33,65},{65,97},{97,1},{2,34}... | collective-permute-start | bytes 61448 | tf_op jit(solution)/shard_map/ppermute | solution.py:455
  50.4 11.5 %all-to-all-start.1 = ((bf16[8,64,128]{2,1,0:T(8,128)(2,1)}), bf16[8,64,128]{2,1,0:T(8,128)(2,1)S(1)}, u32[]{:S(2)}, u32[]{:S(2)}) async-start(bf16[8,64,128]{2,1,0:T(8,128)(2,1)} %shard_map.174), calls=%async_computation.1 | async-start | bytes 262144 | tf_op jit(solution)/shard_map/all_to_all | solution.py:465
  63.4 12.3 %all-to-all-start.2 = ((bf16[4,32,2048]{2,1,0:T(8,128)(2,1)}), bf16[4,32,2048]{2,1,0:T(8,128)(2,1)S(1)}, u32[]{:S(2)}, u32[]{:S(2)}) async-start(bf16[4,32,2048]{2,1,0:T(8,128)(2,1)} %bitcast.3), calls=%async_computation.2 | async-start | bytes 1048576 | tf_op jit(solution)/shard_map/all_to_all | solution.py:472
  119.5 8.7 %collective-permute-start.5 = (bf16[64,2048]{1,0:T(8,128)(2,1)S(1)}, bf16[64,2048]{1,0:T(8,128)(2,1)S(1)}, u32[]{:S(2)}, u32[]{:S(2)}) collective-permute-start(bf16[64,2048]{1,0:T(8,128)(2,1)S(1)} %get-tuple-element.46.low), channel_id=1, source_target_pairs={{0,1},{1,2},{2,3},{3,0},{4,5},{5,6},{6,7},{7,4},{8,9},{9,10},{10,1... | collective-permute-start | bytes 786440 | tf_op jit(solution)/shard_map/ppermute | solution.py:485
  119.9 8.3 %collective-permute-start.7 = (bf16[64,2048]{1,0:T(8,128)(2,1)S(1)}, bf16[64,2048]{1,0:T(8,128)(2,1)S(1)}, u32[]{:S(2)}, u32[]{:S(2)}) collective-permute-start(bf16[64,2048]{1,0:T(8,128)(2,1)S(1)} %get-tuple-element.47.high), channel_id=1, source_target_pairs={{0,3},{1,0},{2,1},{3,2},{4,7},{5,4},{6,5},{7,6},{8,11},{9,8},{10,9... | collective-permute-start | bytes 786440 | tf_op jit(solution)/shard_map/ppermute | solution.py:488
  128.2 9.1 %collective-permute-start.6 = (bf16[64,2048]{1,0:T(8,128)(2,1)S(1)}, bf16[64,2048]{1,0:T(8,128)(2,1)S(1)}, u32[]{:S(2)}, u32[]{:S(2)}) collective-permute-start(bf16[64,2048]{1,0:T(8,128)(2,1)S(1)} %collective-permute-done.5.x), channel_id=1, source_target_pairs={{0,1},{1,2},{2,3},{3,0},{4,5},{5,6},{6,7},{7,4},{8,9},{9,10},{10,1... | collective-permute-start | bytes 786440 | tf_op jit(solution)/shard_map/ppermute | solution.py:485
  128.2 9.1 %collective-permute-start.8 = (bf16[64,2048]{1,0:T(8,128)(2,1)S(1)}, bf16[64,2048]{1,0:T(8,128)(2,1)S(1)}, u32[]{:S(2)}, u32[]{:S(2)}) collective-permute-start(bf16[64,2048]{1,0:T(8,128)(2,1)S(1)} %collective-permute-done.7.y), channel_id=1, source_target_pairs={{0,3},{1,0},{2,1},{3,2},{4,7},{5,4},{6,5},{7,6},{8,11},{9,8},{10,9... | collective-permute-start | bytes 786440 | tf_op jit(solution)/shard_map/ppermute | solution.py:488
  130.8 13.1 %collective-permute-start.4 = (bf16[64,2048]{1,0:T(8,128)(2,1)S(1)}, bf16[64,2048]{1,0:T(8,128)(2,1)S(1)}, u32[]{:S(2)}, u32[]{:S(2)}) collective-permute-start(bf16[64,2048]{1,0:T(8,128)(2,1)S(1)} %get-tuple-element.46.low), channel_id=1, source_target_pairs={{0,3},{1,0},{2,1},{3,2},{4,7},{5,4},{6,5},{7,6},{8,11},{9,8},{10,9... | collective-permute-start | bytes 786440 | tf_op jit(solution)/shard_map/ppermute | solution.py:488
  130.9 14.5 %collective-permute-start.3 = (bf16[64,2048]{1,0:T(8,128)(2,1)S(1)}, bf16[64,2048]{1,0:T(8,128)(2,1)S(1)}, u32[]{:S(2)}, u32[]{:S(2)}) collective-permute-start(bf16[64,2048]{1,0:T(8,128)(2,1)S(1)} %get-tuple-element.47.high), channel_id=1, source_target_pairs={{0,1},{1,2},{2,3},{3,0},{4,5},{5,6},{6,7},{7,4},{8,9},{9,10},{10,1... | collective-permute-start | bytes 786440 | tf_op jit(solution)/shard_map/ppermute | solution.py:485
  139.2 8.1 %collective-permute-start.9 = (bf16[64,2048]{1,0:T(8,128)(2,1)S(1)}, bf16[64,2048]{1,0:T(8,128)(2,1)S(1)}, u32[]{:S(2)}, u32[]{:S(2)}) collective-permute-start(bf16[64,2048]{1,0:T(8,128)(2,1)S(1)} %get-tuple-element.53), channel_id=1, source_target_pairs={{0,1},{1,2},{2,3},{3,0},{4,5},{5,6},{6,7},{7,4},{8,9},{9,10},{10,1... | collective-permute-start | bytes 786440 | tf_op jit(solution)/shard_map/ppermute | solution.py:485
  139.3 8.2 %collective-permute-start.12 = (bf16[64,2048]{1,0:T(8,128)(2,1)S(1)}, bf16[64,2048]{1,0:T(8,128)(2,1)S(1)}, u32[]{:S(2)}, u32[]{:S(2)}) collective-permute-start(bf16[64,2048]{1,0:T(8,128)(2,1)S(1)} %get-tuple-element.57), channel_id=1, source_target_pairs={{0,3},{1,0},{2,1},{3,2},{4,7},{5,4},{6,5},{7,6},{8,11},{9,8},{10,9... | collective-permute-start | bytes 786440 | tf_op jit(solution)/shard_map/ppermute | solution.py:488
  143.8 7.4 %collective-permute-start.11 = (bf16[64,2048]{1,0:T(8,128)(2,1)S(1)}, bf16[64,2048]{1,0:T(8,128)(2,1)S(1)}, u32[]{:S(2)}, u32[]{:S(2)}) collective-permute-start(bf16[64,2048]{1,0:T(8,128)(2,1)S(1)} %get-tuple-element.54), channel_id=1, source_target_pairs={{0,3},{1,0},{2,1},{3,2},{4,7},{5,4},{6,5},{7,6},{8,11},{9,8},{10,9... | collective-permute-start | bytes 786440 | tf_op jit(solution)/shard_map/ppermute | solution.py:488
  144.0 7.6 %collective-permute-start.14 = (bf16[64,2048]{1,0:T(8,128)(2,1)S(1)}, bf16[64,2048]{1,0:T(8,128)(2,1)S(1)}, u32[]{:S(2)}, u32[]{:S(2)}) collective-permute-start(bf16[64,2048]{1,0:T(8,128)(2,1)S(1)} %get-tuple-element.58), channel_id=1, source_target_pairs={{0,1},{1,2},{2,3},{3,0},{4,5},{5,6},{6,7},{7,4},{8,9},{9,10},{10,1... | collective-permute-start | bytes 786440 | tf_op jit(solution)/shard_map/ppermute | solution.py:485
  147.4 8.6 %collective-permute-start.10 = (bf16[64,2048]{1,0:T(8,128)(2,1)S(1)}, bf16[64,2048]{1,0:T(8,128)(2,1)S(1)}, u32[]{:S(2)}, u32[]{:S(2)}) collective-permute-start(bf16[64,2048]{1,0:T(8,128)(2,1)S(1)} %shard_map.183), channel_id=1, source_target_pairs={{0,1},{1,2},{2,3},{3,0},{4,5},{5,6},{6,7},{7,4},{8,9},{9,10},{10,1... | collective-permute-start | bytes 786440 | tf_op jit(solution)/shard_map/ppermute | solution.py:485
  147.6 9.3 %collective-permute-start.13 = (bf16[64,2048]{1,0:T(8,128)(2,1)S(1)}, bf16[64,2048]{1,0:T(8,128)(2,1)S(1)}, u32[]{:S(2)}, u32[]{:S(2)}) collective-permute-start(bf16[64,2048]{1,0:T(8,128)(2,1)S(1)} %shard_map.185), channel_id=1, source_target_pairs={{0,3},{1,0},{2,1},{3,2},{4,7},{5,4},{6,5},{7,6},{8,11},{9,8},{10,9... | collective-permute-start | bytes 786440 | tf_op jit(solution)/shard_map/ppermute | solution.py:488

commit v4 on v3

--- a/solution.py
+++ b/solution.py
@@ -33,14 +33,17 @@
     return hi, (x - hi.astype(F32)).astype(BF16)
 
 
-def exact_sums(ones, x):
+def exact_sums(ones, x, side=1):
     hi, rest = x.astype(BF16), x
     parts = [hi]
     for _ in range(2):
         rest = rest - parts[-1].astype(F32)
         parts.append(rest.astype(BF16))
     bits = ones.astype(F32).astype(BF16)
-    return dot(jnp.concatenate([bits] * 3, axis=1), jnp.concatenate(parts, axis=0))
+    stacked = jnp.concatenate([p.astype(F32) for p in parts], axis=0).astype(BF16)
+    if side == 0:
+        return dot(stacked, jnp.concatenate([bits] * 3, axis=0), (0, 0))
+    return dot(jnp.concatenate([bits] * 3, axis=1), stacked)
 
 
 def key_and_decay(logits, leaks, spikes):
@@ -54,8 +57,7 @@
     heads = spk.shape[0]
     lane = iota((heads, 2 * width), 1)
     owner = jnp.where(lane < width, 0, jnp.where(lane < 3 * width // 2, 1, 2))
-    exact = lax.Precision.HIGHEST
-    spikes = dot(spk, (iota((heads, 2 * width), 0) == owner).astype(F32), (0, 0), exact)
+    spikes = exact_sums(iota((heads, 2 * width), 0) == owner, spk, 0)
     kw, aw = key_and_decay(wd, wleak, spikes[:, :width])
     kn, an = key_and_decay(nd, nleak, spikes[:, width:])
     row, col = iota((n, n), 0), iota((n, n), 1)
@@ -186,24 +188,25 @@
             column = pick_column(got[i, 2 * SLICE :, :], d, member)
             state = jnp.exp(column) * state + got[i, at, :].astype(F32)
             total = total + column
-        tot_ref[at, :] = state.astype(BF16)
+        for g in range(tot_ref.shape[0]):
+            tot_ref[g, at, :] = state.astype(BF16)
     rows = [summed[2 * n : 2 * n + 1] + summed[2 * n + 1 : 2 * n + 2] for n in range(4)]
-    tot_ref[2 * SLICE :, :] = decay_rows(rows)
-
-
-def carry_kernel(place, r1, r2, r3, pre, dec, out):
-    group, member, groups = place[0], place[1], place[2]
+    block = decay_rows(rows)
+    for g in range(tot_ref.shape[0]):
+        tot_ref[g, 2 * SLICE :, :] = block
+
+
+def carry_kernel(place, totals, pre, dec, out):
+    group, member = place[0], place[1]
     count, _, width = pre.shape
-    came = {1: r1, 2: r2, 3: r3}
+    groups = totals.shape[0]
     for d in range(2):
         at = slice(d * SLICE, (d + 1) * SLICE)
         carry = jnp.zeros((SLICE, width), F32)
-        for back in (3, 2, 1):
-            ref = came[back] if d == 0 else came[4 - back]
-            live = group - back >= 0 if d == 0 else group + back < groups
-            column = pick_column(ref[2 * SLICE :, :], d, member)
-            moved = jnp.exp(column) * carry + ref[at, :].astype(F32)
-            carry = jnp.where(live, moved, carry)
+        for g in range(groups) if d == 0 else reversed(range(groups)):
+            column = pick_column(totals[g, 2 * SLICE :, :], d, member)
+            moved = jnp.exp(column) * carry + totals[g, at, :].astype(F32)
+            carry = jnp.where(g < group if d == 0 else g > group, moved, carry)
         for i in range(count):
             out[i, at, :] = (pre[i, at, :] + dec[i, at, :] * carry).astype(BF16)
 
@@ -383,9 +386,7 @@
     groups = lax.axis_size("zh")
     shards = lax.axis_size("tp")
     experts = lax.axis_size(SP)
-    place = jnp.stack(
-        [lax.axis_index("zh"), lax.axis_index(ZG), jnp.int32(groups)]
-    ).astype(jnp.int32)
+    place = jnp.stack([lax.axis_index("zh"), lax.axis_index(ZG)]).astype(jnp.int32)
     decay_args = (
         wide_decay_logits,
         narrow_decay_logits,
@@ -403,6 +404,7 @@
     )(*distant(*decay_args))
     by_slice = lax.all_to_all(summary, ZG, 0, 0, tiled=True)
     slots = experts * CAP
+    head_gain = channel_scale_vector.reshape(1, joint)
     chosen, share_hi, share_lo, skip, norm_gain = pl.pallas_call(
         route_kernel,
         out_shape=[near((slots, rows), BF16)] * 3
@@ -436,7 +438,7 @@
             narrow_probe_logits,
             *decay_args,
             result_switch_logits,
-            channel_scale_vector.reshape(1, joint),
+            head_gain,
             result_mapping_matrix,
         )
     )
@@ -446,22 +448,19 @@
         out_shape=[
             near((members, 2 * SLICE, width), F32),
             near((members, 2 * SLICE, width), F32),
-            near((PAY, width), BF16),
+            near((groups, PAY, width), BF16),
         ],
         compiler_params=params(),
         cost_estimate=cost(4 << 20),
     )(place, *nearby(by_slice))
-    came = [
-        lax.ppermute(total, "zh", [(i, (i + k) % groups) for i in range(groups)])
-        for k in (1, 2, 3)
-    ]
+    came = lax.all_to_all(total, "zh", 0, 0, tiled=True)
     carried = pl.pallas_call(
         carry_kernel,
-        in_specs=[SMEM] + [VMEM] * 5,
+        in_specs=[SMEM] + [VMEM] * 3,
         out_shape=near((members, 2 * SLICE, width), BF16),
         compiler_params=params(),
         cost_estimate=cost(4 << 20),
-    )(place, *nearby(*came, before, decayed))
+    )(place, *nearby(came, before, decayed))
     entering = lax.all_to_all(carried, ZG, 0, 0, tiled=True)
     mixed = pl.pallas_call(
         mix_kernel,

time: 199 us -> 197 us (0.990)
  blocking collectives: 83.3 us -> 96.9 us
  starting transfers between devices: 57.4 us -> 48.1 us
  waiting for transfers between devices: 33.3 us -> 26.9 us
    all_to_all x0 -> x1, blocking collectives: none -> 17.5 us  [local(): came = lax.all_to_all(total, 'zh', 0, 0, tiled=True)]
    ppermute x3 -> x0, starting transfers between devices: 9.61 us -> none  [local(): lax.ppermute(total, 'zh', [(i, (i + k) % groups) for i in range(groups)])]
    ppermute x3 -> x0, waiting for transfers between devices: 6.39 us -> none  [local(): lax.ppermute(total, 'zh', [(i, (i + k) % groups) for i in range(groups)])]
    all_to_all x1, blocking collectives: 43.1 us -> 39.2 us  [local(): own = lax.all_to_all(outgoing, SP, 0, 0, tiled=True)]
  transfers between devices with their start and end apart: 18 -> 15, of which waited for: 9 -> 8; matrix products, arithmetic and copies ran while one was open for 1% -> 1% of each run, Pallas kernels for 8% -> 8%
where the time goes in v4:
time: 197 us; the launch traced here: 196 us
  blocking collectives  96.9 us (49%)
  starting transfers between devices  48.1 us (24%)
  waiting for transfers between devices  26.9 us (14%)
  Pallas kernels  22.7 us (12%)
    all_to_all x1, blocking collectives, local(): back = lax.all_to_all(summed, SP, 0, 0, tiled=True)  40.2 us
    all_to_all x1, blocking collectives, local(): own = lax.all_to_all(outgoing, SP, 0, 0, tiled=True)  39.2 us
    all_to_all x1, starting transfers between devices, local(): by_slice = lax.all_to_all(summary, ZG, 0, 0, tiled=True)  23.7 us
    all_to_all x1, blocking collectives, local(): came = lax.all_to_all(total, 'zh', 0, 0, tiled=True)  17.5 us
    pallas_call x8, Pallas kernels, call(): pl.pallas_call(kernel, compiler_params=params(), cost_estimate=cost(flops...  11.1 us
    ppermute x6, starting transfers between devices, down(): return lax.ppermute(x, 'tp', down_ring)  10.6 us
    ppermute x6, waiting for transfers between devices, up(): return lax.ppermute(x, 'tp', up_ring)  10.6 us
    all_to_all x1, waiting for transfers between devices, local(): lax.all_to_all(mixed.reshape(shards, rows, model), 'tp', 0, 0, tiled=True)  6.92 us
  transfers between devices with their start and end apart: 15, of which 8 were waited for; matrix products, arithmetic and copies ran while one was open for 1% of the time, Pallas kernels for 8%

profile of v4, /device:TPU:33, one launch (start us, length us, event | category | flops | bytes accessed | tf_op | source)
XLA Modules:
  0.0 196.0 jit_solution(8870165099836626442)
XLA Ops:
  0.0 2.3 %shard_map.172 = bf16[8,80,128]{2,1,0:T(8,128)(2,1)} custom-call(bf16[128,128]{1,0:T(8,128)(2,1)} %wd.3, bf16[128,128]{1,0:T(8,128)(2,1)} %nd.3, f32[2,128]{1,0:T(2,128)} %wleak.3, f32[2,128]{1,0:T(2,128)} %nleak.3, bf16[128,384]{1,0:T(8,128)(2,1)} %v.3, f32[3,128]{1,0:T(4,128)} %bitcast.14), custom_call_target="tpu_custom_call" | custom-call | flops 4194304 | bytes 1048576 | tf_op jit(solution)/shard_map/pallas_call | solution.py:399
  2.3 23.7 %all-to-all-start = ((bf16[8,80,128]{2,1,0:T(8,128)(2,1)}), bf16[8,80,128]{2,1,0:T(8,128)(2,1)S(1)}, u32[]{:S(2)}, u32[]{:S(2)}) async-start(bf16[8,80,128]{2,1,0:T(8,128)(2,1)} %shard_map.172), calls=%async_computation | async-start | bytes 327680 | tf_op jit(solution)/shard_map/all_to_all | solution.py:405
  26.1 6.1 %all-to-all-done.got = bf16[8,80,128]{2,1,0:T(8,128)(2,1)S(1)} async-done(((bf16[8,80,128]{2,1,0:T(8,128)(2,1)}), bf16[8,80,128]{2,1,0:T(8,128)(2,1)S(1)}, u32[]{:S(2)}, u32[]{:S(2)}) %all-to-all-start) | async-done | bytes 163872 | tf_op jit(solution)/shard_map/all_to_all | solution.py:405
  32.2 0.7 shard_map.173
  32.9 17.5 %all_to_all.30.totals = bf16[4,80,128]{2,1,0:T(8,128)(2,1)S(1)} all-to-all(bf16[4,80,128]{2,1,0:T(8,128)(2,1)S(1)} %get-tuple-element.33), channel_id=1, replica_groups=mesh['grp'=2,'zh'=4,'zl'=4,'c'=2,'tp'=4] {'zh'}, dimensions={0} | all-to-all | bytes 163840 | tf_op jit(solution)/shard_map/all_to_all | solution.py:456
  50.4 1.3 shard_map.174
  51.8 6.0 %all-to-all-start.2 = ((bf16[8,64,128]{2,1,0:T(8,128)(2,1)}), bf16[8,64,128]{2,1,0:T(8,128)(2,1)S(1)}, u32[]{:S(2)}, u32[]{:S(2)}) async-start(bf16[8,64,128]{2,1,0:T(8,128)(2,1)} %shard_map.174), calls=%async_computation.2 | async-start | bytes 262144 | tf_op jit(solution)/shard_map/all_to_all | solution.py:464
  57.7 1.3 reshape.9.gain
  59.0 3.1 %shard_map.175 = (f32[128,384]{1,0:T(8,128)S(1)}, bf16[128,256]{1,0:T(8,128)(2,1)S(1)}, bf16[128,256]{1,0:T(8,128)(2,1)S(1)}, f32[128,384]{1,0:T(8,128)S(1)}, bf16[384,2048]{1,0:T(8,128)(2,1)S(1)}) custom-call(bf16[128,128]{1,0:T(8,128)(2,1)} %wp.1, bf16[128,128]{1,0:T(8,128)(2,1)} %np_.1, bf16[128,128]{1,0:T(8,128)(2,1)} %wd.3, bf16[128,128]{1,0:T(8,128)(2,1)} %nd.3, ...), custom_call_target="tpu_custom_call" | custom-call | flops 67108864 | bytes 1048576 | tf_op jit(solution)/shard_map/pallas_call | solution.py:422
  62.0 1.5 all-to-all-done.2.states
  63.5 1.5 shard_map.176
  65.0 4.3 %all-to-all-start.3 = ((bf16[4,32,2048]{2,1,0:T(8,128)(2,1)}), bf16[4,32,2048]{2,1,0:T(8,128)(2,1)S(1)}, u32[]{:S(2)}, u32[]{:S(2)}) async-start(bf16[4,32,2048]{2,1,0:T(8,128)(2,1)} %bitcast.3), calls=%async_computation.3 | async-start | bytes 1048576 | tf_op jit(solution)/shard_map/all_to_all | solution.py:471
  69.3 1.1 shard_map.177
  70.4 6.9 %all-to-all-done.3.parts = bf16[4,32,2048]{2,1,0:T(8,128)(2,1)S(1)} async-done(((bf16[4,32,2048]{2,1,0:T(8,128)(2,1)}), bf16[4,32,2048]{2,1,0:T(8,128)(2,1)S(1)}, u32[]{:S(2)}, u32[]{:S(2)}) %all-to-all-start.3) | async-done | bytes 524320 | tf_op jit(solution)/shard_map/all_to_all | solution.py:471
  77.3 0.5 shard_map.178
  77.9 39.2 %all_to_all.31.got = bf16[32,4,2048]{2,1,0:T(4,128)(2,1)S(1)} all-to-all(bf16[32,4,2048]{2,1,0:T(4,128)(2,1)S(1)} %get-tuple-element.45), channel_id=1, replica_groups=mesh['grp'=2,'zh'=4,'zl'=4,'c'=2,'tp'=4] {'zh','zl','c'}, dimensions={0} | all-to-all | bytes 1048576 | tf_op jit(solution)/shard_map/all_to_all | solution.py:478
  117.5 2.4 %collective-permute-start.4 = (bf16[64,2048]{1,0:T(8,128)(2,1)S(1)}, bf16[64,2048]{1,0:T(8,128)(2,1)S(1)}, u32[]{:S(2)}, u32[]{:S(2)}) collective-permute-start(bf16[64,2048]{1,0:T(8,128)(2,1)S(1)} %get-tuple-element.47.high), channel_id=1, source_target_pairs={{0,3},{1,0},{2,1},{3,2},{4,7},{5,4},{6,5},{7,6},{8,11},{9,8},{10,9... | collective-permute-start | bytes 786440 | tf_op jit(solution)/shard_map/ppermute | solution.py:487
  119.9 5.9 %collective-permute-done.2.x = bf16[64,2048]{1,0:T(8,128)(2,1)S(1)} collective-permute-done((bf16[64,2048]{1,0:T(8,128)(2,1)S(1)}, bf16[64,2048]{1,0:T(8,128)(2,1)S(1)}, u32[]{:S(2)}, u32[]{:S(2)}) %collective-permute-start.2) | collective-permute-done | bytes 262176 | tf_op jit(solution)/shard_map/ppermute | solution.py:484
  125.8 2.7 %collective-permute-start.5 = (bf16[64,2048]{1,0:T(8,128)(2,1)S(1)}, bf16[64,2048]{1,0:T(8,128)(2,1)S(1)}, u32[]{:S(2)}, u32[]{:S(2)}) collective-permute-start(bf16[64,2048]{1,0:T(8,128)(2,1)S(1)} %collective-permute-done.4.y), channel_id=1, source_target_pairs={{0,3},{1,0},{2,1},{3,2},{4,7},{5,4},{6,5},{7,6},{8,11},{9,8},{10,9... | collective-permute-start | bytes 786440 | tf_op jit(solution)/shard_map/ppermute | solution.py:487
  128.5 1.4 collective-permute-start
  129.9 5.0 %shard_map.180 = (bf16[64,2048]{1,0:T(8,128)(2,1)S(1)}, bf16[64,2048]{1,0:T(8,128)(2,1)S(1)}, bf16[2048,896]{1,0:T(8,128)(2,1)S(1)}, bf16[2048,896]{1,0:T(8,128)(2,1)S(1)}, bf16[896,2048]{1,0:T(8,128)(2,1)S(1)}) custom-call(bf16[64,2048]{1,0:T(8,128)(2,1)S(1)} %get-tuple-element.46.low, bf16[64,2048]{1,0:T(8,128)(2,1)S(1)} %get-tuple-element.47.high, ...), custom_call_target="tpu_custom_call" | custom-call | flops 2147483648 | bytes 1048576 | tf_op jit(solution)/shard_map/pallas_call | solution.py:494
  134.9 1.9 shard_map.182
  136.9 2.6 %collective-permute-start.9 = (bf16[64,2048]{1,0:T(8,128)(2,1)S(1)}, bf16[64,2048]{1,0:T(8,128)(2,1)S(1)}, u32[]{:S(2)}, u32[]{:S(2)}) collective-permute-start(bf16[64,2048]{1,0:T(8,128)(2,1)S(1)} %get-tuple-element.57), channel_id=1, source_target_pairs={{0,3},{1,0},{2,1},{3,2},{4,7},{5,4},{6,5},{7,6},{8,11},{9,8},{10,9... | collective-permute-start | bytes 786440 | tf_op jit(solution)/shard_map/ppermute | solution.py:487
  139.6 1.9 shard_map.184
  141.6 1.4 collective-permute-start.11
  143.0 1.9 shard_map.181
  145.2 2.8 %collective-permute-start.10 = (bf16[64,2048]{1,0:T(8,128)(2,1)S(1)}, bf16[64,2048]{1,0:T(8,128)(2,1)S(1)}, u32[]{:S(2)}, u32[]{:S(2)}) collective-permute-start(bf16[64,2048]{1,0:T(8,128)(2,1)S(1)} %shard_map.185), channel_id=1, source_target_pairs={{0,3},{1,0},{2,1},{3,2},{4,7},{5,4},{6,5},{7,6},{8,11},{9,8},{10,9... | collective-permute-start | bytes 786440 | tf_op jit(solution)/shard_map/ppermute | solution.py:487
  148.0 0.9 collective-permute-done.8.low_c
  149.2 4.3 %collective-permute-done.7.low_b = bf16[64,2048]{1,0:T(8,128)(2,1)S(1)} collective-permute-done((bf16[64,2048]{1,0:T(8,128)(2,1)S(1)}, bf16[64,2048]{1,0:T(8,128)(2,1)S(1)}, u32[]{:S(2)}, u32[]{:S(2)}) %collective-permute-start.7) | collective-permute-done | bytes 262176 | tf_op jit(solution)/shard_map/ppermute | solution.py:484
  153.5 0.9 collective-permute-done.10.high_b
  154.8 40.2 %all_to_all.32.back = bf16[32,4,2048]{2,1,0:T(4,128)(2,1)S(1)} all-to-all(bf16[32,4,2048]{2,1,0:T(4,128)(2,1)S(1)} %shard_map.186), channel_id=1, replica_groups=mesh['grp'=2,'zh'=4,'zl'=4,'c'=2,'tp'=4] {'zh','zl','c'}, dimensions={0} | all-to-all | bytes 1048576 | tf_op jit(solution)/shard_map/all_to_all | solution.py:536
  195.0 1.0 shard_map.187
  (19 shorter events, 1.9 us)
Async XLA Ops:
  2.3 29.9 %all-to-all-start = ((bf16[8,80,128]{2,1,0:T(8,128)(2,1)}), bf16[8,80,128]{2,1,0:T(8,128)(2,1)S(1)}, u32[]{:S(2)}, u32[]{:S(2)}) async-start(bf16[8,80,128]{2,1,0:T(8,128)(2,1)} %shard_map.172), calls=%async_computation | async-start | bytes 327680 | tf_op jit(solution)/shard_map/all_to_all | solution.py:405
  51.8 11.7 %all-to-all-start.2 = ((bf16[8,64,128]{2,1,0:T(8,128)(2,1)}), bf16[8,64,128]{2,1,0:T(8,128)(2,1)S(1)}, u32[]{:S(2)}, u32[]{:S(2)}) async-start(bf16[8,64,128]{2,1,0:T(8,128)(2,1)} %shard_map.174), calls=%async_computation.2 | async-start | bytes 262144 | tf_op jit(solution)/shard_map/all_to_all | solution.py:464
  65.0 12.3 %all-to-all-start.3 = ((bf16[4,32,2048]{2,1,0:T(8,128)(2,1)}), bf16[4,32,2048]{2,1,0:T(8,128)(2,1)S(1)}, u32[]{:S(2)}, u32[]{:S(2)}) async-start(bf16[4,32,2048]{2,1,0:T(8,128)(2,1)} %bitcast.3), calls=%async_computation.3 | async-start | bytes 1048576 | tf_op jit(solution)/shard_map/all_to_all | solution.py:471
  117.1 8.7 %collective-permute-start.2 = (bf16[64,2048]{1,0:T(8,128)(2,1)S(1)}, bf16[64,2048]{1,0:T(8,128)(2,1)S(1)}, u32[]{:S(2)}, u32[]{:S(2)}) collective-permute-start(bf16[64,2048]{1,0:T(8,128)(2,1)S(1)} %get-tuple-element.46.low), channel_id=1, source_target_pairs={{0,1},{1,2},{2,3},{3,0},{4,5},{5,6},{6,7},{7,4},{8,9},{9,10},{10,1... | collective-permute-start | bytes 786440 | tf_op jit(solution)/shard_map/ppermute | solution.py:484
  117.5 8.3 %collective-permute-start.4 = (bf16[64,2048]{1,0:T(8,128)(2,1)S(1)}, bf16[64,2048]{1,0:T(8,128)(2,1)S(1)}, u32[]{:S(2)}, u32[]{:S(2)}) collective-permute-start(bf16[64,2048]{1,0:T(8,128)(2,1)S(1)} %get-tuple-element.47.high), channel_id=1, source_target_pairs={{0,3},{1,0},{2,1},{3,2},{4,7},{5,4},{6,5},{7,6},{8,11},{9,8},{10,9... | collective-permute-start | bytes 786440 | tf_op jit(solution)/shard_map/ppermute | solution.py:487
  125.8 9.1 %collective-permute-start.3 = (bf16[64,2048]{1,0:T(8,128)(2,1)S(1)}, bf16[64,2048]{1,0:T(8,128)(2,1)S(1)}, u32[]{:S(2)}, u32[]{:S(2)}) collective-permute-start(bf16[64,2048]{1,0:T(8,128)(2,1)S(1)} %collective-permute-done.2.x), channel_id=1, source_target_pairs={{0,1},{1,2},{2,3},{3,0},{4,5},{5,6},{6,7},{7,4},{8,9},{9,10},{10,1... | collective-permute-start | bytes 786440 | tf_op jit(solution)/shard_map/ppermute | solution.py:484
  125.8 9.1 %collective-permute-start.5 = (bf16[64,2048]{1,0:T(8,128)(2,1)S(1)}, bf16[64,2048]{1,0:T(8,128)(2,1)S(1)}, u32[]{:S(2)}, u32[]{:S(2)}) collective-permute-start(bf16[64,2048]{1,0:T(8,128)(2,1)S(1)} %collective-permute-done.4.y), channel_id=1, source_target_pairs={{0,3},{1,0},{2,1},{3,2},{4,7},{5,4},{6,5},{7,6},{8,11},{9,8},{10,9... | collective-permute-start | bytes 786440 | tf_op jit(solution)/shard_map/ppermute | solution.py:487
  128.5 13.1 %collective-permute-start.1 = (bf16[64,2048]{1,0:T(8,128)(2,1)S(1)}, bf16[64,2048]{1,0:T(8,128)(2,1)S(1)}, u32[]{:S(2)}, u32[]{:S(2)}) collective-permute-start(bf16[64,2048]{1,0:T(8,128)(2,1)S(1)} %get-tuple-element.46.low), channel_id=1, source_target_pairs={{0,3},{1,0},{2,1},{3,2},{4,7},{5,4},{6,5},{7,6},{8,11},{9,8},{10,9... | collective-permute-start | bytes 786440 | tf_op jit(solution)/shard_map/ppermute | solution.py:487
  128.5 14.5 %collective-permute-start = (bf16[64,2048]{1,0:T(8,128)(2,1)S(1)}, bf16[64,2048]{1,0:T(8,128)(2,1)S(1)}, u32[]{:S(2)}, u32[]{:S(2)}) collective-permute-start(bf16[64,2048]{1,0:T(8,128)(2,1)S(1)} %get-tuple-element.47.high), channel_id=1, source_target_pairs={{0,1},{1,2},{2,3},{3,0},{4,5},{5,6},{6,7},{7,4},{8,9},{9,10},{10,1... | collective-permute-start | bytes 786440 | tf_op jit(solution)/shard_map/ppermute | solution.py:484
  136.8 8.1 %collective-permute-start.6 = (bf16[64,2048]{1,0:T(8,128)(2,1)S(1)}, bf16[64,2048]{1,0:T(8,128)(2,1)S(1)}, u32[]{:S(2)}, u32[]{:S(2)}) collective-permute-start(bf16[64,2048]{1,0:T(8,128)(2,1)S(1)} %get-tuple-element.53), channel_id=1, source_target_pairs={{0,1},{1,2},{2,3},{3,0},{4,5},{5,6},{6,7},{7,4},{8,9},{9,10},{10,1... | collective-permute-start | bytes 786440 | tf_op jit(solution)/shard_map/ppermute | solution.py:484
  136.9 8.2 %collective-permute-start.9 = (bf16[64,2048]{1,0:T(8,128)(2,1)S(1)}, bf16[64,2048]{1,0:T(8,128)(2,1)S(1)}, u32[]{:S(2)}, u32[]{:S(2)}) collective-permute-start(bf16[64,2048]{1,0:T(8,128)(2,1)S(1)} %get-tuple-element.57), channel_id=1, source_target_pairs={{0,3},{1,0},{2,1},{3,2},{4,7},{5,4},{6,5},{7,6},{8,11},{9,8},{10,9... | collective-permute-start | bytes 786440 | tf_op jit(solution)/shard_map/ppermute | solution.py:487
  141.4 7.4 %collective-permute-start.8 = (bf16[64,2048]{1,0:T(8,128)(2,1)S(1)}, bf16[64,2048]{1,0:T(8,128)(2,1)S(1)}, u32[]{:S(2)}, u32[]{:S(2)}) collective-permute-start(bf16[64,2048]{1,0:T(8,128)(2,1)S(1)} %get-tuple-element.54), channel_id=1, source_target_pairs={{0,3},{1,0},{2,1},{3,2},{4,7},{5,4},{6,5},{7,6},{8,11},{9,8},{10,9... | collective-permute-start | bytes 786440 | tf_op jit(solution)/shard_map/ppermute | solution.py:487
  141.6 7.6 %collective-permute-start.11 = (bf16[64,2048]{1,0:T(8,128)(2,1)S(1)}, bf16[64,2048]{1,0:T(8,128)(2,1)S(1)}, u32[]{:S(2)}, u32[]{:S(2)}) collective-permute-start(bf16[64,2048]{1,0:T(8,128)(2,1)S(1)} %get-tuple-element.58), channel_id=1, source_target_pairs={{0,1},{1,2},{2,3},{3,0},{4,5},{5,6},{6,7},{7,4},{8,9},{9,10},{10,1... | collective-permute-start | bytes 786440 | tf_op jit(solution)/shard_map/ppermute | solution.py:484
  145.0 8.5 %collective-permute-start.7 = (bf16[64,2048]{1,0:T(8,128)(2,1)S(1)}, bf16[64,2048]{1,0:T(8,128)(2,1)S(1)}, u32[]{:S(2)}, u32[]{:S(2)}) collective-permute-start(bf16[64,2048]{1,0:T(8,128)(2,1)S(1)} %shard_map.183), channel_id=1, source_target_pairs={{0,1},{1,2},{2,3},{3,0},{4,5},{5,6},{6,7},{7,4},{8,9},{9,10},{10,1... | collective-permute-start | bytes 786440 | tf_op jit(solution)/shard_map/ppermute | solution.py:484
  145.2 9.2 %collective-permute-start.10 = (bf16[64,2048]{1,0:T(8,128)(2,1)S(1)}, bf16[64,2048]{1,0:T(8,128)(2,1)S(1)}, u32[]{:S(2)}, u32[]{:S(2)}) collective-permute-start(bf16[64,2048]{1,0:T(8,128)(2,1)S(1)} %shard_map.185), channel_id=1, source_target_pairs={{0,3},{1,0},{2,1},{3,2},{4,7},{5,4},{6,5},{7,6},{8,11},{9,8},{10,9... | collective-permute-start | bytes 786440 | tf_op jit(solution)/shard_map/ppermute | solution.py:487

commit v5 on v4

--- a/solution.py
+++ b/solution.py
@@ -172,8 +172,8 @@
     return jnp.sum(jnp.where(hit, row, 0.0), axis=1, keepdims=True)
 
 
-def group_kernel(place, got, pre_ref, dec_ref, tot_ref):
-    member = place[1]
+def group_kernel(got, pre_ref, dec_ref, tot_ref):
+    member = lax.axis_index(ZG)
     count, _, width = got.shape
     summed = jnp.zeros((16, width), F32)
     for i in range(count):
@@ -196,8 +196,8 @@
         tot_ref[g, 2 * SLICE :, :] = block
 
 
-def carry_kernel(place, totals, pre, dec, out):
-    group, member = place[0], place[1]
+def carry_kernel(totals, pre, dec, out):
+    group, member = lax.axis_index("zh"), lax.axis_index(ZG)
     count, _, width = pre.shape
     groups = totals.shape[0]
     for d in range(2):
@@ -352,7 +352,6 @@
 
 
 VMEM = pl.BlockSpec(memory_space=pltpu.VMEM)
-SMEM = pl.BlockSpec(memory_space=pltpu.SMEM)
 
 
 def cost(flops):
@@ -386,7 +385,6 @@
     groups = lax.axis_size("zh")
     shards = lax.axis_size("tp")
     experts = lax.axis_size(SP)
-    place = jnp.stack([lax.axis_index("zh"), lax.axis_index(ZG)]).astype(jnp.int32)
     decay_args = (
         wide_decay_logits,
         narrow_decay_logits,
@@ -444,7 +442,6 @@
     )
     before, decayed, total = pl.pallas_call(
         group_kernel,
-        in_specs=[SMEM, VMEM],
         out_shape=[
             near((members, 2 * SLICE, width), F32),
             near((members, 2 * SLICE, width), F32),
@@ -452,15 +449,14 @@
         ],
         compiler_params=params(),
         cost_estimate=cost(4 << 20),
-    )(place, *nearby(by_slice))
+    )(*nearby(by_slice))
     came = lax.all_to_all(total, "zh", 0, 0, tiled=True)
     carried = pl.pallas_call(
         carry_kernel,
-        in_specs=[SMEM] + [VMEM] * 3,
         out_shape=near((members, 2 * SLICE, width), BF16),
         compiler_params=params(),
         cost_estimate=cost(4 << 20),
-    )(place, *nearby(came, before, decayed))
+    )(*nearby(came, before, decayed))
     entering = lax.all_to_all(carried, ZG, 0, 0, tiled=True)
     mixed = pl.pallas_call(
         mix_kernel,

time: 197 us -> 195 us (0.990)
  blocking collectives: 96.9 us -> 127 us
  starting transfers between devices: 48.1 us -> 24.4 us
  waiting for transfers between devices: 26.9 us -> 20.8 us
    all_to_all x0 -> x1, blocking collectives: none -> 28.9 us  [local(): by_slice = lax.all_to_all(summary, ZG, 0, 0, tiled=True)]
    all_to_all x1 -> x0, starting transfers between devices: 23.7 us -> none  [local(): by_slice = lax.all_to_all(summary, ZG, 0, 0, tiled=True)]
    all_to_all x1 -> x0, waiting for transfers between devices: 6.07 us -> none  [local(): by_slice = lax.all_to_all(summary, ZG, 0, 0, tiled=True)]
  transfers between devices with their start and end apart: 15 -> 14, of which waited for: 8 -> 7; matrix products, arithmetic and copies ran while one was open for 1% -> 1% of each run, Pallas kernels for 8% -> 8%
where the time goes in v5:
time: 195 us; the launch traced here: 194 us
  blocking collectives  127 us (65%)
  starting transfers between devices  24.4 us (13%)
  Pallas kernels  21 us (11%)
  waiting for transfers between devices  20.8 us (11%)
    all_to_all x1, blocking collectives, local(): back = lax.all_to_all(summed, SP, 0, 0, tiled=True)  40.2 us
    all_to_all x1, blocking collectives, local(): own = lax.all_to_all(outgoing, SP, 0, 0, tiled=True)  39.2 us
    all_to_all x1, blocking collectives, local(): by_slice = lax.all_to_all(summary, ZG, 0, 0, tiled=True)  28.9 us
    all_to_all x1, blocking collectives, local(): came = lax.all_to_all(total, 'zh', 0, 0, tiled=True)  18.2 us
    pallas_call x8, Pallas kernels, call(): pl.pallas_call(kernel, compiler_params=params(), cost_estimate=cost(flops...  11.1 us
    ppermute x6, starting transfers between devices, down(): return lax.ppermute(x, 'tp', down_ring)  10.6 us
    ppermute x6, waiting for transfers between devices, up(): return lax.ppermute(x, 'tp', up_ring)  10.6 us
    all_to_all x1, waiting for transfers between devices, local(): lax.all_to_all(mixed.reshape(shards, rows, model), 'tp', 0, 0, tiled=True)  6.91 us
  transfers between devices with their start and end apart: 14, of which 7 were waited for; matrix products, arithmetic and copies ran while one was open for 1% of the time, Pallas kernels for 8%

profile of v5, /device:TPU:33, one launch (start us, length us, event | category | flops | bytes accessed | tf_op | source)
XLA Modules:
  0.0 194.1 jit_solution(8639730748115989071)
XLA Ops:
  0.0 1.7 shard_map.172
  1.7 28.9 %all_to_all.30.got = bf16[8,80,128]{2,1,0:T(8,128)(2,1)S(1)} all-to-all(bf16[8,80,128]{2,1,0:T(8,128)(2,1)S(1)} %shard_map.172), channel_id=1, replica_groups=mesh['grp'=2,'zh'=4,'zl'=4,'c'=2,'tp'=4] {'zl','c'}, dimensions={0} | all-to-all | bytes 327680 | tf_op jit(solution)/shard_map/all_to_all | solution.py:403
  30.8 18.2 %all_to_all.31.totals = bf16[4,80,128]{2,1,0:T(8,128)(2,1)S(1)} all-to-all(bf16[4,80,128]{2,1,0:T(8,128)(2,1)S(1)} %get-tuple-element.33), channel_id=1, replica_groups=mesh['grp'=2,'zh'=4,'zl'=4,'c'=2,'tp'=4] {'zh'}, dimensions={0} | all-to-all | bytes 163840 | tf_op jit(solution)/shard_map/all_to_all | solution.py:453
  49.0 0.8 shard_map.174
  49.8 6.0 %all-to-all-start.2 = ((bf16[8,64,128]{2,1,0:T(8,128)(2,1)}), bf16[8,64,128]{2,1,0:T(8,128)(2,1)S(1)}, u32[]{:S(2)}, u32[]{:S(2)}) async-start(bf16[8,64,128]{2,1,0:T(8,128)(2,1)} %shard_map.174), calls=%async_computation.2 | async-start | bytes 262144 | tf_op jit(solution)/shard_map/all_to_all | solution.py:460
  55.8 1.2 reshape.9.gain
  57.0 3.1 %shard_map.175 = (f32[128,384]{1,0:T(8,128)S(1)}, bf16[128,256]{1,0:T(8,128)(2,1)S(1)}, bf16[128,256]{1,0:T(8,128)(2,1)S(1)}, f32[128,384]{1,0:T(8,128)S(1)}, bf16[384,2048]{1,0:T(8,128)(2,1)S(1)}) custom-call(bf16[128,128]{1,0:T(8,128)(2,1)} %wp.1, bf16[128,128]{1,0:T(8,128)(2,1)} %np_.1, bf16[128,128]{1,0:T(8,128)(2,1)} %wd.3, bf16[128,128]{1,0:T(8,128)(2,1)} %nd.3, ...), custom_call_target="tpu_custom_call" | custom-call | flops 67108864 | bytes 1048576 | tf_op jit(solution)/shard_map/pallas_call | solution.py:420
  60.1 1.5 all-to-all-done.2.states
  61.5 1.5 shard_map.176
  63.1 4.3 %all-to-all-start.3 = ((bf16[4,32,2048]{2,1,0:T(8,128)(2,1)}), bf16[4,32,2048]{2,1,0:T(8,128)(2,1)S(1)}, u32[]{:S(2)}, u32[]{:S(2)}) async-start(bf16[4,32,2048]{2,1,0:T(8,128)(2,1)} %bitcast.1), calls=%async_computation.3 | async-start | bytes 1048576 | tf_op jit(solution)/shard_map/all_to_all | solution.py:467
  67.3 1.1 shard_map.177
  68.4 6.9 %all-to-all-done.3.parts = bf16[4,32,2048]{2,1,0:T(8,128)(2,1)S(1)} async-done(((bf16[4,32,2048]{2,1,0:T(8,128)(2,1)}), bf16[4,32,2048]{2,1,0:T(8,128)(2,1)S(1)}, u32[]{:S(2)}, u32[]{:S(2)}) %all-to-all-start.3) | async-done | bytes 524320 | tf_op jit(solution)/shard_map/all_to_all | solution.py:467
  75.4 0.5 shard_map.178
  75.9 39.2 %all_to_all.32.got = bf16[32,4,2048]{2,1,0:T(4,128)(2,1)S(1)} all-to-all(bf16[32,4,2048]{2,1,0:T(4,128)(2,1)S(1)} %get-tuple-element.45), channel_id=1, replica_groups=mesh['grp'=2,'zh'=4,'zl'=4,'c'=2,'tp'=4] {'zh','zl','c'}, dimensions={0} | all-to-all | bytes 1048576 | tf_op jit(solution)/shard_map/all_to_all | solution.py:474
  115.1 0.4 collective-permute-start.2
  115.5 2.4 %collective-permute-start.4 = (bf16[64,2048]{1,0:T(8,128)(2,1)S(1)}, bf16[64,2048]{1,0:T(8,128)(2,1)S(1)}, u32[]{:S(2)}, u32[]{:S(2)}) collective-permute-start(bf16[64,2048]{1,0:T(8,128)(2,1)S(1)} %get-tuple-element.47.high), channel_id=1, source_target_pairs={{0,3},{1,0},{2,1},{3,2},{4,7},{5,4},{6,5},{7,6},{8,11},{9,8},{10,9... | collective-permute-start | bytes 786440 | tf_op jit(solution)/shard_map/ppermute | solution.py:483
  117.9 5.9 %collective-permute-done.2.x = bf16[64,2048]{1,0:T(8,128)(2,1)S(1)} collective-permute-done((bf16[64,2048]{1,0:T(8,128)(2,1)S(1)}, bf16[64,2048]{1,0:T(8,128)(2,1)S(1)}, u32[]{:S(2)}, u32[]{:S(2)}) %collective-permute-start.2) | collective-permute-done | bytes 262176 | tf_op jit(solution)/shard_map/ppermute | solution.py:480
  123.8 2.7 %collective-permute-start.5 = (bf16[64,2048]{1,0:T(8,128)(2,1)S(1)}, bf16[64,2048]{1,0:T(8,128)(2,1)S(1)}, u32[]{:S(2)}, u32[]{:S(2)}) collective-permute-start(bf16[64,2048]{1,0:T(8,128)(2,1)S(1)} %collective-permute-done.4.y), channel_id=1, source_target_pairs={{0,3},{1,0},{2,1},{3,2},{4,7},{5,4},{6,5},{7,6},{8,11},{9,8},{10,9... | collective-permute-start | bytes 786440 | tf_op jit(solution)/shard_map/ppermute | solution.py:483
  126.5 1.4 collective-permute-start
  128.0 5.0 %shard_map.180 = (bf16[64,2048]{1,0:T(8,128)(2,1)S(1)}, bf16[64,2048]{1,0:T(8,128)(2,1)S(1)}, bf16[2048,896]{1,0:T(8,128)(2,1)S(1)}, bf16[2048,896]{1,0:T(8,128)(2,1)S(1)}, bf16[896,2048]{1,0:T(8,128)(2,1)S(1)}) custom-call(bf16[64,2048]{1,0:T(8,128)(2,1)S(1)} %get-tuple-element.46.low, bf16[64,2048]{1,0:T(8,128)(2,1)S(1)} %get-tuple-element.47.high, ...), custom_call_target="tpu_custom_call" | custom-call | flops 2147483648 | bytes 1048576 | tf_op jit(solution)/shard_map/pallas_call | solution.py:490
  133.0 1.9 shard_map.182
  135.0 2.6 %collective-permute-start.9 = (bf16[64,2048]{1,0:T(8,128)(2,1)S(1)}, bf16[64,2048]{1,0:T(8,128)(2,1)S(1)}, u32[]{:S(2)}, u32[]{:S(2)}) collective-permute-start(bf16[64,2048]{1,0:T(8,128)(2,1)S(1)} %get-tuple-element.57), channel_id=1, source_target_pairs={{0,3},{1,0},{2,1},{3,2},{4,7},{5,4},{6,5},{7,6},{8,11},{9,8},{10,9... | collective-permute-start | bytes 786440 | tf_op jit(solution)/shard_map/ppermute | solution.py:483
  137.6 1.9 shard_map.184
  139.7 1.4 collective-permute-start.11
  141.1 1.9 shard_map.181
  143.3 2.8 %collective-permute-start.10 = (bf16[64,2048]{1,0:T(8,128)(2,1)S(1)}, bf16[64,2048]{1,0:T(8,128)(2,1)S(1)}, u32[]{:S(2)}, u32[]{:S(2)}) collective-permute-start(bf16[64,2048]{1,0:T(8,128)(2,1)S(1)} %shard_map.185), channel_id=1, source_target_pairs={{0,3},{1,0},{2,1},{3,2},{4,7},{5,4},{6,5},{7,6},{8,11},{9,8},{10,9... | collective-permute-start | bytes 786440 | tf_op jit(solution)/shard_map/ppermute | solution.py:483
  146.0 0.9 collective-permute-done.8.low_c
  146.9 0.4 collective-permute-done.11.high_c
  147.3 4.3 %collective-permute-done.7.low_b = bf16[64,2048]{1,0:T(8,128)(2,1)S(1)} collective-permute-done((bf16[64,2048]{1,0:T(8,128)(2,1)S(1)}, bf16[64,2048]{1,0:T(8,128)(2,1)S(1)}, u32[]{:S(2)}, u32[]{:S(2)}) %collective-permute-start.7) | collective-permute-done | bytes 262176 | tf_op jit(solution)/shard_map/ppermute | solution.py:480
  151.6 0.9 collective-permute-done.10.high_b
  152.9 40.2 %all_to_all.33.back = bf16[32,4,2048]{2,1,0:T(4,128)(2,1)S(1)} all-to-all(bf16[32,4,2048]{2,1,0:T(4,128)(2,1)S(1)} %shard_map.186), channel_id=1, replica_groups=mesh['grp'=2,'zh'=4,'zl'=4,'c'=2,'tp'=4] {'zh','zl','c'}, dimensions={0} | all-to-all | bytes 1048576 | tf_op jit(solution)/shard_map/all_to_all | solution.py:532
  193.1 1.0 shard_map.187
  (17 shorter events, 1.2 us)
Async XLA Ops:
  49.8 11.7 %all-to-all-start.2 = ((bf16[8,64,128]{2,1,0:T(8,128)(2,1)}), bf16[8,64,128]{2,1,0:T(8,128)(2,1)S(1)}, u32[]{:S(2)}, u32[]{:S(2)}) async-start(bf16[8,64,128]{2,1,0:T(8,128)(2,1)} %shard_map.174), calls=%async_computation.2 | async-start | bytes 262144 | tf_op jit(solution)/shard_map/all_to_all | solution.py:460
  63.1 12.3 %all-to-all-start.3 = ((bf16[4,32,2048]{2,1,0:T(8,128)(2,1)}), bf16[4,32,2048]{2,1,0:T(8,128)(2,1)S(1)}, u32[]{:S(2)}, u32[]{:S(2)}) async-start(bf16[4,32,2048]{2,1,0:T(8,128)(2,1)} %bitcast.1), calls=%async_computation.3 | async-start | bytes 1048576 | tf_op jit(solution)/shard_map/all_to_all | solution.py:467
  115.1 8.7 %collective-permute-start.2 = (bf16[64,2048]{1,0:T(8,128)(2,1)S(1)}, bf16[64,2048]{1,0:T(8,128)(2,1)S(1)}, u32[]{:S(2)}, u32[]{:S(2)}) collective-permute-start(bf16[64,2048]{1,0:T(8,128)(2,1)S(1)} %get-tuple-element.46.low), channel_id=1, source_target_pairs={{0,1},{1,2},{2,3},{3,0},{4,5},{5,6},{6,7},{7,4},{8,9},{9,10},{10,1... | collective-permute-start | bytes 786440 | tf_op jit(solution)/shard_map/ppermute | solution.py:480
  115.5 8.3 %collective-permute-start.4 = (bf16[64,2048]{1,0:T(8,128)(2,1)S(1)}, bf16[64,2048]{1,0:T(8,128)(2,1)S(1)}, u32[]{:S(2)}, u32[]{:S(2)}) collective-permute-start(bf16[64,2048]{1,0:T(8,128)(2,1)S(1)} %get-tuple-element.47.high), channel_id=1, source_target_pairs={{0,3},{1,0},{2,1},{3,2},{4,7},{5,4},{6,5},{7,6},{8,11},{9,8},{10,9... | collective-permute-start | bytes 786440 | tf_op jit(solution)/shard_map/ppermute | solution.py:483
  123.8 9.1 %collective-permute-start.3 = (bf16[64,2048]{1,0:T(8,128)(2,1)S(1)}, bf16[64,2048]{1,0:T(8,128)(2,1)S(1)}, u32[]{:S(2)}, u32[]{:S(2)}) collective-permute-start(bf16[64,2048]{1,0:T(8,128)(2,1)S(1)} %collective-permute-done.2.x), channel_id=1, source_target_pairs={{0,1},{1,2},{2,3},{3,0},{4,5},{5,6},{6,7},{7,4},{8,9},{9,10},{10,1... | collective-permute-start | bytes 786440 | tf_op jit(solution)/shard_map/ppermute | solution.py:480
  123.8 9.1 %collective-permute-start.5 = (bf16[64,2048]{1,0:T(8,128)(2,1)S(1)}, bf16[64,2048]{1,0:T(8,128)(2,1)S(1)}, u32[]{:S(2)}, u32[]{:S(2)}) collective-permute-start(bf16[64,2048]{1,0:T(8,128)(2,1)S(1)} %collective-permute-done.4.y), channel_id=1, source_target_pairs={{0,3},{1,0},{2,1},{3,2},{4,7},{5,4},{6,5},{7,6},{8,11},{9,8},{10,9... | collective-permute-start | bytes 786440 | tf_op jit(solution)/shard_map/ppermute | solution.py:483
  126.5 13.1 %collective-permute-start.1 = (bf16[64,2048]{1,0:T(8,128)(2,1)S(1)}, bf16[64,2048]{1,0:T(8,128)(2,1)S(1)}, u32[]{:S(2)}, u32[]{:S(2)}) collective-permute-start(bf16[64,2048]{1,0:T(8,128)(2,1)S(1)} %get-tuple-element.46.low), channel_id=1, source_target_pairs={{0,3},{1,0},{2,1},{3,2},{4,7},{5,4},{6,5},{7,6},{8,11},{9,8},{10,9... | collective-permute-start | bytes 786440 | tf_op jit(solution)/shard_map/ppermute | solution.py:483
  126.5 14.6 %collective-permute-start = (bf16[64,2048]{1,0:T(8,128)(2,1)S(1)}, bf16[64,2048]{1,0:T(8,128)(2,1)S(1)}, u32[]{:S(2)}, u32[]{:S(2)}) collective-permute-start(bf16[64,2048]{1,0:T(8,128)(2,1)S(1)} %get-tuple-element.47.high), channel_id=1, source_target_pairs={{0,1},{1,2},{2,3},{3,0},{4,5},{5,6},{6,7},{7,4},{8,9},{9,10},{10,1... | collective-permute-start | bytes 786440 | tf_op jit(solution)/shard_map/ppermute | solution.py:480
  134.8 8.1 %collective-permute-start.6 = (bf16[64,2048]{1,0:T(8,128)(2,1)S(1)}, bf16[64,2048]{1,0:T(8,128)(2,1)S(1)}, u32[]{:S(2)}, u32[]{:S(2)}) collective-permute-start(bf16[64,2048]{1,0:T(8,128)(2,1)S(1)} %get-tuple-element.53), channel_id=1, source_target_pairs={{0,1},{1,2},{2,3},{3,0},{4,5},{5,6},{6,7},{7,4},{8,9},{9,10},{10,1... | collective-permute-start | bytes 786440 | tf_op jit(solution)/shard_map/ppermute | solution.py:480
  135.0 8.2 %collective-permute-start.9 = (bf16[64,2048]{1,0:T(8,128)(2,1)S(1)}, bf16[64,2048]{1,0:T(8,128)(2,1)S(1)}, u32[]{:S(2)}, u32[]{:S(2)}) collective-permute-start(bf16[64,2048]{1,0:T(8,128)(2,1)S(1)} %get-tuple-element.57), channel_id=1, source_target_pairs={{0,3},{1,0},{2,1},{3,2},{4,7},{5,4},{6,5},{7,6},{8,11},{9,8},{10,9... | collective-permute-start | bytes 786440 | tf_op jit(solution)/shard_map/ppermute | solution.py:483
  139.5 7.4 %collective-permute-start.8 = (bf16[64,2048]{1,0:T(8,128)(2,1)S(1)}, bf16[64,2048]{1,0:T(8,128)(2,1)S(1)}, u32[]{:S(2)}, u32[]{:S(2)}) collective-permute-start(bf16[64,2048]{1,0:T(8,128)(2,1)S(1)} %get-tuple-element.54), channel_id=1, source_target_pairs={{0,3},{1,0},{2,1},{3,2},{4,7},{5,4},{6,5},{7,6},{8,11},{9,8},{10,9... | collective-permute-start | bytes 786440 | tf_op jit(solution)/shard_map/ppermute | solution.py:483
  139.7 7.6 %collective-permute-start.11 = (bf16[64,2048]{1,0:T(8,128)(2,1)S(1)}, bf16[64,2048]{1,0:T(8,128)(2,1)S(1)}, u32[]{:S(2)}, u32[]{:S(2)}) collective-permute-start(bf16[64,2048]{1,0:T(8,128)(2,1)S(1)} %get-tuple-element.58), channel_id=1, source_target_pairs={{0,1},{1,2},{2,3},{3,0},{4,5},{5,6},{6,7},{7,4},{8,9},{9,10},{10,1... | collective-permute-start | bytes 786440 | tf_op jit(solution)/shard_map/ppermute | solution.py:480
  143.0 8.5 %collective-permute-start.7 = (bf16[64,2048]{1,0:T(8,128)(2,1)S(1)}, bf16[64,2048]{1,0:T(8,128)(2,1)S(1)}, u32[]{:S(2)}, u32[]{:S(2)}) collective-permute-start(bf16[64,2048]{1,0:T(8,128)(2,1)S(1)} %shard_map.183), channel_id=1, source_target_pairs={{0,1},{1,2},{2,3},{3,0},{4,5},{5,6},{6,7},{7,4},{8,9},{9,10},{10,1... | collective-permute-start | bytes 786440 | tf_op jit(solution)/shard_map/ppermute | solution.py:480
  143.3 9.2 %collective-permute-start.10 = (bf16[64,2048]{1,0:T(8,128)(2,1)S(1)}, bf16[64,2048]{1,0:T(8,128)(2,1)S(1)}, u32[]{:S(2)}, u32[]{:S(2)}) collective-permute-start(bf16[64,2048]{1,0:T(8,128)(2,1)S(1)} %shard_map.185), channel_id=1, source_target_pairs={{0,3},{1,0},{2,1},{3,2},{4,7},{5,4},{6,5},{7,6},{8,11},{9,8},{10,9... | collective-permute-start | bytes 786440 | tf_op jit(solution)/shard_map/ppermute | solution.py:483

commit v6 on v5

--- a/solution.py
+++ b/solution.py
@@ -251,13 +251,15 @@
     return jnp.logical_and(first, placed), jnp.logical_and(second, placed)
 
 
-def route_kernel(routes, share, skip, gain, chosen_ref, hi_ref, lo_ref, skip_ref, gain_ref):
+def route_kernel(routes, share, skip, gain, chosen_ref, pair_ref, skip_ref, gain_ref):
     skip_ref[...] = skip[...]
     gain_ref[...] = gain[...]
     first, second = slot_matrix(routes[...])
     chosen_ref[...] = jnp.logical_or(first, second).astype(F32).astype(BF16)
     weight = jnp.where(first, share[0:1], 0.0) + jnp.where(second, share[1:2], 0.0)
-    hi_ref[...], lo_ref[...] = split_parts(weight)
+    hi, lo = split_parts(weight)
+    both = jnp.concatenate([hi.astype(F32), lo.astype(F32)], axis=1)
+    pair_ref[...] = both.astype(BF16)
 
 
 def dispatch_kernel(parts, skip, gain, chosen, hidden_ref, out):
@@ -325,9 +327,10 @@
     out[half:] = block_of((f(high_a) + f(high_b) + f(high_c)).astype(BF16))
 
 
-def combine_kernel(hidden, back, hi, lo, out):
+def combine_kernel(hidden, back, pair, out):
     rows = rows_of(back[...])
-    mixture = dot(hi[...], rows, (0, 0)) + dot(lo[...], rows, (0, 0))
+    both = dot(pair[...], rows, (0, 0))
+    mixture = both[: out.shape[0]] + both[out.shape[0] :]
     out[...] = (hidden[...].astype(F32) + mixture).astype(BF16)
 
 
@@ -403,9 +406,9 @@
     by_slice = lax.all_to_all(summary, ZG, 0, 0, tiled=True)
     slots = experts * CAP
     head_gain = channel_scale_vector.reshape(1, joint)
-    chosen, share_hi, share_lo, skip, norm_gain = pl.pallas_call(
+    chosen, share_pair, skip, norm_gain = pl.pallas_call(
         route_kernel,
-        out_shape=[near((slots, rows), BF16)] * 3
+        out_shape=[near((slots, rows), BF16), near((slots, 2 * rows), BF16)]
         + [near((rows, model), BF16), near((1, model), F32)],
         compiler_params=params(),
         cost_estimate=cost(1 << 20),
@@ -535,7 +538,7 @@
         out_shape=sds((rows, model), BF16),
         compiler_params=params(),
         cost_estimate=cost(16 << 20),
-    )(*nearby(hidden, back, share_hi, share_lo))
+    )(*nearby(hidden, back, share_pair))
 
 
 def solution(mesh):

time: 195 us -> 195 us (level)
  no operation moved by 1% of the time
where the time goes in v6:
time: 195 us; the launch traced here: 194 us
  blocking collectives  127 us (65%)
  starting transfers between devices  24.4 us (13%)
  Pallas kernels  21 us (11%)
  waiting for transfers between devices  20.7 us (11%)
    all_to_all x1, blocking collectives, local(): back = lax.all_to_all(summed, SP, 0, 0, tiled=True)  40.2 us
    all_to_all x1, blocking collectives, local(): own = lax.all_to_all(outgoing, SP, 0, 0, tiled=True)  39.2 us
    all_to_all x1, blocking collectives, local(): by_slice = lax.all_to_all(summary, ZG, 0, 0, tiled=True)  28.9 us
    all_to_all x1, blocking collectives, local(): came = lax.all_to_all(total, 'zh', 0, 0, tiled=True)  18.2 us
    pallas_call x8, Pallas kernels, call(): pl.pallas_call(kernel, compiler_params=params(), cost_estimate=cost(flops...  11.1 us
    ppermute x6, starting transfers between devices, down(): return lax.ppermute(x, 'tp', down_ring)  10.6 us
    ppermute x6, waiting for transfers between devices, up(): return lax.ppermute(x, 'tp', up_ring)  10.6 us
    all_to_all x1, waiting for transfers between devices, local(): lax.all_to_all(mixed.reshape(shards, rows, model), 'tp', 0, 0, tiled=True)  6.85 us
  transfers between devices with their start and end apart: 14, of which 7 were waited for; matrix products, arithmetic and copies ran while one was open for 1% of the time, Pallas kernels for 8%

profile of v6, /device:TPU:33, one launch (start us, length us, event | category | flops | bytes accessed | tf_op | source)
XLA Modules:
  0.0 194.0 jit_solution(17665909109016896430)
XLA Ops:
  0.0 1.7 shard_map.172
  1.7 28.9 %all_to_all.30.got = bf16[8,80,128]{2,1,0:T(8,128)(2,1)S(1)} all-to-all(bf16[8,80,128]{2,1,0:T(8,128)(2,1)S(1)} %shard_map.172), channel_id=1, replica_groups=mesh['grp'=2,'zh'=4,'zl'=4,'c'=2,'tp'=4] {'zl','c'}, dimensions={0} | all-to-all | bytes 327680 | tf_op jit(solution)/shard_map/all_to_all | solution.py:406
  30.8 18.2 %all_to_all.31.totals = bf16[4,80,128]{2,1,0:T(8,128)(2,1)S(1)} all-to-all(bf16[4,80,128]{2,1,0:T(8,128)(2,1)S(1)} %get-tuple-element.32), channel_id=1, replica_groups=mesh['grp'=2,'zh'=4,'zl'=4,'c'=2,'tp'=4] {'zh'}, dimensions={0} | all-to-all | bytes 163840 | tf_op jit(solution)/shard_map/all_to_all | solution.py:456
  49.0 0.8 shard_map.174
  49.8 6.0 %all-to-all-start.2 = ((bf16[8,64,128]{2,1,0:T(8,128)(2,1)}), bf16[8,64,128]{2,1,0:T(8,128)(2,1)S(1)}, u32[]{:S(2)}, u32[]{:S(2)}) async-start(bf16[8,64,128]{2,1,0:T(8,128)(2,1)} %shard_map.174), calls=%async_computation.2 | async-start | bytes 262144 | tf_op jit(solution)/shard_map/all_to_all | solution.py:463
  55.8 1.2 reshape.9.gain
  57.0 3.1 %shard_map.175 = (f32[128,384]{1,0:T(8,128)S(1)}, bf16[128,256]{1,0:T(8,128)(2,1)S(1)}, bf16[128,256]{1,0:T(8,128)(2,1)S(1)}, f32[128,384]{1,0:T(8,128)S(1)}, bf16[384,2048]{1,0:T(8,128)(2,1)S(1)}) custom-call(bf16[128,128]{1,0:T(8,128)(2,1)} %wp.1, bf16[128,128]{1,0:T(8,128)(2,1)} %np_.1, bf16[128,128]{1,0:T(8,128)(2,1)} %wd.3, bf16[128,128]{1,0:T(8,128)(2,1)} %nd.3, ...), custom_call_target="tpu_custom_call" | custom-call | flops 67108864 | bytes 1048576 | tf_op jit(solution)/shard_map/pallas_call | solution.py:423
  60.1 1.5 all-to-all-done.2.states
  61.5 1.5 shard_map.176
  63.1 4.3 %all-to-all-start.3 = ((bf16[4,32,2048]{2,1,0:T(8,128)(2,1)}), bf16[4,32,2048]{2,1,0:T(8,128)(2,1)S(1)}, u32[]{:S(2)}, u32[]{:S(2)}) async-start(bf16[4,32,2048]{2,1,0:T(8,128)(2,1)} %bitcast.1), calls=%async_computation.3 | async-start | bytes 1048576 | tf_op jit(solution)/shard_map/all_to_all | solution.py:470
  67.3 1.2 shard_map.177
  68.5 6.8 %all-to-all-done.3.parts = bf16[4,32,2048]{2,1,0:T(8,128)(2,1)S(1)} async-done(((bf16[4,32,2048]{2,1,0:T(8,128)(2,1)}), bf16[4,32,2048]{2,1,0:T(8,128)(2,1)S(1)}, u32[]{:S(2)}, u32[]{:S(2)}) %all-to-all-start.3) | async-done | bytes 524320 | tf_op jit(solution)/shard_map/all_to_all | solution.py:470
  75.4 0.5 shard_map.178
  75.9 39.2 %all_to_all.32.got = bf16[32,4,2048]{2,1,0:T(4,128)(2,1)S(1)} all-to-all(bf16[32,4,2048]{2,1,0:T(4,128)(2,1)S(1)} %get-tuple-element.44), channel_id=1, replica_groups=mesh['grp'=2,'zh'=4,'zl'=4,'c'=2,'tp'=4] {'zh','zl','c'}, dimensions={0} | all-to-all | bytes 1048576 | tf_op jit(solution)/shard_map/all_to_all | solution.py:477
  115.1 0.4 collective-permute-start.2
  115.5 2.4 %collective-permute-start.4 = (bf16[64,2048]{1,0:T(8,128)(2,1)S(1)}, bf16[64,2048]{1,0:T(8,128)(2,1)S(1)}, u32[]{:S(2)}, u32[]{:S(2)}) collective-permute-start(bf16[64,2048]{1,0:T(8,128)(2,1)S(1)} %get-tuple-element.46.high), channel_id=1, source_target_pairs={{0,3},{1,0},{2,1},{3,2},{4,7},{5,4},{6,5},{7,6},{8,11},{9,8},{10,9... | collective-permute-start | bytes 786440 | tf_op jit(solution)/shard_map/ppermute | solution.py:486
  117.9 5.9 %collective-permute-done.2.x = bf16[64,2048]{1,0:T(8,128)(2,1)S(1)} collective-permute-done((bf16[64,2048]{1,0:T(8,128)(2,1)S(1)}, bf16[64,2048]{1,0:T(8,128)(2,1)S(1)}, u32[]{:S(2)}, u32[]{:S(2)}) %collective-permute-start.2) | collective-permute-done | bytes 262176 | tf_op jit(solution)/shard_map/ppermute | solution.py:483
  123.8 2.7 %collective-permute-start.5 = (bf16[64,2048]{1,0:T(8,128)(2,1)S(1)}, bf16[64,2048]{1,0:T(8,128)(2,1)S(1)}, u32[]{:S(2)}, u32[]{:S(2)}) collective-permute-start(bf16[64,2048]{1,0:T(8,128)(2,1)S(1)} %collective-permute-done.4.y), channel_id=1, source_target_pairs={{0,3},{1,0},{2,1},{3,2},{4,7},{5,4},{6,5},{7,6},{8,11},{9,8},{10,9... | collective-permute-start | bytes 786440 | tf_op jit(solution)/shard_map/ppermute | solution.py:486
  126.5 1.4 collective-permute-start
  128.0 5.0 %shard_map.180 = (bf16[64,2048]{1,0:T(8,128)(2,1)S(1)}, bf16[64,2048]{1,0:T(8,128)(2,1)S(1)}, bf16[2048,896]{1,0:T(8,128)(2,1)S(1)}, bf16[2048,896]{1,0:T(8,128)(2,1)S(1)}, bf16[896,2048]{1,0:T(8,128)(2,1)S(1)}) custom-call(bf16[64,2048]{1,0:T(8,128)(2,1)S(1)} %get-tuple-element.45.low, bf16[64,2048]{1,0:T(8,128)(2,1)S(1)} %get-tuple-element.46.high, ...), custom_call_target="tpu_custom_call" | custom-call | flops 2147483648 | bytes 1048576 | tf_op jit(solution)/shard_map/pallas_call | solution.py:493
  133.0 1.9 shard_map.182
  135.0 2.6 %collective-permute-start.9 = (bf16[64,2048]{1,0:T(8,128)(2,1)S(1)}, bf16[64,2048]{1,0:T(8,128)(2,1)S(1)}, u32[]{:S(2)}, u32[]{:S(2)}) collective-permute-start(bf16[64,2048]{1,0:T(8,128)(2,1)S(1)} %get-tuple-element.56), channel_id=1, source_target_pairs={{0,3},{1,0},{2,1},{3,2},{4,7},{5,4},{6,5},{7,6},{8,11},{9,8},{10,9... | collective-permute-start | bytes 786440 | tf_op jit(solution)/shard_map/ppermute | solution.py:486
  137.6 1.9 shard_map.184
  139.7 1.4 collective-permute-start.11
  141.1 1.9 shard_map.181
  143.3 2.8 %collective-permute-start.10 = (bf16[64,2048]{1,0:T(8,128)(2,1)S(1)}, bf16[64,2048]{1,0:T(8,128)(2,1)S(1)}, u32[]{:S(2)}, u32[]{:S(2)}) collective-permute-start(bf16[64,2048]{1,0:T(8,128)(2,1)S(1)} %shard_map.185), channel_id=1, source_target_pairs={{0,3},{1,0},{2,1},{3,2},{4,7},{5,4},{6,5},{7,6},{8,11},{9,8},{10,9... | collective-permute-start | bytes 786440 | tf_op jit(solution)/shard_map/ppermute | solution.py:486
  146.0 0.9 collective-permute-done.8.low_c
  146.9 0.4 collective-permute-done.11.high_c
  147.3 4.3 %collective-permute-done.7.low_b = bf16[64,2048]{1,0:T(8,128)(2,1)S(1)} collective-permute-done((bf16[64,2048]{1,0:T(8,128)(2,1)S(1)}, bf16[64,2048]{1,0:T(8,128)(2,1)S(1)}, u32[]{:S(2)}, u32[]{:S(2)}) %collective-permute-start.7) | collective-permute-done | bytes 262176 | tf_op jit(solution)/shard_map/ppermute | solution.py:483
  151.6 0.9 collective-permute-done.10.high_b
  152.9 40.2 %all_to_all.33.back = bf16[32,4,2048]{2,1,0:T(4,128)(2,1)S(1)} all-to-all(bf16[32,4,2048]{2,1,0:T(4,128)(2,1)S(1)} %shard_map.186), channel_id=1, replica_groups=mesh['grp'=2,'zh'=4,'zl'=4,'c'=2,'tp'=4] {'zh','zl','c'}, dimensions={0} | all-to-all | bytes 1048576 | tf_op jit(solution)/shard_map/all_to_all | solution.py:535
  193.1 0.9 shard_map.187
  (17 shorter events, 1.2 us)
Async XLA Ops:
  49.8 11.7 %all-to-all-start.2 = ((bf16[8,64,128]{2,1,0:T(8,128)(2,1)}), bf16[8,64,128]{2,1,0:T(8,128)(2,1)S(1)}, u32[]{:S(2)}, u32[]{:S(2)}) async-start(bf16[8,64,128]{2,1,0:T(8,128)(2,1)} %shard_map.174), calls=%async_computation.2 | async-start | bytes 262144 | tf_op jit(solution)/shard_map/all_to_all | solution.py:463
  63.1 12.3 %all-to-all-start.3 = ((bf16[4,32,2048]{2,1,0:T(8,128)(2,1)}), bf16[4,32,2048]{2,1,0:T(8,128)(2,1)S(1)}, u32[]{:S(2)}, u32[]{:S(2)}) async-start(bf16[4,32,2048]{2,1,0:T(8,128)(2,1)} %bitcast.1), calls=%async_computation.3 | async-start | bytes 1048576 | tf_op jit(solution)/shard_map/all_to_all | solution.py:470
  115.1 8.7 %collective-permute-start.2 = (bf16[64,2048]{1,0:T(8,128)(2,1)S(1)}, bf16[64,2048]{1,0:T(8,128)(2,1)S(1)}, u32[]{:S(2)}, u32[]{:S(2)}) collective-permute-start(bf16[64,2048]{1,0:T(8,128)(2,1)S(1)} %get-tuple-element.45.low), channel_id=1, source_target_pairs={{0,1},{1,2},{2,3},{3,0},{4,5},{5,6},{6,7},{7,4},{8,9},{9,10},{10,1... | collective-permute-start | bytes 786440 | tf_op jit(solution)/shard_map/ppermute | solution.py:483
  115.5 8.3 %collective-permute-start.4 = (bf16[64,2048]{1,0:T(8,128)(2,1)S(1)}, bf16[64,2048]{1,0:T(8,128)(2,1)S(1)}, u32[]{:S(2)}, u32[]{:S(2)}) collective-permute-start(bf16[64,2048]{1,0:T(8,128)(2,1)S(1)} %get-tuple-element.46.high), channel_id=1, source_target_pairs={{0,3},{1,0},{2,1},{3,2},{4,7},{5,4},{6,5},{7,6},{8,11},{9,8},{10,9... | collective-permute-start | bytes 786440 | tf_op jit(solution)/shard_map/ppermute | solution.py:486
  123.8 9.1 %collective-permute-start.3 = (bf16[64,2048]{1,0:T(8,128)(2,1)S(1)}, bf16[64,2048]{1,0:T(8,128)(2,1)S(1)}, u32[]{:S(2)}, u32[]{:S(2)}) collective-permute-start(bf16[64,2048]{1,0:T(8,128)(2,1)S(1)} %collective-permute-done.2.x), channel_id=1, source_target_pairs={{0,1},{1,2},{2,3},{3,0},{4,5},{5,6},{6,7},{7,4},{8,9},{9,10},{10,1... | collective-permute-start | bytes 786440 | tf_op jit(solution)/shard_map/ppermute | solution.py:483
  123.8 9.1 %collective-permute-start.5 = (bf16[64,2048]{1,0:T(8,128)(2,1)S(1)}, bf16[64,2048]{1,0:T(8,128)(2,1)S(1)}, u32[]{:S(2)}, u32[]{:S(2)}) collective-permute-start(bf16[64,2048]{1,0:T(8,128)(2,1)S(1)} %collective-permute-done.4.y), channel_id=1, source_target_pairs={{0,3},{1,0},{2,1},{3,2},{4,7},{5,4},{6,5},{7,6},{8,11},{9,8},{10,9... | collective-permute-start | bytes 786440 | tf_op jit(solution)/shard_map/ppermute | solution.py:486
  126.5 13.1 %collective-permute-start.1 = (bf16[64,2048]{1,0:T(8,128)(2,1)S(1)}, bf16[64,2048]{1,0:T(8,128)(2,1)S(1)}, u32[]{:S(2)}, u32[]{:S(2)}) collective-permute-start(bf16[64,2048]{1,0:T(8,128)(2,1)S(1)} %get-tuple-element.45.low), channel_id=1, source_target_pairs={{0,3},{1,0},{2,1},{3,2},{4,7},{5,4},{6,5},{7,6},{8,11},{9,8},{10,9... | collective-permute-start | bytes 786440 | tf_op jit(solution)/shard_map/ppermute | solution.py:486
  126.5 14.6 %collective-permute-start = (bf16[64,2048]{1,0:T(8,128)(2,1)S(1)}, bf16[64,2048]{1,0:T(8,128)(2,1)S(1)}, u32[]{:S(2)}, u32[]{:S(2)}) collective-permute-start(bf16[64,2048]{1,0:T(8,128)(2,1)S(1)} %get-tuple-element.46.high), channel_id=1, source_target_pairs={{0,1},{1,2},{2,3},{3,0},{4,5},{5,6},{6,7},{7,4},{8,9},{9,10},{10,1... | collective-permute-start | bytes 786440 | tf_op jit(solution)/shard_map/ppermute | solution.py:483
  134.8 8.1 %collective-permute-start.6 = (bf16[64,2048]{1,0:T(8,128)(2,1)S(1)}, bf16[64,2048]{1,0:T(8,128)(2,1)S(1)}, u32[]{:S(2)}, u32[]{:S(2)}) collective-permute-start(bf16[64,2048]{1,0:T(8,128)(2,1)S(1)} %get-tuple-element.52), channel_id=1, source_target_pairs={{0,1},{1,2},{2,3},{3,0},{4,5},{5,6},{6,7},{7,4},{8,9},{9,10},{10,1... | collective-permute-start | bytes 786440 | tf_op jit(solution)/shard_map/ppermute | solution.py:483
  135.0 8.2 %collective-permute-start.9 = (bf16[64,2048]{1,0:T(8,128)(2,1)S(1)}, bf16[64,2048]{1,0:T(8,128)(2,1)S(1)}, u32[]{:S(2)}, u32[]{:S(2)}) collective-permute-start(bf16[64,2048]{1,0:T(8,128)(2,1)S(1)} %get-tuple-element.56), channel_id=1, source_target_pairs={{0,3},{1,0},{2,1},{3,2},{4,7},{5,4},{6,5},{7,6},{8,11},{9,8},{10,9... | collective-permute-start | bytes 786440 | tf_op jit(solution)/shard_map/ppermute | solution.py:486
  139.5 7.4 %collective-permute-start.8 = (bf16[64,2048]{1,0:T(8,128)(2,1)S(1)}, bf16[64,2048]{1,0:T(8,128)(2,1)S(1)}, u32[]{:S(2)}, u32[]{:S(2)}) collective-permute-start(bf16[64,2048]{1,0:T(8,128)(2,1)S(1)} %get-tuple-element.53), channel_id=1, source_target_pairs={{0,3},{1,0},{2,1},{3,2},{4,7},{5,4},{6,5},{7,6},{8,11},{9,8},{10,9... | collective-permute-start | bytes 786440 | tf_op jit(solution)/shard_map/ppermute | solution.py:486
  139.7 7.6 %collective-permute-start.11 = (bf16[64,2048]{1,0:T(8,128)(2,1)S(1)}, bf16[64,2048]{1,0:T(8,128)(2,1)S(1)}, u32[]{:S(2)}, u32[]{:S(2)}) collective-permute-start(bf16[64,2048]{1,0:T(8,128)(2,1)S(1)} %get-tuple-element.57), channel_id=1, source_target_pairs={{0,1},{1,2},{2,3},{3,0},{4,5},{5,6},{6,7},{7,4},{8,9},{9,10},{10,1... | collective-permute-start | bytes 786440 | tf_op jit(solution)/shard_map/ppermute | solution.py:483
  143.0 8.5 %collective-permute-start.7 = (bf16[64,2048]{1,0:T(8,128)(2,1)S(1)}, bf16[64,2048]{1,0:T(8,128)(2,1)S(1)}, u32[]{:S(2)}, u32[]{:S(2)}) collective-permute-start(bf16[64,2048]{1,0:T(8,128)(2,1)S(1)} %shard_map.183), channel_id=1, source_target_pairs={{0,1},{1,2},{2,3},{3,0},{4,5},{5,6},{6,7},{7,4},{8,9},{9,10},{10,1... | collective-permute-start | bytes 786440 | tf_op jit(solution)/shard_map/ppermute | solution.py:483
  143.3 9.2 %collective-permute-start.10 = (bf16[64,2048]{1,0:T(8,128)(2,1)S(1)}, bf16[64,2048]{1,0:T(8,128)(2,1)S(1)}, u32[]{:S(2)}, u32[]{:S(2)}) collective-permute-start(bf16[64,2048]{1,0:T(8,128)(2,1)S(1)} %shard_map.185), channel_id=1, source_target_pairs={{0,3},{1,0},{2,1},{3,2},{4,7},{5,4},{6,5},{7,6},{8,11},{9,8},{10,9... | collective-permute-start | bytes 786440 | tf_op jit(solution)/shard_map/ppermute | solution.py:486
